TPU v7x, 256 devices: a whole 4x4x8 slice. The times are simulated.
256 devices in a mesh: fs: 32 (over z, y), tp: 8 (over x, core).
Axes of the slice: x: 4, y: 4, z: 8, core: 2. Of those that a mesh axis runs over, the one named last changes fastest.
Arguments:
- inputs: bfloat16 [65536, 2048], P('fs'), may hold values from -6 to 6
- cotangents: bfloat16 [3, 65536, 1024], P(None, 'fs', 'tp'), as said below
- factor: bfloat16 [2048, 256], P('fs'), as said below
- weights: float32 [3, 2048, 1024], P(None, 'fs', 'tp'), may hold values from -0.125 to 0.125
- first_moment: float32 [3, 256, 1024], P(None, 'fs', 'tp'), may hold values from -0.6 to 0.6
- second_moment: float32 [3, 256, 1024], P(None, 'fs', 'tp'), may hold values from 0.001 to 0.01
Outputs:
- update: float32 [3, 2048, 1024], P(None, 'fs', 'tp')
- new_weights: float32 [3, 2048, 1024], P(None, 'fs', 'tp')
- copies: bfloat16 [3, 2048, 1024], P(None, None, 'tp')
- new_first: float32 [3, 256, 1024], P(None, 'fs', 'tp')
- new_second: float32 [3, 256, 1024], P(None, 'fs', 'tp')
Inputs may be any that keep to these rules, and one draw needn't show every extreme that they name: A real-valued factor of full rank. real-valued cotangents.
All inputs are finite; a program needn't handle non-finite values.
Results may differ from a plain program's by a relative error of at most 0.0085.
Values may be sent and summed in bfloat16 or wider, within the bound.
No kernel may reach another device: no remote copies, remote signals or barrier semaphores. Data moves between devices by JAX's collectives and lax.ppermute only.
A program may use at most 64 MiB of HBM per device.

v0:
```python
import jax
import jax.numpy as jnp
from jax import lax
from jax.sharding import Mesh
from jax.sharding import PartitionSpec as P

MW = 1024
RANK = 256
FS = ("fs_0", "fs_1")
FS_TP = ("fs_0", "fs_1", "tp_0", "tp_1")
TP = ("tp_0", "tp_1")


def joined_along(blocks, dim):
    blocks = jnp.moveaxis(blocks, 0, dim)
    shape = blocks.shape
    return blocks.reshape(*shape[:dim], shape[dim] * shape[dim + 1], *shape[dim + 2 :])


def sent_to_all(array, axis):
    copies = jnp.broadcast_to(array, (lax.axis_size(axis), *array.shape))
    return lax.all_to_all(copies, axis, split_axis=0, concat_axis=0, tiled=True)


def collect(array, axis, dim):
    return joined_along(sent_to_all(array, axis), dim)


def split_up(array, dim, count):
    before, after = (array.shape[:dim], array.shape[dim + 1 :])
    return jnp.moveaxis(array.reshape(*before, count, -1, *after), dim, 0)


def sent_and_summed(array, axis, dim):
    blocks = split_up(array, dim, lax.axis_size(axis))
    arrived = lax.all_to_all(blocks, axis, split_axis=0, concat_axis=0, tiled=True)
    return arrived.sum(axis=0)


def over_axes(array, axes):
    for axis in axes:
        array = lax.psum(array, axis)
    return array


def on_device(inputs, cotangents, factor, weights, first_moment, second_moment):
    factor_wide = factor.astype(jnp.float32)
    local_gradient = jnp.einsum(
        "td,mtc->dmc", inputs, cotangents, preferred_element_type=jnp.float32
    )
    gradient_high = local_gradient.astype(jnp.bfloat16)
    gradient_low = (local_gradient - gradient_high.astype(jnp.float32)).astype(jnp.bfloat16)
    factor_piece = collect(factor, FS, 0)
    high_term = jnp.einsum(
        "dr,dmc->rmc", factor_piece, gradient_high, preferred_element_type=jnp.float32
    )
    low_term = jnp.einsum(
        "dr,dmc->rmc", factor_piece, gradient_low, preferred_element_type=jnp.float32
    )
    partial_value = high_term + low_term
    summed = sent_and_summed(partial_value, FS, 0)
    projected = jnp.transpose(summed, (1, 0, 2))
    square_sum = over_axes(jnp.sum(projected * projected), FS_TP)
    root_mean = jnp.sqrt(square_sum / (3 * RANK * MW) + 1e-06)
    clip_factor = jnp.minimum(1.0, 0.25 / root_mean)
    clipped = clip_factor * projected
    new_first = 0.9 * first_moment + 0.1 * clipped
    new_second = 0.95 * second_moment + 0.05 * clipped * clipped
    normed = new_first / (jnp.sqrt(new_second) + 1e-08)
    normed_whole = collect(normed, FS, 1)
    update = jnp.einsum("dr,mrc->mdc", factor_wide, normed_whole)
    new_weights = weights - 0.02 * update
    copies = collect(new_weights.astype(jnp.bfloat16), FS, 1)
    return (update, new_weights, copies, new_first, new_second)


def solution(mesh):
    torus = Mesh(mesh.devices.reshape(8, 4, 4, 2), ("fs_0", "fs_1", "tp_0", "tp_1"))
    return jax.shard_map(
        on_device,
        mesh=torus,
        in_specs=(
            P(FS, None),
            P(None, FS, TP),
            P(FS, None),
            P(None, FS, TP),
            P(None, FS, TP),
            P(None, FS, TP),
        ),
        out_specs=(
            P(None, FS, TP),
            P(None, FS, TP),
            P(None, None, TP),
            P(None, FS, TP),
            P(None, FS, TP),
        ),
        check_vma=False,
    )
```

profile of v0, /device:TPU:32, one launch (start us, length us, event | category | flops | bytes accessed | tf_op | source)
XLA Modules:
  0.0 169.0 jit_solution(2127882930247664799)
XLA Ops:
  0.6 0.0 copy-start
  0.6 2.0 %broadcast_in_dim.9 = bf16[32,64,256]{2,1,0:T(8,128)(2,1)} broadcast(bf16[64,256]{1,0:T(8,128)(2,1)} %param.8), dimensions={1,2} | broadcast | bytes 1081344 | tf_op jit(solution)/shard_map/broadcast_in_dim | solution.py:21
  2.6 11.4 %all-to-all-start = ((bf16[32,64,256]{2,1,0:T(8,128)(2,1)}), bf16[32,64,256]{2,1,0:T(8,128)(2,1)S(1)}, u32[]{:S(2)}, u32[]{:S(2)}) async-start(bf16[32,64,256]{2,1,0:T(8,128)(2,1)} %broadcast_in_dim.9), calls=%async_computation | async-start | bytes 2097152 | tf_op jit(solution)/shard_map/all_to_all | solution.py:22
  14.0 0.0 copy-done
  14.0 8.6 %fusion = f32[2048,3,128]{2,0,1:T(8,128)} fusion(bf16[3,2048,128]{2,1,0:T(8,128)(2,1)S(1)} %copy-done, bf16[2048,2048]{1,0:T(8,128)(2,1)} %param.6), kind=kOutput, calls=%fused_computation | convolution fusion | flops 3221225472 | bytes 13107200 | tf_op jit(solution)/shard_map/td,mtc->dmc/dot_general | solution.py:48
  22.6 18.5 %all-to-all-done = bf16[32,64,256]{2,1,0:T(8,128)(2,1)S(1)} async-done(((bf16[32,64,256]{2,1,0:T(8,128)(2,1)}), bf16[32,64,256]{2,1,0:T(8,128)(2,1)S(1)}, u32[]{:S(2)}, u32[]{:S(2)}) %all-to-all-start) | async-done | bytes 1048608 | tf_op jit(solution)/shard_map/all_to_all | solution.py:22
  41.2 0.0 copy-start.1
  41.2 2.7 %fusion.6 = f32[3,128,256]{2,1,0:T(8,128)S(1)} fusion(bf16[2048,256,1]{1,0,2:T(8,128)(2,1)S(1)} %bitcast.38, f32[2048,3,128]{2,0,1:T(8,128)} %fusion), kind=kOutput, calls=%fused_computation.8 | convolution fusion | flops 403439616 | bytes 4587520 | tf_op jit(solution)/shard_map/dr,dmc->rmc/dot_general | solution.py:54
  43.8 0.1 copy-done.1
  44.0 0.0 copy-start.4
  44.0 0.0 copy-start.5
  44.0 0.0 copy-start.2
  44.0 0.0 copy-start.3
  44.0 0.6 fusion.4
  44.7 0.2 copy.27
  44.9 19.9 %all_to_all.20 = f32[32,8,3,128]{3,1,2,0:T(8,128)S(1)} all-to-all(f32[32,8,3,128]{3,1,2,0:T(8,128)S(1)} %copy.28), channel_id=1, replica_groups=mesh['fs_0'=8,'fs_1'=4,'tp_0'=4,'tp_1'=2] {'fs_0','fs_1'}, dimensions={0} | all-to-all | bytes 786432 | tf_op jit(solution)/shard_map/all_to_all | solution.py:36
  64.8 0.6 multiply_reduce_fusion
  65.4 15.6 %psum.28 = f32[]{:T(128)} all-reduce(f32[]{:T(128)} %multiply_reduce_fusion), channel_id=1, replica_groups=mesh['fs_0'=8,'fs_1'=4,'tp_0'=4,'tp_1'=2] {'fs_0'}, use_global_device_ids=true, to_apply=%region_2.0 | all-reduce | flops 1 | bytes 8 | tf_op jit(solution)/shard_map/psum | solution.py:42
  81.0 10.1 %psum.29 = f32[]{:T(128)} all-reduce(f32[]{:T(128)} %psum.28), channel_id=1, replica_groups=mesh['fs_0'=8,'fs_1'=4,'tp_0'=4,'tp_1'=2] {'fs_1'}, use_global_device_ids=true, to_apply=%region_3.0 | all-reduce | flops 1 | bytes 8 | tf_op jit(solution)/shard_map/psum | solution.py:42
  91.0 11.1 %psum.30 = f32[]{:T(128)} all-reduce(f32[]{:T(128)} %psum.29), channel_id=1, replica_groups=mesh['fs_0'=8,'fs_1'=4,'tp_0'=4,'tp_1'=2] {'tp_0'}, use_global_device_ids=true, to_apply=%region_4.0 | all-reduce | flops 1 | bytes 8 | tf_op jit(solution)/shard_map/psum | solution.py:42
  102.1 3.1 %psum.31 = f32[]{:T(128)} all-reduce(f32[]{:T(128)} %psum.30), channel_id=1, replica_groups=mesh['fs_0'=8,'fs_1'=4,'tp_0'=4,'tp_1'=2] {'tp_1'}, use_global_device_ids=true, to_apply=%region_5.0 | all-reduce | flops 1 | bytes 8 | tf_op jit(solution)/shard_map/psum | solution.py:42
  105.9 0.0 copy-done.4
  105.9 0.0 copy-done.5
  105.9 0.6 add_divide_fusion
  106.6 16.5 %all_to_all.21 = bf16[32,3,8,128]{3,2,1,0:T(8,128)(2,1)S(1)} all-to-all(bf16[32,3,8,128]{3,2,1,0:T(8,128)(2,1)S(1)} %broadcast_in_dim.10), channel_id=1, replica_groups=mesh['fs_0'=8,'fs_1'=4,'tp_0'=4,'tp_1'=2] {'fs_0','fs_1'}, dimensions={0} | all-to-all | bytes 393216 | tf_op jit(solution)/shard_map/all_to_all | solution.py:22
  123.1 0.0 copy-done.2
  123.1 0.0 copy-done.3
  123.1 0.8 fusion.13
  123.9 0.4 broadcast_in_dim.11
  124.3 43.4 %all_to_all.22 = bf16[32,3,64,128]{3,2,1,0:T(8,128)(2,1)S(1)} all-to-all(bf16[32,3,64,128]{3,2,1,0:T(8,128)(2,1)S(1)} %broadcast_in_dim.11), channel_id=1, replica_groups=mesh['fs_0'=8,'fs_1'=4,'tp_0'=4,'tp_1'=2] {'fs_0','fs_1'}, dimensions={0} | all-to-all | bytes 3145728 | tf_op jit(solution)/shard_map/all_to_all | solution.py:22
  167.7 1.3 copy.30
  (3 shorter events, 0.1 us)
Async XLA Ops:
  0.6 13.4 %copy-start = (bf16[3,2048,128]{2,1,0:T(8,128)(2,1)S(1)}, bf16[3,2048,128]{2,1,0:T(8,128)(2,1)}, u32[]{:S(2)}) copy-start(bf16[3,2048,128]{2,1,0:T(8,128)(2,1)} %param.7) | copy-start | bytes 4718596
  2.6 38.5 %all-to-all-start = ((bf16[32,64,256]{2,1,0:T(8,128)(2,1)}), bf16[32,64,256]{2,1,0:T(8,128)(2,1)S(1)}, u32[]{:S(2)}, u32[]{:S(2)}) async-start(bf16[32,64,256]{2,1,0:T(8,128)(2,1)} %broadcast_in_dim.9), calls=%async_computation | async-start | bytes 2097152 | tf_op jit(solution)/shard_map/all_to_all | solution.py:22
  41.2 2.8 %copy-start.1 = (f32[2048,3,128]{2,0,1:T(8,128)S(1)}, f32[2048,3,128]{2,0,1:T(8,128)}, u32[]{:S(2)}) copy-start(f32[2048,3,128]{2,0,1:T(8,128)} %fusion) | copy-start | bytes 9437188
  44.0 61.9 %copy-start.4 = (f32[3,8,128]{2,1,0:T(8,128)S(1)}, f32[3,8,128]{2,1,0:T(8,128)}, u32[]{:S(2)}) copy-start(f32[3,8,128]{2,1,0:T(8,128)} %param.11) | copy-start | bytes 36868
  44.0 61.9 %copy-start.5 = (f32[3,8,128]{2,1,0:T(8,128)S(1)}, f32[3,8,128]{2,1,0:T(8,128)}, u32[]{:S(2)}) copy-start(f32[3,8,128]{2,1,0:T(8,128)} %param.10) | copy-start | bytes 36868
  44.0 79.1 %copy-start.2 = (bf16[64,256]{1,0:T(8,128)(2,1)S(1)}, bf16[64,256]{1,0:T(8,128)(2,1)}, u32[]{:S(2)}) copy-start(bf16[64,256]{1,0:T(8,128)(2,1)} %param.8) | copy-start | bytes 98308
  44.0 79.1 %copy-start.3 = (f32[3,64,128]{2,1,0:T(8,128)S(1)}, f32[3,64,128]{2,1,0:T(8,128)}, u32[]{:S(2)}) copy-start(f32[3,64,128]{2,1,0:T(8,128)} %param.9) | copy-start | bytes 294916
where the time goes:
time: 169 us
  blocking collectives  120 us (71%)
  waiting for transfers between devices  18.5 us (11%)
  matrix products  12.8 us (8%)
  starting transfers between devices  11.4 us (7%)
  local copies, waits for them, and re-layouts  4.01 us (2%)
    all_to_all x2, blocking collectives, sent_to_all(): return lax.all_to_all(copies, axis, split_axis=0, concat_axis=0, tiled=True)  59.9 us
    psum x4, blocking collectives, over_axes(): array = lax.psum(array, axis)  39.8 us
    all_to_all x1, blocking collectives, sent_and_summed(): lax.all_to_all(blocks, axis, split_axis=0, concat_axis=0, tiled=True)  19.9 us
    all_to_all x1, waiting for transfers between devices, sent_to_all(): return lax.all_to_all(copies, axis, split_axis=0, concat_axis=0, tiled=True)  18.5 us
    all_to_all x1, starting transfers between devices, sent_to_all(): return lax.all_to_all(copies, axis, split_axis=0, concat_axis=0, tiled=True)  11.4 us
    dot_general x1, matrix products, on_device(): jnp.einsum('td,mtc->dmc', inputs, cotangents, preferred_element_type=jnp....  8.65 us
  transfers between devices with their start and end apart: 1, of which 1 were waited for; matrix products, arithmetic and copies ran while one was open for 5% of the time, Pallas kernels for 0%

commit v1 on v0

v1 whole, which is shorter than its diff:
```python
import jax
import jax.numpy as jnp
from jax import lax
from jax.sharding import Mesh
from jax.sharding import PartitionSpec as P

MW = 1024
RANK = 256
Z, Y = ("fs_0", "fs_1")
FS = ("fs_0", "fs_1")
TP = ("tp_0", "tp_1")
BF = jnp.bfloat16


def sent_to_all(array, axis):
    copies = jnp.broadcast_to(array, (lax.axis_size(axis), *array.shape))
    return lax.all_to_all(copies, axis, split_axis=0, concat_axis=0, tiled=True)


def staged(array):
    return sent_to_all(sent_to_all(array, Z), Y)


def on_device(inputs, cotangents, factor, weights, first_moment, second_moment):
    with jax.named_scope("factor_gather"):
        factor_all = jnp.transpose(staged(factor), (1, 0, 2, 3)).reshape(-1, RANK)
    with jax.named_scope("gradient"):
        local_gradient = jnp.einsum(
            "td,mtc->dmc", inputs, cotangents, preferred_element_type=jnp.float32
        )
        gradient_high = local_gradient.astype(BF)
        gradient_low = (local_gradient - gradient_high.astype(jnp.float32)).astype(BF)
    with jax.named_scope("state_gather"):
        state = jnp.concatenate([weights, first_moment, second_moment], axis=1).astype(BF)
        state_all = jnp.transpose(staged(state), (2, 1, 0, 3, 4))
        weights_all = state_all[:, :, :, :64].reshape(3, -1, 128).astype(jnp.float32)
        first_all = state_all[:, :, :, 64:72].reshape(3, -1, 128).astype(jnp.float32)
        second_all = state_all[:, :, :, 72:].reshape(3, -1, 128).astype(jnp.float32)
    with jax.named_scope("partial"):
        high_term = jnp.einsum(
            "dr,dmc->rmc", factor_all, gradient_high, preferred_element_type=jnp.float32
        )
        low_term = jnp.einsum(
            "dr,dmc->rmc", factor_all, gradient_low, preferred_element_type=jnp.float32
        )
        partial_value = (high_term + low_term).astype(BF).reshape(32, 8, 3, 128)
    with jax.named_scope("partial_exchange"):
        arrived = lax.all_to_all(partial_value, FS, split_axis=0, concat_axis=0, tiled=True)
        projected = jnp.transpose(arrived.astype(jnp.float32).sum(axis=0), (1, 0, 2))
    with jax.named_scope("projected_gather"):
        projected_all = sent_to_all(projected.astype(BF), FS)
        projected_all = (
            jnp.transpose(projected_all, (1, 0, 2, 3)).reshape(3, -1, 128).astype(jnp.float32)
        )
    with jax.named_scope("square_sum"):
        square_sum = jnp.sum(projected_all * projected_all)
        square_sum = jnp.sum(sent_to_all(jnp.full((1, 128), square_sum), TP)[:, 0, 0])
        root_mean = jnp.sqrt(square_sum / (3 * RANK * MW) + 1e-06)
        clip_factor = jnp.minimum(1.0, 0.25 / root_mean)

    def moments(projected, first_moment, second_moment):
        clipped = clip_factor * projected
        new_first = 0.9 * first_moment + 0.1 * clipped
        new_second = 0.95 * second_moment + 0.05 * clipped * clipped
        return new_first, new_second, new_first / (jnp.sqrt(new_second) + 1e-08)

    with jax.named_scope("own_moments"):
        new_first, new_second, _ = moments(projected, first_moment, second_moment)
    with jax.named_scope("update"):
        normed = moments(projected_all, first_all, second_all)[2].astype(BF)
        update = jnp.einsum("dr,mrc->mdc", factor, normed, preferred_element_type=jnp.float32)
        new_weights = weights - 0.02 * update
        update_all = jnp.einsum(
            "dr,mrc->mdc", factor_all, normed, preferred_element_type=jnp.float32
        )
        copies = (weights_all - 0.02 * update_all).astype(BF)
    return (update, new_weights, copies, new_first, new_second)


def solution(mesh):
    torus = Mesh(mesh.devices.reshape(8, 4, 4, 2), ("fs_0", "fs_1", "tp_0", "tp_1"))
    return jax.shard_map(
        on_device,
        mesh=torus,
        in_specs=(
            P(FS, None),
            P(None, FS, TP),
            P(FS, None),
            P(None, FS, TP),
            P(None, FS, TP),
            P(None, FS, TP),
        ),
        out_specs=(
            P(None, FS, TP),
            P(None, FS, TP),
            P(None, None, TP),
            P(None, FS, TP),
            P(None, FS, TP),
        ),
        check_vma=False,
    )
```

time: 169 us -> 154 us (0.911); the launches traced: 169 us -> 152 us
  blocking collectives: 120 us -> 68.3 us
  waiting for transfers between devices: 18.5 us -> 32.3 us
  local copies, waits for them, and re-layouts: 4.01 us -> 15.7 us
  matrix products: 12.8 us -> 16.3 us
  other arithmetic: 1.25 us -> 4.51 us
  starting transfers between devices: 11.4 us -> 13.2 us
    psum x4 -> x0, blocking collectives: 39.8 us -> none  [over_axes(): array = lax.psum(array, axis)]
    all_to_all x1 -> x3, waiting for transfers between devices: 18.5 us -> 32.3 us  [sent_to_all(): return lax.all_to_all(copies, axis, split_axis=0, concat_axis=0, tiled=True)]
    all_to_all x2 -> x3, blocking collectives: 59.9 us -> 52.2 us  [sent_to_all(): return lax.all_to_all(copies, axis, split_axis=0, concat_axis=0, tiled=True)]
    all_to_all x1, blocking collectives: 19.9 us -> 16 us  [on_device(): lax.all_to_all(partial_value, FS, split_axis=0, concat_axis=0, tiled=True)]
    convert_element_type x0 -> x2, local copies, waits for them, and re-layouts: none -> 3.71 us  [the longest x1 3.55 us: on_device(): state_all[:, :, :, :64].reshape(3, -1, 128).astype(jnp.float32)]
    dot_general x3 -> x4, matrix products: 4.17 us -> 7.65 us  [the longest x1 3.67 us: on_device(): jnp.einsum('dr,mrc->mdc', factor_all, normed, preferred_element_type=jnp....]
    unnamed x12 -> x15, local copies, waits for them, and re-layouts: 0.17 us -> 3.6 us
    broadcast_in_dim x3 -> x6, local copies, waits for them, and re-layouts: 2.37 us -> 4.92 us  [sent_to_all(): copies = jnp.broadcast_to(array, (lax.axis_size(axis), *array.shape))]
  transfers between devices with their start and end apart: 1 -> 3, of which waited for: 1 -> 3; matrix products, arithmetic and copies ran while one was open for 5% -> 6% of each run, Pallas kernels for 0% -> 0%
where the time goes in v1:
time: 154 us; the launch traced here: 152 us
  blocking collectives  68.3 us (44%)
  waiting for transfers between devices  32.3 us (21%)
  matrix products  16.3 us (11%)
  local copies, waits for them, and re-layouts  15.7 us (10%)
  starting transfers between devices  13.2 us (9%)
  other arithmetic  4.51 us (3%)
    all_to_all x3, blocking collectives, sent_to_all(): return lax.all_to_all(copies, axis, split_axis=0, concat_axis=0, tiled=True)  52.2 us
    all_to_all x3, waiting for transfers between devices, sent_to_all(): return lax.all_to_all(copies, axis, split_axis=0, concat_axis=0, tiled=True)  32.3 us
    all_to_all x1, blocking collectives, on_device(): lax.all_to_all(partial_value, FS, split_axis=0, concat_axis=0, tiled=True)  16 us
    all_to_all x3, starting transfers between devices, sent_to_all(): return lax.all_to_all(copies, axis, split_axis=0, concat_axis=0, tiled=True)  13.2 us
    dot_general x1, matrix products, on_device(): jnp.einsum('td,mtc->dmc', inputs, cotangents, preferred_element_type=jnp....  8.62 us
    broadcast_in_dim x6, local copies, waits for them, and re-layouts, sent_to_all(): copies = jnp.broadcast_to(array, (lax.axis_size(axis), *array.shape))  4.92 us
    dot_general x1, matrix products, on_device(): jnp.einsum('dr,mrc->mdc', factor_all, normed, preferred_element_type=jnp....  3.67 us
    unnamed x15, local copies, waits for them, and re-layouts  3.6 us
  transfers between devices with their start and end apart: 3, of which 3 were waited for; matrix products, arithmetic and copies ran while one was open for 6% of the time, Pallas kernels for 0%

profile of v1, /device:TPU:32, one launch (start us, length us, event | category | flops | bytes accessed | tf_op | source)
XLA Modules:
  0.0 151.8 jit_solution(17173124908381811135)
XLA Ops:
  0.6 0.9 broadcast_in_dim.20
  1.5 18.8 %all_to_all.35 = bf16[8,64,256]{2,1,0:T(8,128)(2,1)S(1)} all-to-all(bf16[8,64,256]{2,1,0:T(8,128)(2,1)S(1)} %broadcast_in_dim.20), channel_id=1, replica_groups=mesh['fs_0'=8,'fs_1'=4,'tp_0'=4,'tp_1'=2] {'fs_0'}, dimensions={0} | all-to-all | bytes 524288 | tf_op jit(solution)/shard_map/factor_gather/all_to_all | solution.py:17
  20.3 1.1 broadcast_in_dim.21
  21.4 4.5 %all-to-all-start.3 = ((bf16[4,8,64,256]{3,2,1,0:T(8,128)(2,1)}), bf16[4,8,64,256]{3,2,1,0:T(8,128)(2,1)S(1)}, u32[]{:S(2)}, u32[]{:S(2)}) async-start(bf16[4,8,64,256]{3,2,1,0:T(8,128)(2,1)} %broadcast_in_dim.21), calls=%async_computation.3 | async-start | bytes 2097152 | tf_op jit(solution)/shard_map/factor_gather/all_to_all | solution.py:17
  25.9 8.6 %fusion = f32[2048,3,128]{2,0,1:T(8,128)} fusion(bf16[3,2048,128]{2,1,0:T(8,128)(2,1)S(1)} %copy-done, bf16[2048,2048]{1,0:T(8,128)(2,1)} %param.6), kind=kOutput, calls=%fused_computation | convolution fusion | flops 3221225472 | bytes 13107200 | tf_op jit(solution)/shard_map/gradient/td,mtc->dmc/dot_general | solution.py:28
  34.5 4.0 %all-to-all-done.3 = bf16[4,8,64,256]{3,2,1,0:T(8,128)(2,1)S(1)} async-done(((bf16[4,8,64,256]{3,2,1,0:T(8,128)(2,1)}), bf16[4,8,64,256]{3,2,1,0:T(8,128)(2,1)S(1)}, u32[]{:S(2)}, u32[]{:S(2)}) %all-to-all-start.3) | async-done | bytes 1048608 | tf_op jit(solution)/shard_map/factor_gather/all_to_all | solution.py:17
  38.5 1.0 copy-done.2
  39.4 1.5 copy.65
  40.9 2.5 %fusion.8 = f32[3,128,256]{2,1,0:T(8,128)S(1)} fusion(bf16[2048,256,1]{1,0,2:T(8,128)(2,1)S(1)} %bitcast.62, f32[2048,3,128]{2,0,1:T(8,128)} %fusion), kind=kOutput, calls=%fused_computation.13 | convolution fusion | flops 403439616 | bytes 4587520 | tf_op jit(solution)/shard_map/partial/dr,dmc->rmc/dot_general | solution.py:40
  43.5 0.6 fusion.6
  44.1 0.2 copy.68
  44.3 16.0 %all_to_all.36 = bf16[32,8,3,128]{3,1,2,0:T(8,128)(2,1)S(1)} all-to-all(bf16[32,8,3,128]{3,1,2,0:T(8,128)(2,1)S(1)} %copy.69), channel_id=1, replica_groups=mesh['fs_0'=8,'fs_1'=4,'tp_0'=4,'tp_1'=2] {'fs_0','fs_1'}, dimensions={0} | all-to-all | bytes 393216 | tf_op jit(solution)/shard_map/partial_exchange/all_to_all | solution.py:48
  60.5 14.5 %all_to_all.37 = bf16[32,3,8,128]{3,2,1,0:T(8,128)(2,1)S(1)} all-to-all(bf16[32,3,8,128]{3,2,1,0:T(8,128)(2,1)S(1)} %broadcast_in_dim.22), channel_id=1, replica_groups=mesh['fs_0'=8,'fs_1'=4,'tp_0'=4,'tp_1'=2] {'fs_0','fs_1'}, dimensions={0} | all-to-all | bytes 393216 | tf_op jit(solution)/shard_map/projected_gather/all_to_all | solution.py:17
  74.9 0.7 fusion.10
  75.6 1.2 broadcast_in_dim.23
  76.9 4.3 %all-to-all-start.6 = ((f32[8,1,128]{2,1,0:T(1,128)}), f32[8,1,128]{2,1,0:T(1,128)S(1)}, u32[]{:S(2)}, u32[]{:S(2)}) async-start(f32[8,1,128]{2,1,0:T(1,128)} %broadcast_in_dim.23), calls=%async_computation.6 | async-start | bytes 8192 | tf_op jit(solution)/shard_map/square_sum/all_to_all | solution.py:17
  81.2 5.2 %all-to-all-done.6 = f32[8,1,128]{2,1,0:T(1,128)S(1)} async-done(((f32[8,1,128]{2,1,0:T(1,128)}), f32[8,1,128]{2,1,0:T(1,128)S(1)}, u32[]{:S(2)}, u32[]{:S(2)}) %all-to-all-start.6) | async-done | bytes 4128 | tf_op jit(solution)/shard_map/square_sum/all_to_all | solution.py:17
  86.4 0.6 slice_reduce_fusion
  87.7 0.6 fusion.23
  88.4 19.0 %all_to_all.38 = bf16[8,3,80,128]{3,2,1,0:T(8,128)(2,1)S(1)} all-to-all(bf16[8,3,80,128]{3,2,1,0:T(8,128)(2,1)S(1)} %broadcast_in_dim.18), channel_id=1, replica_groups=mesh['fs_0'=8,'fs_1'=4,'tp_0'=4,'tp_1'=2] {'fs_0'}, dimensions={0} | all-to-all | bytes 983040 | tf_op jit(solution)/shard_map/state_gather/all_to_all | solution.py:17
  107.4 1.6 %broadcast_in_dim.19 = bf16[4,8,3,80,128]{4,3,1,2,0:T(8,128)(2,1)} broadcast(bf16[8,3,80,128]{3,2,0,1:T(8,128)(2,1)S(1)} %copy.62), dimensions={1,2,3,4} | broadcast | bytes 2457600 | tf_op jit(solution)/shard_map/state_gather/broadcast_in_dim | solution.py:16
  109.0 4.4 %all-to-all-start.1 = ((bf16[4,8,3,80,128]{4,3,1,2,0:T(8,128)(2,1)}), bf16[4,8,3,80,128]{4,3,1,2,0:T(8,128)(2,1)}, u32[]{:S(2)}, u32[]{:S(2)}) async-start(bf16[4,8,3,80,128]{4,3,1,2,0:T(8,128)(2,1)} %broadcast_in_dim.19), calls=%async_computation.1 | async-start | bytes 3932160 | tf_op jit(solution)/shard_map/state_gather/all_to_all | solution.py:17
  113.4 23.2 %all-to-all-done.1 = bf16[4,8,3,80,128]{4,3,1,2,0:T(8,128)(2,1)} async-done(((bf16[4,8,3,80,128]{4,3,1,2,0:T(8,128)(2,1)}), bf16[4,8,3,80,128]{4,3,1,2,0:T(8,128)(2,1)}, u32[]{:S(2)}, u32[]{:S(2)}) %all-to-all-start.1) | async-done | bytes 1966112 | tf_op jit(solution)/shard_map/state_gather/all_to_all | solution.py:17
  136.6 1.8 %copy.86 = bf16[4,8,3,80,128]{4,3,0,1,2:T(8,128)(2,1)S(1)} copy(bf16[4,8,3,80,128]{4,3,1,2,0:T(8,128)(2,1)} %all-to-all-done.1) | data formatting | bytes 3932160 | tf_op jit(solution)/shard_map/state_gather/all_to_all | solution.py:17
  138.4 0.2 slice.19
  138.6 0.3 fusion.20
  138.9 0.2 fusion.21
  139.2 0.8 multiply_subtract_fusion
  140.0 2.0 %bitcast_convert_fusion = f32[3,2048,128]{2,1,0:T(8,128)} fusion(bf16[3,8,4,64,128]{4,3,2,1,0:T(8,128)(2,1)S(1)} %slice.19), kind=kLoop, calls=%fused_computation.7 | loop fusion | flops 786432 | bytes 4718592 | tf_op jit(solution)/shard_map/state_gather/convert_element_type | solution.py:36
  142.0 3.6 %copy.73 = f32[3,2048,128]{1,2,0:T(8,128)} copy(f32[3,2048,128]{2,1,0:T(8,128)} %bitcast_convert_fusion) | data formatting | bytes 6291456 | tf_op jit(solution)/shard_map/state_gather/convert_element_type | solution.py:36
  145.5 3.7 %fusion.2 = bf16[3,2048,128]{1,2,0:T(8,128)(2,1)} fusion(f32[3,2048,128]{1,2,0:T(8,128)} %copy.73, bf16[3,256,128]{2,1,0:T(8,128)(2,1)S(1)} %bitcast.69, bf16[2048,256,1]{1,0,2:T(8,128)(2,1)S(1)} %bitcast.64), kind=kOutput, calls=%fused_computation.3 | convolution fusion | flops 405012480 | bytes 5963776 | tf_op jit(solution)/shard_map/update/dr,mrc->mdc/dot_general | solution.py:73
  149.2 2.6 %copy.74 = bf16[3,2048,128]{2,1,0:T(8,128)(2,1)} copy(bf16[3,2048,128]{1,2,0:T(8,128)(2,1)} %fusion.2) | data formatting | bytes 3145728
  (22 shorter events, 0.3 us)
Async XLA Ops:
  0.6 25.3 %copy-start = (bf16[3,2048,128]{2,1,0:T(8,128)(2,1)S(1)}, bf16[3,2048,128]{2,1,0:T(8,128)(2,1)}, u32[]{:S(2)}) copy-start(bf16[3,2048,128]{2,1,0:T(8,128)(2,1)} %param.7) | copy-start | bytes 4718596
  21.4 17.0 %all-to-all-start.3 = ((bf16[4,8,64,256]{3,2,1,0:T(8,128)(2,1)}), bf16[4,8,64,256]{3,2,1,0:T(8,128)(2,1)S(1)}, u32[]{:S(2)}, u32[]{:S(2)}) async-start(bf16[4,8,64,256]{3,2,1,0:T(8,128)(2,1)} %broadcast_in_dim.21), calls=%async_computation.3 | async-start | bytes 2097152 | tf_op jit(solution)/shard_map/factor_gather/all_to_all | solution.py:17
  38.5 1.0 copy-start.2
  39.4 4.0 %copy-start.1 = (f32[2048,3,128]{2,0,1:T(8,128)S(1)}, f32[2048,3,128]{2,0,1:T(8,128)}, u32[]{:S(2)}) copy-start(f32[2048,3,128]{2,0,1:T(8,128)} %fusion) | copy-start | bytes 9437188
  43.4 37.7 %copy-start.3 = (f32[3,64,128]{2,1,0:T(8,128)S(1)}, f32[3,64,128]{2,1,0:T(8,128)}, u32[]{:S(2)}) copy-start(f32[3,64,128]{2,1,0:T(8,128)} %param.9) | copy-start | bytes 294916
  43.4 44.2 %copy-start.5 = (f32[3,8,128]{2,1,0:T(8,128)S(1)}, f32[3,8,128]{2,1,0:T(8,128)}, u32[]{:S(2)}) copy-start(f32[3,8,128]{2,1,0:T(8,128)} %param.11) | copy-start | bytes 36868
  43.5 44.2 %copy-start.6 = (f32[3,8,128]{2,1,0:T(8,128)S(1)}, f32[3,8,128]{2,1,0:T(8,128)}, u32[]{:S(2)}) copy-start(f32[3,8,128]{2,1,0:T(8,128)} %param.10) | copy-start | bytes 36868
  76.9 9.5 %all-to-all-start.6 = ((f32[8,1,128]{2,1,0:T(1,128)}), f32[8,1,128]{2,1,0:T(1,128)S(1)}, u32[]{:S(2)}, u32[]{:S(2)}) async-start(f32[8,1,128]{2,1,0:T(1,128)} %broadcast_in_dim.23), calls=%async_computation.6 | async-start | bytes 8192 | tf_op jit(solution)/shard_map/square_sum/all_to_all | solution.py:17
  109.0 27.6 %all-to-all-start.1 = ((bf16[4,8,3,80,128]{4,3,1,2,0:T(8,128)(2,1)}), bf16[4,8,3,80,128]{4,3,1,2,0:T(8,128)(2,1)}, u32[]{:S(2)}, u32[]{:S(2)}) async-start(bf16[4,8,3,80,128]{4,3,1,2,0:T(8,128)(2,1)} %broadcast_in_dim.19), calls=%async_computation.1 | async-start | bytes 3932160 | tf_op jit(solution)/shard_map/state_gather/all_to_all | solution.py:17
  138.4 0.8 copy-start.4

commit v2 on v0

v2 whole, which is shorter than its diff:
```python
import jax
import jax.numpy as jnp
from jax import lax
from jax.experimental import pallas as pl
from jax.experimental.pallas import tpu as pltpu
from jax.sharding import Mesh
from jax.sharding import PartitionSpec as P

MW = 1024
RANK = 256
Z, Y = ("fs_0", "fs_1")
FS = ("fs_0", "fs_1")
TP = ("tp_0", "tp_1")
CORE = "tp_1"
BF = jnp.bfloat16
F32 = jnp.float32
VMEM = pl.BlockSpec(memory_space=pltpu.VMEM)


def sent_to_all(array, axis):
    copies = jnp.broadcast_to(array, (lax.axis_size(axis), *array.shape))
    return lax.all_to_all(copies, axis, split_axis=0, concat_axis=0, tiled=True)


def moved(array, axis, shift):
    size = lax.axis_size(axis)
    return lax.ppermute(array, axis, [(i, (i + shift) % size) for i in range(size)])


def gathered_z(array):
    right, left = [array], [array]
    for _ in range(3):
        right.append(moved(right[-1], Z, 1))
        left.append(moved(left[-1], Z, -1))
    right.append(moved(right[-1], Z, 1))
    return jnp.stack(right + left[:0:-1])


def gathered_y(array):
    right = moved(array, Y, 1)
    left = moved(array, Y, -1)
    return (
        array, right, left,
        moved(right[:4], Y, 1), moved(left[4:], Y, -1),
    )


def partial_kernel(core, gradient_a, gradient_b, mine, other, out, factor):
    for z in range(8):
        for y in range(4):
            row = z * 256 + y * 64
            factor[pl.ds(row + pl.multiple_of(core[0] * 32, 32), 32)] = mine[y, z]
            factor[pl.ds(row + pl.multiple_of(32 - core[0] * 32, 32), 32)] = other[y, z]
    projected = jnp.dot(gradient_a[...], factor[:1024], preferred_element_type=F32)
    projected += jnp.dot(gradient_b[...], factor[1024:], preferred_element_type=F32)
    rows = [projected[m * 128 : (m + 1) * 128].T.reshape(32, 8, 128) for m in range(3)]
    out[...] = jnp.concatenate(rows, axis=1).astype(BF)


def square_kernel(projected, out):
    values = projected[...].astype(F32).reshape(96, 8, 128)
    out[...] = jnp.broadcast_to(jnp.sum(values * values, axis=0), out.shape)


def moments(clip, projected, first, second):
    clipped = clip * projected
    new_first = 0.9 * first + 0.1 * clipped
    new_second = 0.95 * second + 0.05 * clipped * clipped
    return new_first, new_second, new_first / (jnp.sqrt(new_second) + 1e-08)


def final_kernel(
    place, squares, projected, own, state, right, left, across_a, across_b,
    first, second, weights, factor, own_factor,
    update, new_weights, copies, new_first, new_second, normed, change,
):
    total = jnp.sum(jnp.sum(squares[...], axis=0), keepdims=True)
    root_mean = jnp.sqrt(total / (3 * RANK * MW) + 1e-06)
    clip = jnp.minimum(1.0, 0.25 / root_mean)
    blocks = []
    for j in range(8):
        across = across_a.at[j] if j < 4 else across_b.at[j - 4]
        for i, block in enumerate((state.at[j], right.at[j], across, left.at[j])):
            at = ((place[0] + 8 - j) % 8) * 4 + (place[1] + 4 - i) % 4
            blocks.append((at, block))
    for at, block in blocks:
        _, _, values = moments(
            clip,
            projected[at].astype(F32),
            block[192:216].astype(F32),
            block[216:240].astype(F32),
        )
        for m in range(3):
            normed[pl.ds(pl.multiple_of(at * 8, 8), 8), m * 128 : (m + 1) * 128] = values[
                m * 8 : (m + 1) * 8
            ]
    values = normed[...].astype(BF)
    own_change = jnp.dot(own_factor[...], values, preferred_element_type=F32)
    for m in range(3):
        part = own_change[:, m * 128 : (m + 1) * 128]
        update[m] = part
        new_weights[m] = weights[m] - 0.02 * part
        own_first, own_second, _ = moments(
            clip, own[m * 8 : (m + 1) * 8], first[m], second[m]
        )
        new_first[m] = own_first
        new_second[m] = own_second
    change[...] = jnp.dot(factor[...], values, preferred_element_type=F32)
    for at, block in blocks:
        rows = pl.ds(pl.multiple_of(at * 64, 64), 64)
        for m in range(3):
            before = block[m * 64 : (m + 1) * 64].astype(F32)
            part = change[rows, m * 128 : (m + 1) * 128]
            copies[m, rows] = (before - 0.02 * part).astype(BF)


def step(inputs, cotangents, factor, weights, first_moment, second_moment):
    core = lax.axis_index(CORE)
    place = jnp.stack([lax.axis_index(Z), lax.axis_index(Y)]).astype(jnp.int32)
    half = lax.dynamic_slice_in_dim(factor, core * 32, 32, 0)
    half = sent_to_all(half, Z)
    half = sent_to_all(half, Y)
    other_half = moved(half, CORE, 1)
    state = jnp.concatenate(
        [array.reshape(-1, 128) for array in (weights, first_moment, second_moment)]
    ).astype(BF)
    state_z = gathered_z(state)
    states = gathered_y(state_z)

    def gradient_of(part):
        return (
            jnp.einsum("mtc,td->mcd", cotangents, part, preferred_element_type=F32)
            .astype(BF)
            .reshape(384, -1)
        )

    gradient_a = gradient_of(inputs[:, :1024])
    gradient_b = gradient_of(inputs[:, 1024:])
    smem = pl.BlockSpec(memory_space=pltpu.SMEM)
    partial_value, factor_all = pl.pallas_call(
        partial_kernel,
        out_shape=(
            jax.ShapeDtypeStruct((32, 24, 128), BF),
            jax.ShapeDtypeStruct((2048, RANK), BF),
        ),
        in_specs=[smem] + [VMEM] * 4,
        out_specs=(VMEM, VMEM),
        compiler_params=pltpu.CompilerParams(vmem_limit_bytes=12 << 20),
    )(core.reshape(1).astype(jnp.int32), gradient_a, gradient_b, half, other_half)
    arrived = lax.all_to_all(partial_value, FS, split_axis=0, concat_axis=0, tiled=True)
    projected = arrived.astype(F32).sum(axis=0)
    projected_all = sent_to_all(projected.astype(BF), FS)
    squares = pl.pallas_call(
        square_kernel,
        out_shape=jax.ShapeDtypeStruct((8, 8, 128), F32),
        in_specs=[VMEM],
        out_specs=VMEM,
        compiler_params=pltpu.CompilerParams(vmem_limit_bytes=4 << 20),
    )(projected_all)
    squares = lax.all_to_all(squares, TP, split_axis=0, concat_axis=0, tiled=True)
    return pl.pallas_call(
        final_kernel,
        out_shape=(
            jax.ShapeDtypeStruct((3, 64, 128), F32),
            jax.ShapeDtypeStruct((3, 64, 128), F32),
            jax.ShapeDtypeStruct((3, 2048, 128), BF),
            jax.ShapeDtypeStruct((3, 8, 128), F32),
            jax.ShapeDtypeStruct((3, 8, 128), F32),
        ),
        in_specs=[smem] + [VMEM] * 13,
        out_specs=(VMEM,) * 5,
        scratch_shapes=[pltpu.VMEM((RANK, 384), F32), pltpu.VMEM((2048, 384), F32)],
        compiler_params=pltpu.CompilerParams(vmem_limit_bytes=24 << 20),
    )(
        place, squares, projected_all, projected, *states, first_moment, second_moment,
        weights, factor_all, factor,
    )


def solution(mesh):
    torus = Mesh(mesh.devices.reshape(8, 4, 4, 2), ("fs_0", "fs_1", "tp_0", "tp_1"))
    return jax.shard_map(
        step,
        mesh=torus,
        in_specs=(
            P(FS, None),
            P(None, FS, TP),
            P(FS, None),
            P(None, FS, TP),
            P(None, FS, TP),
            P(None, FS, TP),
        ),
        out_specs=(
            P(None, FS, TP),
            P(None, FS, TP),
            P(None, None, TP),
            P(None, FS, TP),
            P(None, FS, TP),
        ),
        check_vma=False,
    )
```

time: 169 us -> 104 us (0.62)
  the two profiles are of different devices: /device:TPU:32 before, /device:TPU:1 now
where the time goes in v2:
time: 104 us; the launch traced here: 103 us
  starting transfers between devices  56.1 us (54%)
  waiting for transfers between devices  18.9 us (18%)
  local copies, waits for them, and re-layouts  13.1 us (13%)
  matrix products  6.86 us (7%)
  Pallas kernels  5.17 us (5%)
  other arithmetic  1.88 us (2%)
    ppermute x12, starting transfers between devices, moved(): lax.ppermute(array, axis, [(i, (i + shift) % size) for i in range(size)])  21 us
    all_to_all x3, starting transfers between devices, sent_to_all(): return lax.all_to_all(copies, axis, split_axis=0, concat_axis=0, tiled=True)  13.2 us
    all_to_all x1, starting transfers between devices, step(): lax.all_to_all(squares, TP, split_axis=0, concat_axis=0, tiled=True)  11.2 us
    all_to_all x1, starting transfers between devices, step(): lax.all_to_all(partial_value, FS, split_axis=0, concat_axis=0, tiled=True)  10.7 us
    unnamed x26, local copies, waits for them, and re-layouts  8.75 us
    all_to_all x1, waiting for transfers between devices, step(): lax.all_to_all(partial_value, FS, split_axis=0, concat_axis=0, tiled=True)  7.1 us
    dot_general x2, matrix products, gradient_of(): jnp.einsum('mtc,td->mcd', cotangents, part, preferred_element_type=F32)  6.86 us
    all_to_all x3, waiting for transfers between devices, sent_to_all(): return lax.all_to_all(copies, axis, split_axis=0, concat_axis=0, tiled=True)  6.04 us
  transfers between devices with their start and end apart: 17, of which 7 were waited for; matrix products, arithmetic and copies ran while one was open for 15% of the time, Pallas kernels for 1%

profile of v2, /device:TPU:1, one launch (start us, length us, event | category | flops | bytes accessed | tf_op | source)
XLA Modules:
  0.0 102.9 jit_solution(10816672908325672425)
XLA Ops:
  0.6 1.0 convert.18
  1.7 0.7 convert_bitcast_fusion
  2.4 2.5 %collective-permute-start.1 = (bf16[240,128]{1,0:T(8,128)(2,1)S(1)}, bf16[240,128]{1,0:T(8,128)(2,1)}, u32[]{:S(2)}, u32[]{:S(2)}) collective-permute-start(bf16[240,128]{1,0:T(8,128)(2,1)S(1)} %pad_maximum_fusion), channel_id=1, source_target_pairs={{0,32},{32,64},{64,96},{96,128},{128,160},{160,192},{192,224},{224... | collective-permute-start | bytes 184328 | tf_op jit(solution)/shard_map/ppermute | solution.py:27
  4.9 4.0 %collective-permute-start.5 = (bf16[240,128]{1,0:T(8,128)(2,1)S(1)}, bf16[240,128]{1,0:T(8,128)(2,1)S(1)}, u32[]{:S(2)}, u32[]{:S(2)}) collective-permute-start(bf16[240,128]{1,0:T(8,128)(2,1)S(1)} %pad_maximum_fusion), channel_id=1, source_target_pairs={{0,224},{32,0},{64,32},{96,64},{128,96},{160,128},{192,160},{224,1... | collective-permute-start | bytes 184328 | tf_op jit(solution)/shard_map/ppermute | solution.py:27
  10.3 5.2 %all-to-all-start = ((bf16[8,32,256]{2,1,0:T(8,128)(2,1)}), bf16[8,32,256]{2,1,0:T(8,128)(2,1)S(1)}, u32[]{:S(2)}, u32[]{:S(2)}) async-start(bf16[8,32,256]{2,1,0:T(8,128)(2,1)} %broadcast_in_dim.9), calls=%async_computation | async-start | bytes 262144 | tf_op jit(solution)/shard_map/all_to_all | solution.py:22
  15.6 4.1 %fusion.6 = bf16[3,128,1024]{2,1,0:T(8,128)(2,1)S(1)} fusion(bf16[3,2048,128]{2,1,0:T(8,128)(2,1)S(1)} %copy-done, bf16[2048,2048]{1,0:T(8,128)(2,1)} %param.6), kind=kOutput, calls=%fused_computation.6 | convolution fusion | flops 1611005952 | bytes 6553600 | tf_op jit(solution)/shard_map/mtc,td->mcd/dot_general | solution.py:132
  20.2 2.7 %fusion.9 = bf16[3,128,1024]{2,1,0:T(8,128)(2,1)} fusion(bf16[3,2048,128]{2,1,0:T(8,128)(2,1)S(1)} %copy-done, bf16[2048,2048]{1,0:T(8,128)(2,1)S(1)} %copy-done.9), kind=kOutput, calls=%fused_computation.7 | convolution fusion | flops 1611005952 | bytes 6553600 | tf_op jit(solution)/shard_map/mtc,td->mcd/dot_general | solution.py:132
  22.9 1.5 %collective-permute-start.2 = (bf16[240,128]{1,0:T(8,128)(2,1)}, bf16[240,128]{1,0:T(8,128)(2,1)}, u32[]{:S(2)}, u32[]{:S(2)}) collective-permute-start(bf16[240,128]{1,0:T(8,128)(2,1)} %collective-permute-done.1), channel_id=1, source_target_pairs={{0,32},{32,64},{64,96},{96,128},{128,160},{160,192},{192,224},{224... | collective-permute-start | bytes 184328 | tf_op jit(solution)/shard_map/ppermute | solution.py:27
  24.5 0.9 broadcast_in_dim.10
  25.3 4.2 %all-to-all-start.1 = ((bf16[4,8,32,256]{3,2,1,0:T(8,128)(2,1)}), bf16[4,8,32,256]{3,2,1,0:T(8,128)(2,1)S(1)}, u32[]{:S(2)}, u32[]{:S(2)}) async-start(bf16[4,8,32,256]{3,2,1,0:T(8,128)(2,1)} %broadcast_in_dim.10), calls=%async_computation.1 | async-start | bytes 1048576 | tf_op jit(solution)/shard_map/all_to_all | solution.py:22
  29.5 0.8 bitcast_dynamic-update-slice_fusion.6
  30.4 1.3 %collective-permute-start.6 = (bf16[240,128]{1,0:T(8,128)(2,1)S(1)}, bf16[240,128]{1,0:T(8,128)(2,1)S(1)}, u32[]{:S(2)}, u32[]{:S(2)}) collective-permute-start(bf16[240,128]{1,0:T(8,128)(2,1)S(1)} %collective-permute-done.5), channel_id=1, source_target_pairs={{0,224},{32,0},{64,32},{96,64},{128,96},{160,128},{192,160},{224,1... | collective-permute-start | bytes 184328 | tf_op jit(solution)/shard_map/ppermute | solution.py:27
  31.9 0.9 bitcast_dynamic-update-slice_fusion.5
  33.5 2.5 %collective-permute-start.7 = (bf16[240,128]{1,0:T(8,128)(2,1)S(1)}, bf16[240,128]{1,0:T(8,128)(2,1)}, u32[]{:S(2)}, u32[]{:S(2)}) collective-permute-start(bf16[240,128]{1,0:T(8,128)(2,1)S(1)} %collective-permute-done.6), channel_id=1, source_target_pairs={{0,224},{32,0},{64,32},{96,64},{128,96},{160,128},{192,160},{224,1... | collective-permute-start | bytes 184328 | tf_op jit(solution)/shard_map/ppermute | solution.py:27
  36.5 3.5 %collective-permute-start = (bf16[4,8,32,256]{3,2,1,0:T(8,128)(2,1)S(1)}, bf16[4,8,32,256]{3,2,1,0:T(8,128)(2,1)S(1)}, u32[]{:S(2)}, u32[]{:S(2)}) collective-permute-start(bf16[4,8,32,256]{3,2,1,0:T(8,128)(2,1)S(1)} %all-to-all-done.1.mine), channel_id=1, source_target_pairs={{0,1},{1,0},{2,3},{3,2},{4,5},{5,4},{6,7},{7,6},{8,9},{9,8},{10,11... | collective-permute-start | bytes 1572872 | tf_op jit(solution)/shard_map/ppermute | solution.py:27
  40.0 0.8 bitcast_dynamic-update-slice_fusion.4
  40.9 0.8 bitcast_dynamic-update-slice_fusion.3
  41.7 0.8 bitcast_dynamic-update-slice_fusion.2
  42.6 1.1 %copy-done.3 = bf16[3,128,1024]{2,1,0:T(8,128)(2,1)S(1)} copy-done((bf16[3,128,1024]{2,1,0:T(8,128)(2,1)S(1)}, bf16[3,128,1024]{2,1,0:T(8,128)(2,1)}, u32[]{:S(2)}) %copy-start.3) | copy-done | bytes 786456
  44.5 1.0 copy-done.1
  46.1 10.7 %all-to-all-start.2 = ((bf16[32,24,128]{2,1,0:T(8,128)(2,1)}), bf16[32,24,128]{2,1,0:T(8,128)(2,1)S(1)}, u32[]{:S(2)}, u32[]{:S(2)}) async-start(bf16[32,24,128]{2,1,0:T(8,128)(2,1)} %copy-done.5), calls=%async_computation.2 | async-start | bytes 393216 | tf_op jit(solution)/shard_map/all_to_all | solution.py:150
  56.9 1.3 %collective-permute-start.8 = (bf16[8,240,128]{2,1,0:T(8,128)(2,1)S(1)}, bf16[8,240,128]{2,1,0:T(8,128)(2,1)S(1)}, u32[]{:S(2)}, u32[]{:S(2)}) collective-permute-start(bf16[8,240,128]{2,1,0:T(8,128)(2,1)S(1)} %bitcast_dynamic-update-slice_fusion.state), channel_id=1, source_target_pairs={{0,8},{8,16},{16,24},{24,0},{1,9},{9,17},{17,25},{25,1},{2,10},{10... | collective-permute-start | bytes 1474568 | tf_op jit(solution)/shard_map/ppermute | solution.py:27
  58.2 1.4 %collective-permute-start.9 = (bf16[8,240,128]{2,1,0:T(8,128)(2,1)S(1)}, bf16[8,240,128]{2,1,0:T(8,128)(2,1)S(1)}, u32[]{:S(2)}, u32[]{:S(2)}) collective-permute-start(bf16[8,240,128]{2,1,0:T(8,128)(2,1)S(1)} %bitcast_dynamic-update-slice_fusion.state), channel_id=1, source_target_pairs={{0,24},{8,0},{16,8},{24,16},{1,25},{9,1},{17,9},{25,17},{2,26},{10... | collective-permute-start | bytes 1474568 | tf_op jit(solution)/shard_map/ppermute | solution.py:27
  59.7 7.1 %all-to-all-done.2 = bf16[32,24,128]{2,1,0:T(8,128)(2,1)S(1)} async-done(((bf16[32,24,128]{2,1,0:T(8,128)(2,1)}), bf16[32,24,128]{2,1,0:T(8,128)(2,1)S(1)}, u32[]{:S(2)}, u32[]{:S(2)}) %all-to-all-start.2) | async-done | bytes 196640 | tf_op jit(solution)/shard_map/all_to_all | solution.py:150
  67.5 3.9 %all-to-all-start.3 = ((bf16[32,24,128]{2,1,0:T(8,128)(2,1)}), bf16[32,24,128]{2,1,0:T(8,128)(2,1)S(1)}, u32[]{:S(2)}, u32[]{:S(2)}) async-start(bf16[32,24,128]{2,1,0:T(8,128)(2,1)} %broadcast_in_dim.11), calls=%async_computation.3 | async-start | bytes 393216 | tf_op jit(solution)/shard_map/all_to_all | solution.py:22
  72.1 1.1 %collective-permute-start.10 = (bf16[4,240,128]{2,1,0:T(8,128)(2,1)}, bf16[4,240,128]{2,1,0:T(8,128)(2,1)}, u32[]{:S(2)}, u32[]{:S(2)}) collective-permute-start(bf16[4,240,128]{2,1,0:T(8,128)(2,1)} %slice.16), channel_id=1, source_target_pairs={{0,8},{8,16},{16,24},{24,0},{1,9},{9,17},{17,25},{25,1},{2,10},{10... | collective-permute-start | bytes 737288 | tf_op jit(solution)/shard_map/ppermute | solution.py:27
  73.9 1.6 %collective-permute-start.11 = (bf16[4,240,128]{2,1,0:T(8,128)(2,1)}, bf16[4,240,128]{2,1,0:T(8,128)(2,1)}, u32[]{:S(2)}, u32[]{:S(2)}) collective-permute-start(bf16[4,240,128]{2,1,0:T(8,128)(2,1)} %slice.17), channel_id=1, source_target_pairs={{0,24},{8,0},{16,8},{24,16},{1,25},{9,1},{17,9},{25,17},{2,26},{10... | collective-permute-start | bytes 737288 | tf_op jit(solution)/shard_map/ppermute | solution.py:27
  75.5 5.9 %all-to-all-done.3.projected = bf16[32,24,128]{2,1,0:T(8,128)(2,1)S(1)} async-done(((bf16[32,24,128]{2,1,0:T(8,128)(2,1)}), bf16[32,24,128]{2,1,0:T(8,128)(2,1)S(1)}, u32[]{:S(2)}, u32[]{:S(2)}) %all-to-all-start.3) | async-done | bytes 196640 | tf_op jit(solution)/shard_map/all_to_all | solution.py:22
  82.1 11.2 %all-to-all-start.4 = ((f32[8,8,128]{2,1,0:T(8,128)}), f32[8,8,128]{2,1,0:T(8,128)S(1)}, u32[]{:S(2)}, u32[]{:S(2)}) async-start(f32[8,8,128]{2,1,0:T(8,128)} %shard_map.102), calls=%async_computation.4 | async-start | bytes 65536 | tf_op jit(solution)/shard_map/all_to_all | solution.py:160
  93.3 4.6 %all-to-all-done.4.squares = f32[8,8,128]{2,1,0:T(8,128)S(1)} async-done(((f32[8,8,128]{2,1,0:T(8,128)}), f32[8,8,128]{2,1,0:T(8,128)S(1)}, u32[]{:S(2)}, u32[]{:S(2)}) %all-to-all-start.4) | async-done | bytes 32800 | tf_op jit(solution)/shard_map/all_to_all | solution.py:160
  98.0 1.2 %copy-done.2 = bf16[2048,256]{1,0:T(8,128)(2,1)S(1)} copy-done((bf16[2048,256]{1,0:T(8,128)(2,1)S(1)}, bf16[2048,256]{1,0:T(8,128)(2,1)}, u32[]{:S(2)}) %copy-start.2) | copy-done | bytes 1048600
  99.2 3.7 %shard_map.103 = (f32[3,64,128]{2,1,0:T(8,128)}, f32[3,64,128]{2,1,0:T(8,128)}, bf16[3,2048,128]{2,1,0:T(8,128)(2,1)}, f32[3,8,128]{2,1,0:T(8,128)}, f32[3,8,128]{2,1,0:T(8,128)}) custom-call(s32[2]{0:T(128)S(1)} %pad_add_fusion.place, f32[8,8,128]{2,1,0:T(8,128)S(1)} %all-to-all-done.4.squares, bf16[32,24,128]{2,1,0:T(8,128)(2,1)S(1)} %all-to-all-done.3.projected, ...), custom_call_target="tpu_custom_call" | custom-call | tf_op jit(solution)/shard_map/pallas_call | solution.py:161
  (47 shorter events, 7.9 us)
Async XLA Ops:
  0.6 14.9 %copy-start = (bf16[3,2048,128]{2,1,0:T(8,128)(2,1)S(1)}, bf16[3,2048,128]{2,1,0:T(8,128)(2,1)}, u32[]{:S(2)}) copy-start(bf16[3,2048,128]{2,1,0:T(8,128)(2,1)} %param.7) | copy-start | bytes 4718596
  2.4 20.5 %collective-permute-start.1 = (bf16[240,128]{1,0:T(8,128)(2,1)S(1)}, bf16[240,128]{1,0:T(8,128)(2,1)}, u32[]{:S(2)}, u32[]{:S(2)}) collective-permute-start(bf16[240,128]{1,0:T(8,128)(2,1)S(1)} %pad_maximum_fusion), channel_id=1, source_target_pairs={{0,32},{32,64},{64,96},{96,128},{128,160},{160,192},{192,224},{224... | collective-permute-start | bytes 184328 | tf_op jit(solution)/shard_map/ppermute | solution.py:27
  4.9 25.4 %collective-permute-start.5 = (bf16[240,128]{1,0:T(8,128)(2,1)S(1)}, bf16[240,128]{1,0:T(8,128)(2,1)S(1)}, u32[]{:S(2)}, u32[]{:S(2)}) collective-permute-start(bf16[240,128]{1,0:T(8,128)(2,1)S(1)} %pad_maximum_fusion), channel_id=1, source_target_pairs={{0,224},{32,0},{64,32},{96,64},{128,96},{160,128},{192,160},{224,1... | collective-permute-start | bytes 184328 | tf_op jit(solution)/shard_map/ppermute | solution.py:27
  10.3 14.1 %all-to-all-start = ((bf16[8,32,256]{2,1,0:T(8,128)(2,1)}), bf16[8,32,256]{2,1,0:T(8,128)(2,1)S(1)}, u32[]{:S(2)}, u32[]{:S(2)}) async-start(bf16[8,32,256]{2,1,0:T(8,128)(2,1)} %broadcast_in_dim.9), calls=%async_computation | async-start | bytes 262144 | tf_op jit(solution)/shard_map/all_to_all | solution.py:22
  15.6 4.6 %copy-start.9 = (bf16[2048,2048]{1,0:T(8,128)(2,1)S(1)}, bf16[2048,2048]{1,0:T(8,128)(2,1)}, u32[]{:S(2)}) copy-start(bf16[2048,2048]{1,0:T(8,128)(2,1)} %param.6) | copy-start | bytes 25165828
  22.9 8.8 %collective-permute-start.2 = (bf16[240,128]{1,0:T(8,128)(2,1)}, bf16[240,128]{1,0:T(8,128)(2,1)}, u32[]{:S(2)}, u32[]{:S(2)}) collective-permute-start(bf16[240,128]{1,0:T(8,128)(2,1)} %collective-permute-done.1), channel_id=1, source_target_pairs={{0,32},{32,64},{64,96},{96,128},{128,160},{160,192},{192,224},{224... | collective-permute-start | bytes 184328 | tf_op jit(solution)/shard_map/ppermute | solution.py:27
  25.3 11.1 %all-to-all-start.1 = ((bf16[4,8,32,256]{3,2,1,0:T(8,128)(2,1)}), bf16[4,8,32,256]{3,2,1,0:T(8,128)(2,1)S(1)}, u32[]{:S(2)}, u32[]{:S(2)}) async-start(bf16[4,8,32,256]{3,2,1,0:T(8,128)(2,1)} %broadcast_in_dim.10), calls=%async_computation.1 | async-start | bytes 1048576 | tf_op jit(solution)/shard_map/all_to_all | solution.py:22
  30.4 3.1 %collective-permute-start.6 = (bf16[240,128]{1,0:T(8,128)(2,1)S(1)}, bf16[240,128]{1,0:T(8,128)(2,1)S(1)}, u32[]{:S(2)}, u32[]{:S(2)}) collective-permute-start(bf16[240,128]{1,0:T(8,128)(2,1)S(1)} %collective-permute-done.5), channel_id=1, source_target_pairs={{0,224},{32,0},{64,32},{96,64},{128,96},{160,128},{192,160},{224,1... | collective-permute-start | bytes 184328 | tf_op jit(solution)/shard_map/ppermute | solution.py:27
  31.7 4.6 %collective-permute-start.3 = (bf16[240,128]{1,0:T(8,128)(2,1)}, bf16[240,128]{1,0:T(8,128)(2,1)}, u32[]{:S(2)}, u32[]{:S(2)}) collective-permute-start(bf16[240,128]{1,0:T(8,128)(2,1)} %collective-permute-done.2), channel_id=1, source_target_pairs={{0,32},{32,64},{64,96},{96,128},{128,160},{160,192},{192,224},{224... | collective-permute-start | bytes 184328 | tf_op jit(solution)/shard_map/ppermute | solution.py:27
  33.5 8.2 %collective-permute-start.7 = (bf16[240,128]{1,0:T(8,128)(2,1)S(1)}, bf16[240,128]{1,0:T(8,128)(2,1)}, u32[]{:S(2)}, u32[]{:S(2)}) collective-permute-start(bf16[240,128]{1,0:T(8,128)(2,1)S(1)} %collective-permute-done.6), channel_id=1, source_target_pairs={{0,224},{32,0},{64,32},{96,64},{128,96},{160,128},{192,160},{224,1... | collective-permute-start | bytes 184328 | tf_op jit(solution)/shard_map/ppermute | solution.py:27
  36.3 4.6 %collective-permute-start.4 = (bf16[240,128]{1,0:T(8,128)(2,1)}, bf16[240,128]{1,0:T(8,128)(2,1)}, u32[]{:S(2)}, u32[]{:S(2)}) collective-permute-start(bf16[240,128]{1,0:T(8,128)(2,1)} %collective-permute-done.3), channel_id=1, source_target_pairs={{0,32},{32,64},{64,96},{96,128},{128,160},{160,192},{192,224},{224... | collective-permute-start | bytes 184328 | tf_op jit(solution)/shard_map/ppermute | solution.py:27
  36.5 6.1 %collective-permute-start = (bf16[4,8,32,256]{3,2,1,0:T(8,128)(2,1)S(1)}, bf16[4,8,32,256]{3,2,1,0:T(8,128)(2,1)S(1)}, u32[]{:S(2)}, u32[]{:S(2)}) collective-permute-start(bf16[4,8,32,256]{3,2,1,0:T(8,128)(2,1)S(1)} %all-to-all-done.1.mine), channel_id=1, source_target_pairs={{0,1},{1,0},{2,3},{3,2},{4,5},{5,4},{6,7},{7,6},{8,9},{9,8},{10,11... | collective-permute-start | bytes 1572872 | tf_op jit(solution)/shard_map/ppermute | solution.py:27
  42.6 1.1 %copy-start.3 = (bf16[3,128,1024]{2,1,0:T(8,128)(2,1)S(1)}, bf16[3,128,1024]{2,1,0:T(8,128)(2,1)}, u32[]{:S(2)}) copy-start(bf16[3,128,1024]{2,1,0:T(8,128)(2,1)} %fusion.9) | copy-start | bytes 2359300
  44.5 1.0 copy-start.1
  45.4 0.7 copy-start.5
  46.1 51.9 %copy-start.4 = (f32[3,64,128]{2,1,0:T(8,128)S(1)}, f32[3,64,128]{2,1,0:T(8,128)}, u32[]{:S(2)}) copy-start(f32[3,64,128]{2,1,0:T(8,128)} %weights.1) | copy-start | bytes 294916
  46.1 51.9 %copy-start.6 = (bf16[64,256]{1,0:T(8,128)(2,1)S(1)}, bf16[64,256]{1,0:T(8,128)(2,1)}, u32[]{:S(2)}) copy-start(bf16[64,256]{1,0:T(8,128)(2,1)} %own_factor.1) | copy-start | bytes 98308
  46.1 51.9 %copy-start.7 = (f32[3,8,128]{2,1,0:T(8,128)S(1)}, f32[3,8,128]{2,1,0:T(8,128)}, u32[]{:S(2)}) copy-start(f32[3,8,128]{2,1,0:T(8,128)} %second.1) | copy-start | bytes 36868
  46.1 51.9 %copy-start.8 = (f32[3,8,128]{2,1,0:T(8,128)S(1)}, f32[3,8,128]{2,1,0:T(8,128)}, u32[]{:S(2)}) copy-start(f32[3,8,128]{2,1,0:T(8,128)} %first.1) | copy-start | bytes 36868
  46.1 20.6 %all-to-all-start.2 = ((bf16[32,24,128]{2,1,0:T(8,128)(2,1)}), bf16[32,24,128]{2,1,0:T(8,128)(2,1)S(1)}, u32[]{:S(2)}, u32[]{:S(2)}) async-start(bf16[32,24,128]{2,1,0:T(8,128)(2,1)} %copy-done.5), calls=%async_computation.2 | async-start | bytes 393216 | tf_op jit(solution)/shard_map/all_to_all | solution.py:150
  56.9 14.5 %collective-permute-start.8 = (bf16[8,240,128]{2,1,0:T(8,128)(2,1)S(1)}, bf16[8,240,128]{2,1,0:T(8,128)(2,1)S(1)}, u32[]{:S(2)}, u32[]{:S(2)}) collective-permute-start(bf16[8,240,128]{2,1,0:T(8,128)(2,1)S(1)} %bitcast_dynamic-update-slice_fusion.state), channel_id=1, source_target_pairs={{0,8},{8,16},{16,24},{24,0},{1,9},{9,17},{17,25},{25,1},{2,10},{10... | collective-permute-start | bytes 1474568 | tf_op jit(solution)/shard_map/ppermute | solution.py:27
  58.2 15.0 %collective-permute-start.9 = (bf16[8,240,128]{2,1,0:T(8,128)(2,1)S(1)}, bf16[8,240,128]{2,1,0:T(8,128)(2,1)S(1)}, u32[]{:S(2)}, u32[]{:S(2)}) collective-permute-start(bf16[8,240,128]{2,1,0:T(8,128)(2,1)S(1)} %bitcast_dynamic-update-slice_fusion.state), channel_id=1, source_target_pairs={{0,24},{8,0},{16,8},{24,16},{1,25},{9,1},{17,9},{25,17},{2,26},{10... | collective-permute-start | bytes 1474568 | tf_op jit(solution)/shard_map/ppermute | solution.py:27
  67.5 13.8 %all-to-all-start.3 = ((bf16[32,24,128]{2,1,0:T(8,128)(2,1)}), bf16[32,24,128]{2,1,0:T(8,128)(2,1)S(1)}, u32[]{:S(2)}, u32[]{:S(2)}) async-start(bf16[32,24,128]{2,1,0:T(8,128)(2,1)} %broadcast_in_dim.11), calls=%async_computation.3 | async-start | bytes 393216 | tf_op jit(solution)/shard_map/all_to_all | solution.py:22
  72.1 21.2 %collective-permute-start.10 = (bf16[4,240,128]{2,1,0:T(8,128)(2,1)}, bf16[4,240,128]{2,1,0:T(8,128)(2,1)}, u32[]{:S(2)}, u32[]{:S(2)}) collective-permute-start(bf16[4,240,128]{2,1,0:T(8,128)(2,1)} %slice.16), channel_id=1, source_target_pairs={{0,8},{8,16},{16,24},{24,0},{1,9},{9,17},{17,25},{25,1},{2,10},{10... | collective-permute-start | bytes 737288 | tf_op jit(solution)/shard_map/ppermute | solution.py:27
  73.9 19.4 %collective-permute-start.11 = (bf16[4,240,128]{2,1,0:T(8,128)(2,1)}, bf16[4,240,128]{2,1,0:T(8,128)(2,1)}, u32[]{:S(2)}, u32[]{:S(2)}) collective-permute-start(bf16[4,240,128]{2,1,0:T(8,128)(2,1)} %slice.17), channel_id=1, source_target_pairs={{0,24},{8,0},{16,8},{24,16},{1,25},{9,1},{17,9},{25,17},{2,26},{10... | collective-permute-start | bytes 737288 | tf_op jit(solution)/shard_map/ppermute | solution.py:27
  82.1 15.9 %all-to-all-start.4 = ((f32[8,8,128]{2,1,0:T(8,128)}), f32[8,8,128]{2,1,0:T(8,128)S(1)}, u32[]{:S(2)}, u32[]{:S(2)}) async-start(f32[8,8,128]{2,1,0:T(8,128)} %shard_map.102), calls=%async_computation.4 | async-start | bytes 65536 | tf_op jit(solution)/shard_map/all_to_all | solution.py:160
  98.0 1.2 %copy-start.2 = (bf16[2048,256]{1,0:T(8,128)(2,1)S(1)}, bf16[2048,256]{1,0:T(8,128)(2,1)}, u32[]{:S(2)}) copy-start(bf16[2048,256]{1,0:T(8,128)(2,1)} %copy-done.1) | copy-start | bytes 3145732

commit v3 on v2

--- a/solution.py
+++ b/solution.py
@@ -27,13 +27,16 @@
     return lax.ppermute(array, axis, [(i, (i + shift) % size) for i in range(size)])
 
 
+def swapped(array, axis, bit):
+    size = lax.axis_size(axis)
+    return lax.ppermute(array, axis, [(i, i ^ bit) for i in range(size)])
+
+
 def gathered_z(array):
-    right, left = [array], [array]
-    for _ in range(3):
-        right.append(moved(right[-1], Z, 1))
-        left.append(moved(left[-1], Z, -1))
-    right.append(moved(right[-1], Z, 1))
-    return jnp.stack(right + left[:0:-1])
+    array = array[None]
+    for bit in (4, 2, 1):
+        array = jnp.concatenate([array, swapped(array, Z, bit)])
+    return array
 
 
 def gathered_y(array):
@@ -45,14 +48,26 @@
     )
 
 
-def partial_kernel(core, gradient_a, gradient_b, mine, other, out, factor):
+def gradient_kernel(cotangents, inputs, out, turned):
+    @pl.when(pl.program_id(0) == 0)
+    def _():
+        for m in range(3):
+            turned[m * 128 : (m + 1) * 128] = cotangents[m].T
+
+    out[...] = jnp.dot(turned[...], inputs[...], preferred_element_type=F32).astype(BF)
+
+
+def assemble(core, mine, other, factor):
     for z in range(8):
         for y in range(4):
             row = z * 256 + y * 64
             factor[pl.ds(row + pl.multiple_of(core[0] * 32, 32), 32)] = mine[y, z]
             factor[pl.ds(row + pl.multiple_of(32 - core[0] * 32, 32), 32)] = other[y, z]
-    projected = jnp.dot(gradient_a[...], factor[:1024], preferred_element_type=F32)
-    projected += jnp.dot(gradient_b[...], factor[1024:], preferred_element_type=F32)
+
+
+def partial_kernel(core, gradient, mine, other, out, factor):
+    assemble(core, mine, other, factor)
+    projected = jnp.dot(gradient[...], factor[...], preferred_element_type=F32)
     rows = [projected[m * 128 : (m + 1) * 128].T.reshape(32, 8, 128) for m in range(3)]
     out[...] = jnp.concatenate(rows, axis=1).astype(BF)
 
@@ -81,7 +96,8 @@
     for j in range(8):
         across = across_a.at[j] if j < 4 else across_b.at[j - 4]
         for i, block in enumerate((state.at[j], right.at[j], across, left.at[j])):
-            at = ((place[0] + 8 - j) % 8) * 4 + (place[1] + 4 - i) % 4
+            away = j // 4 + (j // 2 % 2) * 2 + (j % 2) * 4
+            at = (place[0] ^ away) * 4 + (place[1] + 4 - i) % 4
             blocks.append((at, block))
     for at, block in blocks:
         _, _, values = moments(
@@ -127,26 +143,35 @@
     state_z = gathered_z(state)
     states = gathered_y(state_z)
 
-    def gradient_of(part):
-        return (
-            jnp.einsum("mtc,td->mcd", cotangents, part, preferred_element_type=F32)
-            .astype(BF)
-            .reshape(384, -1)
-        )
-
-    gradient_a = gradient_of(inputs[:, :1024])
-    gradient_b = gradient_of(inputs[:, 1024:])
+    gradient = pl.pallas_call(
+        gradient_kernel,
+        grid=(8,),
+        out_shape=jax.ShapeDtypeStruct((384, 2048), BF),
+        in_specs=[
+            pl.BlockSpec((3, 2048, 128), lambda n: (0, 0, 0)),
+            pl.BlockSpec((2048, 256), lambda n: (0, n)),
+        ],
+        out_specs=pl.BlockSpec((384, 256), lambda n: (0, n)),
+        scratch_shapes=[pltpu.VMEM((384, 2048), BF)],
+        compiler_params=pltpu.CompilerParams(vmem_limit_bytes=57 << 20),
+    )(cotangents, inputs)
     smem = pl.BlockSpec(memory_space=pltpu.SMEM)
-    partial_value, factor_all = pl.pallas_call(
+    core_id = core.reshape(1).astype(jnp.int32)
+    partial_value = pl.pallas_call(
         partial_kernel,
-        out_shape=(
-            jax.ShapeDtypeStruct((32, 24, 128), BF),
-            jax.ShapeDtypeStruct((2048, RANK), BF),
-        ),
-        in_specs=[smem] + [VMEM] * 4,
-        out_specs=(VMEM, VMEM),
+        out_shape=jax.ShapeDtypeStruct((32, 24, 128), BF),
+        in_specs=[smem] + [VMEM] * 3,
+        out_specs=VMEM,
+        scratch_shapes=[pltpu.VMEM((2048, RANK), BF)],
         compiler_params=pltpu.CompilerParams(vmem_limit_bytes=12 << 20),
-    )(core.reshape(1).astype(jnp.int32), gradient_a, gradient_b, half, other_half)
+    )(core_id, gradient, half, other_half)
+    factor_all = pl.pallas_call(
+        assemble,
+        out_shape=jax.ShapeDtypeStruct((2048, RANK), BF),
+        in_specs=[smem] + [VMEM] * 2,
+        out_specs=VMEM,
+        compiler_params=pltpu.CompilerParams(vmem_limit_bytes=8 << 20),
+    )(core_id, half, other_half)
     arrived = lax.all_to_all(partial_value, FS, split_axis=0, concat_axis=0, tiled=True)
     projected = arrived.astype(F32).sum(axis=0)
     projected_all = sent_to_all(projected.astype(BF), FS)

time: 104 us -> 103 us (level)
  starting transfers between devices: 56.1 us -> 30.4 us
  blocking collectives: 0 us -> 16.6 us
  waiting for transfers between devices: 18.9 us -> 32.5 us
  Pallas kernels: 5.17 us -> 15.9 us
  matrix products: 6.86 us -> 0 us
  local copies, waits for them, and re-layouts: 13.1 us -> 6.29 us
  other arithmetic: 1.88 us -> 0.21 us
    all_to_all x0 -> x1, blocking collectives: none -> 16.6 us  [sent_to_all(): return lax.all_to_all(copies, axis, split_axis=0, concat_axis=0, tiled=True)]
    ppermute x12 -> x5, starting transfers between devices: 21 us -> 9.15 us  [moved(): lax.ppermute(array, axis, [(i, (i + shift) % size) for i in range(size)])]
    pallas_call x1 -> x3, Pallas kernels: 0.72 us -> 11.4 us  [the longest x1 9.96 us: step(): pl.pallas_call(gradient_kernel, grid=(8,), out_shape=jax.ShapeDtypeStruct...]
    ppermute x0 -> x3, waiting for transfers between devices: none -> 8.71 us  [swapped(): return lax.ppermute(array, axis, [(i, i ^ bit) for i in range(size)])]
    all_to_all x1, starting transfers between devices: 10.7 us -> 3.86 us  [step(): lax.all_to_all(partial_value, FS, split_axis=0, concat_axis=0, tiled=True)]
    dot_general x2 -> x0, matrix products: 6.86 us -> none  [gradient_of(): jnp.einsum('mtc,td->mcd', cotangents, part, preferred_element_type=F32)]
    unnamed x26 -> x14, local copies, waits for them, and re-layouts: 8.75 us -> 2.46 us
    all_to_all x3 -> x2, waiting for transfers between devices: 6.04 us -> 11.8 us  [sent_to_all(): return lax.all_to_all(copies, axis, split_axis=0, concat_axis=0, tiled=True)]
  transfers between devices with their start and end apart: 17 -> 12, of which waited for: 7 -> 6; matrix products, arithmetic and copies ran while one was open for 15% -> 2% of each run, Pallas kernels for 1% -> 12%
where the time goes in v3:
time: 103 us
  waiting for transfers between devices  32.5 us (32%)
  starting transfers between devices  30.4 us (30%)
  blocking collectives  16.6 us (16%)
  Pallas kernels  15.9 us (15%)
  local copies, waits for them, and re-layouts  6.29 us (6%)
    all_to_all x1, blocking collectives, sent_to_all(): return lax.all_to_all(copies, axis, split_axis=0, concat_axis=0, tiled=True)  16.6 us
    all_to_all x2, waiting for transfers between devices, sent_to_all(): return lax.all_to_all(copies, axis, split_axis=0, concat_axis=0, tiled=True)  11.8 us
    pallas_call x1, Pallas kernels, step(): pl.pallas_call(gradient_kernel, grid=(8,), out_shape=jax.ShapeDtypeStruct...  9.96 us
    ppermute x5, starting transfers between devices, moved(): lax.ppermute(array, axis, [(i, (i + shift) % size) for i in range(size)])  9.15 us
    ppermute x3, waiting for transfers between devices, swapped(): return lax.ppermute(array, axis, [(i, i ^ bit) for i in range(size)])  8.71 us
    all_to_all x1, starting transfers between devices, step(): lax.all_to_all(squares, TP, split_axis=0, concat_axis=0, tiled=True)  8.49 us
    all_to_all x2, starting transfers between devices, sent_to_all(): return lax.all_to_all(copies, axis, split_axis=0, concat_axis=0, tiled=True)  8.05 us
    all_to_all x1, waiting for transfers between devices, step(): lax.all_to_all(partial_value, FS, split_axis=0, concat_axis=0, tiled=True)  7.17 us
  transfers between devices with their start and end apart: 12, of which 6 were waited for; matrix products, arithmetic and copies ran while one was open for 2% of the time, Pallas kernels for 12%

profile of v3, /device:TPU:1, one launch (start us, length us, event | category | flops | bytes accessed | tf_op | source)
XLA Modules:
  0.0 102.6 jit_solution(16696296219657639200)
XLA Ops:
  0.7 0.8 constant_dynamic-slice_fusion
  1.4 16.6 %all_to_all.25 = bf16[8,32,256]{2,1,0:T(8,128)(2,1)S(1)} all-to-all(bf16[8,32,256]{2,1,0:T(8,128)(2,1)S(1)} %broadcast_in_dim.10), channel_id=1, replica_groups=mesh['fs_0'=8,'fs_1'=4,'tp_0'=4,'tp_1'=2] {'fs_0'}, dimensions={0} | all-to-all | bytes 262144 | tf_op jit(solution)/shard_map/all_to_all | solution.py:22
  18.0 0.9 broadcast_in_dim.11
  18.9 4.2 %all-to-all-start.1 = ((bf16[4,8,32,256]{3,2,1,0:T(8,128)(2,1)}), bf16[4,8,32,256]{3,2,1,0:T(8,128)(2,1)S(1)}, u32[]{:S(2)}, u32[]{:S(2)}) async-start(bf16[4,8,32,256]{3,2,1,0:T(8,128)(2,1)} %broadcast_in_dim.11), calls=%async_computation.1 | async-start | bytes 1048576 | tf_op jit(solution)/shard_map/all_to_all | solution.py:22
  23.1 0.7 collective-permute-start.1
  23.8 6.2 %all-to-all-done.1.mine = bf16[4,8,32,256]{3,2,1,0:T(8,128)(2,1)S(1)} async-done(((bf16[4,8,32,256]{3,2,1,0:T(8,128)(2,1)}), bf16[4,8,32,256]{3,2,1,0:T(8,128)(2,1)S(1)}, u32[]{:S(2)}, u32[]{:S(2)}) %all-to-all-start.1) | async-done | bytes 524320 | tf_op jit(solution)/shard_map/all_to_all | solution.py:22
  30.0 3.7 %collective-permute-start = (bf16[4,8,32,256]{3,2,1,0:T(8,128)(2,1)S(1)}, bf16[4,8,32,256]{3,2,1,0:T(8,128)(2,1)S(1)}, u32[]{:S(2)}, u32[]{:S(2)}) collective-permute-start(bf16[4,8,32,256]{3,2,1,0:T(8,128)(2,1)S(1)} %all-to-all-done.1.mine), channel_id=1, source_target_pairs={{0,1},{1,0},{2,3},{3,2},{4,5},{5,4},{6,7},{7,6},{8,9},{9,8},{10,11... | collective-permute-start | bytes 1572872 | tf_op jit(solution)/shard_map/ppermute | solution.py:27
  33.7 0.1 collective-permute-start.2
  33.8 8.7 %collective-permute-done.2 = bf16[2,240,128]{2,1,0:T(8,128)(2,1)S(1)} collective-permute-done((bf16[2,240,128]{2,1,0:T(8,128)(2,1)S(1)}, bf16[2,240,128]{2,1,0:T(8,128)(2,1)S(1)}, u32[]{:S(2)}, u32[]{:S(2)}) %collective-permute-start.2) | collective-permute-done | bytes 122912 | tf_op jit(solution)/shard_map/ppermute | solution.py:32
  42.5 0.1 collective-permute-start.3
  42.6 10.0 %shard_map.101.gradient = bf16[384,2048]{1,0:T(8,128)(2,1)} custom-call(bf16[3,2048,128]{2,1,0:T(8,128)(2,1)} %cotangents.1, bf16[2048,2048]{1,0:T(8,128)(2,1)} %inputs.1), custom_call_target="tpu_custom_call" | custom-call | tf_op jit(solution)/shard_map/pallas_call | solution.py:146
  52.6 1.4 %copy-done = bf16[384,2048]{1,0:T(8,128)(2,1)S(1)} copy-done((bf16[384,2048]{1,0:T(8,128)(2,1)S(1)}, bf16[384,2048]{1,0:T(8,128)(2,1)}, u32[]{:S(2)}) %copy-start) | copy-done | bytes 1572888
  54.0 1.4 %shard_map.102 = bf16[32,24,128]{2,1,0:T(8,128)(2,1)} custom-call(s32[1]{0:T(128)} %bitcast.2.core, bf16[384,2048]{1,0:T(8,128)(2,1)S(1)} %copy-done, bf16[4,8,32,256]{3,2,1,0:T(8,128)(2,1)S(1)} %all-to-all-done.1.mine, bf16[4,8,32,256]{3,2,1,0:T(8,128)(2,1)S(1)} %collective-permute-done.other), custom_call_target="tpu_custom_call" | custom-call | tf_op jit(solution)/shard_map/pallas_call | solution.py:160
  55.4 3.9 %all-to-all-start.2 = ((bf16[32,24,128]{2,1,0:T(8,128)(2,1)}), bf16[32,24,128]{2,1,0:T(8,128)(2,1)S(1)}, u32[]{:S(2)}, u32[]{:S(2)}) async-start(bf16[32,24,128]{2,1,0:T(8,128)(2,1)} %shard_map.102), calls=%async_computation.2 | async-start | bytes 393216 | tf_op jit(solution)/shard_map/all_to_all | solution.py:175
  59.3 1.2 %collective-permute-start.4 = (bf16[8,240,128]{2,1,0:T(8,128)(2,1)S(1)}, bf16[8,240,128]{2,1,0:T(8,128)(2,1)S(1)}, u32[]{:S(2)}, u32[]{:S(2)}) collective-permute-start(bf16[8,240,128]{2,1,0:T(8,128)(2,1)S(1)} %pad_maximum_fusion.state), channel_id=1, source_target_pairs={{0,8},{8,16},{16,24},{24,0},{1,9},{9,17},{17,25},{25,1},{2,10},{10... | collective-permute-start | bytes 1474568 | tf_op jit(solution)/shard_map/ppermute | solution.py:27
  60.5 1.6 %collective-permute-start.5 = (bf16[8,240,128]{2,1,0:T(8,128)(2,1)S(1)}, bf16[8,240,128]{2,1,0:T(8,128)(2,1)S(1)}, u32[]{:S(2)}, u32[]{:S(2)}) collective-permute-start(bf16[8,240,128]{2,1,0:T(8,128)(2,1)S(1)} %pad_maximum_fusion.state), channel_id=1, source_target_pairs={{0,24},{8,0},{16,8},{24,16},{1,25},{9,1},{17,9},{25,17},{2,26},{10... | collective-permute-start | bytes 1474568 | tf_op jit(solution)/shard_map/ppermute | solution.py:27
  62.1 7.2 %all-to-all-done.2 = bf16[32,24,128]{2,1,0:T(8,128)(2,1)S(1)} async-done(((bf16[32,24,128]{2,1,0:T(8,128)(2,1)}), bf16[32,24,128]{2,1,0:T(8,128)(2,1)S(1)}, u32[]{:S(2)}, u32[]{:S(2)}) %all-to-all-start.2) | async-done | bytes 196640 | tf_op jit(solution)/shard_map/all_to_all | solution.py:175
  69.3 0.7 broadcast_in_dim.12
  70.0 3.9 %all-to-all-start.3 = ((bf16[32,24,128]{2,1,0:T(8,128)(2,1)}), bf16[32,24,128]{2,1,0:T(8,128)(2,1)S(1)}, u32[]{:S(2)}, u32[]{:S(2)}) async-start(bf16[32,24,128]{2,1,0:T(8,128)(2,1)} %broadcast_in_dim.12), calls=%async_computation.3 | async-start | bytes 393216 | tf_op jit(solution)/shard_map/all_to_all | solution.py:22
  73.9 0.2 collective-permute-done.4.right
  74.1 0.7 slice.8
  74.8 0.9 collective-permute-start.6
  75.7 0.8 slice.9
  76.5 1.8 %collective-permute-start.7 = (bf16[4,240,128]{2,1,0:T(8,128)(2,1)}, bf16[4,240,128]{2,1,0:T(8,128)(2,1)}, u32[]{:S(2)}, u32[]{:S(2)}) collective-permute-start(bf16[4,240,128]{2,1,0:T(8,128)(2,1)} %slice.9), channel_id=1, source_target_pairs={{0,24},{8,0},{16,8},{24,16},{1,25},{9,1},{17,9},{25,17},{2,26},{10... | collective-permute-start | bytes 737288 | tf_op jit(solution)/shard_map/ppermute | solution.py:27
  78.3 5.6 %all-to-all-done.3.projected = bf16[32,24,128]{2,1,0:T(8,128)(2,1)S(1)} async-done(((bf16[32,24,128]{2,1,0:T(8,128)(2,1)}), bf16[32,24,128]{2,1,0:T(8,128)(2,1)S(1)}, u32[]{:S(2)}, u32[]{:S(2)}) %all-to-all-start.3) | async-done | bytes 196640 | tf_op jit(solution)/shard_map/all_to_all | solution.py:22
  83.9 0.7 shard_map.103
  84.6 8.5 %all-to-all-start.4 = ((f32[8,8,128]{2,1,0:T(8,128)}), f32[8,8,128]{2,1,0:T(8,128)S(1)}, u32[]{:S(2)}, u32[]{:S(2)}) async-start(f32[8,8,128]{2,1,0:T(8,128)} %shard_map.103), calls=%async_computation.4 | async-start | bytes 65536 | tf_op jit(solution)/shard_map/all_to_all | solution.py:185
  93.1 0.1 pad_add_fusion.place
  93.2 0.1 shard_map.104.factor
  93.3 4.5 %all-to-all-done.4.squares = f32[8,8,128]{2,1,0:T(8,128)S(1)} async-done(((f32[8,8,128]{2,1,0:T(8,128)}), f32[8,8,128]{2,1,0:T(8,128)S(1)}, u32[]{:S(2)}, u32[]{:S(2)}) %all-to-all-start.4) | async-done | bytes 32800 | tf_op jit(solution)/shard_map/all_to_all | solution.py:185
  97.8 1.0 %copy-done.2 = bf16[8,240,128]{2,1,0:T(8,128)(2,1)S(1)} copy-done((bf16[8,240,128]{2,1,0:T(8,128)(2,1)S(1)}, bf16[8,240,128]{2,1,0:T(8,128)(2,1)}, u32[]{:S(2)}) %copy-start.2) | copy-done | bytes 491544
  98.8 3.7 %shard_map.105 = (f32[3,64,128]{2,1,0:T(8,128)}, f32[3,64,128]{2,1,0:T(8,128)}, bf16[3,2048,128]{2,1,0:T(8,128)(2,1)}, f32[3,8,128]{2,1,0:T(8,128)}, f32[3,8,128]{2,1,0:T(8,128)}) custom-call(s32[2]{0:T(128)S(1)} %pad_add_fusion.place, f32[8,8,128]{2,1,0:T(8,128)S(1)} %all-to-all-done.4.squares, bf16[32,24,128]{2,1,0:T(8,128)(2,1)S(1)} %all-to-all-done.3.projected, ...), custom_call_target="tpu_custom_call" | custom-call | tf_op jit(solution)/shard_map/pallas_call | solution.py:186
  (27 shorter events, 0.2 us)
Async XLA Ops:
  0.6 22.4 %copy-start.3 = (f32[3,64,128]{2,1,0:T(8,128)S(1)}, f32[3,64,128]{2,1,0:T(8,128)}, u32[]{:S(2)}) copy-start(f32[3,64,128]{2,1,0:T(8,128)} %weights.1) | copy-start | bytes 294916
  0.6 22.4 %copy-start.6 = (f32[3,8,128]{2,1,0:T(8,128)S(1)}, f32[3,8,128]{2,1,0:T(8,128)}, u32[]{:S(2)}) copy-start(f32[3,8,128]{2,1,0:T(8,128)} %first.1) | copy-start | bytes 36868
  0.7 22.4 %copy-start.5 = (f32[3,8,128]{2,1,0:T(8,128)S(1)}, f32[3,8,128]{2,1,0:T(8,128)}, u32[]{:S(2)}) copy-start(f32[3,8,128]{2,1,0:T(8,128)} %second.1) | copy-start | bytes 36868
  18.9 11.1 %all-to-all-start.1 = ((bf16[4,8,32,256]{3,2,1,0:T(8,128)(2,1)}), bf16[4,8,32,256]{3,2,1,0:T(8,128)(2,1)S(1)}, u32[]{:S(2)}, u32[]{:S(2)}) async-start(bf16[4,8,32,256]{3,2,1,0:T(8,128)(2,1)} %broadcast_in_dim.11), calls=%async_computation.1 | async-start | bytes 1048576 | tf_op jit(solution)/shard_map/all_to_all | solution.py:22
  23.1 10.6 %collective-permute-start.1 = (bf16[1,240,128]{2,1,0:T(8,128)(2,1)S(1)}, bf16[1,240,128]{2,1,0:T(8,128)(2,1)S(1)}, u32[]{:S(2)}, u32[]{:S(2)}) collective-permute-start(bf16[1,240,128]{2,1,0:T(8,128)(2,1)S(1)} %pad_maximum_fusion.3), channel_id=1, source_target_pairs={{0,128},{32,160},{64,192},{96,224},{128,0},{160,32},{192,64},{224,... | collective-permute-start | bytes 184328 | tf_op jit(solution)/shard_map/ppermute | solution.py:32
  30.0 22.6 %collective-permute-start = (bf16[4,8,32,256]{3,2,1,0:T(8,128)(2,1)S(1)}, bf16[4,8,32,256]{3,2,1,0:T(8,128)(2,1)S(1)}, u32[]{:S(2)}, u32[]{:S(2)}) collective-permute-start(bf16[4,8,32,256]{3,2,1,0:T(8,128)(2,1)S(1)} %all-to-all-done.1.mine), channel_id=1, source_target_pairs={{0,1},{1,0},{2,3},{3,2},{4,5},{5,4},{6,7},{7,6},{8,9},{9,8},{10,11... | collective-permute-start | bytes 1572872 | tf_op jit(solution)/shard_map/ppermute | solution.py:27
  33.7 8.8 %collective-permute-start.2 = (bf16[2,240,128]{2,1,0:T(8,128)(2,1)S(1)}, bf16[2,240,128]{2,1,0:T(8,128)(2,1)S(1)}, u32[]{:S(2)}, u32[]{:S(2)}) collective-permute-start(bf16[2,240,128]{2,1,0:T(8,128)(2,1)S(1)} %pad_maximum_fusion.2), channel_id=1, source_target_pairs={{0,64},{32,96},{64,0},{96,32},{128,192},{160,224},{192,128},{224,1... | collective-permute-start | bytes 368648 | tf_op jit(solution)/shard_map/ppermute | solution.py:32
  42.5 16.7 %collective-permute-start.3 = (bf16[4,240,128]{2,1,0:T(8,128)(2,1)S(1)}, bf16[4,240,128]{2,1,0:T(8,128)(2,1)S(1)}, u32[]{:S(2)}, u32[]{:S(2)}) collective-permute-start(bf16[4,240,128]{2,1,0:T(8,128)(2,1)S(1)} %pad_maximum_fusion.1), channel_id=1, source_target_pairs={{0,32},{32,0},{64,96},{96,64},{128,160},{160,128},{192,224},{224,1... | collective-permute-start | bytes 737288 | tf_op jit(solution)/shard_map/ppermute | solution.py:32
  52.6 1.4 %copy-start = (bf16[384,2048]{1,0:T(8,128)(2,1)S(1)}, bf16[384,2048]{1,0:T(8,128)(2,1)}, u32[]{:S(2)}) copy-start(bf16[384,2048]{1,0:T(8,128)(2,1)} %shard_map.101.gradient) | copy-start | bytes 4718596
  55.4 13.8 %all-to-all-start.2 = ((bf16[32,24,128]{2,1,0:T(8,128)(2,1)}), bf16[32,24,128]{2,1,0:T(8,128)(2,1)S(1)}, u32[]{:S(2)}, u32[]{:S(2)}) async-start(bf16[32,24,128]{2,1,0:T(8,128)(2,1)} %shard_map.102), calls=%async_computation.2 | async-start | bytes 393216 | tf_op jit(solution)/shard_map/all_to_all | solution.py:175
  59.3 14.8 %collective-permute-start.4 = (bf16[8,240,128]{2,1,0:T(8,128)(2,1)S(1)}, bf16[8,240,128]{2,1,0:T(8,128)(2,1)S(1)}, u32[]{:S(2)}, u32[]{:S(2)}) collective-permute-start(bf16[8,240,128]{2,1,0:T(8,128)(2,1)S(1)} %pad_maximum_fusion.state), channel_id=1, source_target_pairs={{0,8},{8,16},{16,24},{24,0},{1,9},{9,17},{17,25},{25,1},{2,10},{10... | collective-permute-start | bytes 1474568 | tf_op jit(solution)/shard_map/ppermute | solution.py:27
  60.5 15.2 %collective-permute-start.5 = (bf16[8,240,128]{2,1,0:T(8,128)(2,1)S(1)}, bf16[8,240,128]{2,1,0:T(8,128)(2,1)S(1)}, u32[]{:S(2)}, u32[]{:S(2)}) collective-permute-start(bf16[8,240,128]{2,1,0:T(8,128)(2,1)S(1)} %pad_maximum_fusion.state), channel_id=1, source_target_pairs={{0,24},{8,0},{16,8},{24,16},{1,25},{9,1},{17,9},{25,17},{2,26},{10... | collective-permute-start | bytes 1474568 | tf_op jit(solution)/shard_map/ppermute | solution.py:27
  70.0 13.9 %all-to-all-start.3 = ((bf16[32,24,128]{2,1,0:T(8,128)(2,1)}), bf16[32,24,128]{2,1,0:T(8,128)(2,1)S(1)}, u32[]{:S(2)}, u32[]{:S(2)}) async-start(bf16[32,24,128]{2,1,0:T(8,128)(2,1)} %broadcast_in_dim.12), calls=%async_computation.3 | async-start | bytes 393216 | tf_op jit(solution)/shard_map/all_to_all | solution.py:22
  74.8 23.0 %copy-start.4 = (bf16[64,256]{1,0:T(8,128)(2,1)S(1)}, bf16[64,256]{1,0:T(8,128)(2,1)}, u32[]{:S(2)}) copy-start(bf16[64,256]{1,0:T(8,128)(2,1)} %own_factor.1) | copy-start | bytes 98308
  74.8 18.4 %collective-permute-start.6 = (bf16[4,240,128]{2,1,0:T(8,128)(2,1)}, bf16[4,240,128]{2,1,0:T(8,128)(2,1)}, u32[]{:S(2)}, u32[]{:S(2)}) collective-permute-start(bf16[4,240,128]{2,1,0:T(8,128)(2,1)} %slice.8), channel_id=1, source_target_pairs={{0,8},{8,16},{16,24},{24,0},{1,9},{9,17},{17,25},{25,1},{2,10},{10... | collective-permute-start | bytes 737288 | tf_op jit(solution)/shard_map/ppermute | solution.py:27
  75.7 17.3 %copy-start.1 = (bf16[8,240,128]{2,1,0:T(8,128)(2,1)}, bf16[8,240,128]{2,1,0:T(8,128)(2,1)S(1)}, u32[]{:S(2)}) copy-start(bf16[8,240,128]{2,1,0:T(8,128)(2,1)S(1)} %collective-permute-done.5.left) | copy-start | bytes 1474564
  76.5 16.7 %collective-permute-start.7 = (bf16[4,240,128]{2,1,0:T(8,128)(2,1)}, bf16[4,240,128]{2,1,0:T(8,128)(2,1)}, u32[]{:S(2)}, u32[]{:S(2)}) collective-permute-start(bf16[4,240,128]{2,1,0:T(8,128)(2,1)} %slice.9), channel_id=1, source_target_pairs={{0,24},{8,0},{16,8},{24,16},{1,25},{9,1},{17,9},{25,17},{2,26},{10... | collective-permute-start | bytes 737288 | tf_op jit(solution)/shard_map/ppermute | solution.py:27
  84.6 13.2 %all-to-all-start.4 = ((f32[8,8,128]{2,1,0:T(8,128)}), f32[8,8,128]{2,1,0:T(8,128)S(1)}, u32[]{:S(2)}, u32[]{:S(2)}) async-start(f32[8,8,128]{2,1,0:T(8,128)} %shard_map.103), calls=%async_computation.4 | async-start | bytes 65536 | tf_op jit(solution)/shard_map/all_to_all | solution.py:185
  97.8 1.0 %copy-start.2 = (bf16[8,240,128]{2,1,0:T(8,128)(2,1)S(1)}, bf16[8,240,128]{2,1,0:T(8,128)(2,1)}, u32[]{:S(2)}) copy-start(bf16[8,240,128]{2,1,0:T(8,128)(2,1)} %copy-done.1) | copy-start | bytes 1474564

commit v4 on v2

v4 whole, which is shorter than its diff:
```python
import jax
import jax.numpy as jnp
from jax import lax
from jax.experimental import pallas as pl
from jax.experimental.pallas import tpu as pltpu
from jax.sharding import Mesh
from jax.sharding import PartitionSpec as P

MW = 1024
RANK = 256
Z, Y = ("fs_0", "fs_1")
FS = ("fs_0", "fs_1")
TP = ("tp_0", "tp_1")
CORE = "tp_1"
BF = jnp.bfloat16
F32 = jnp.float32
VMEM = pl.BlockSpec(memory_space=pltpu.VMEM)


def sent_to_all(array, axis):
    copies = jnp.broadcast_to(array, (lax.axis_size(axis), *array.shape))
    return lax.all_to_all(copies, axis, split_axis=0, concat_axis=0, tiled=True)


def moved(array, axis, shift):
    size = lax.axis_size(axis)
    return lax.ppermute(array, axis, [(i, (i + shift) % size) for i in range(size)])


def swapped(array, axis, bit):
    size = lax.axis_size(axis)
    return lax.ppermute(array, axis, [(i, i ^ bit) for i in range(size)])


def gathered_z(array):
    for bit in (4, 2, 1):
        array = jnp.concatenate([array, swapped(array, Z, bit)])
    return array


def gathered_y(array):
    right = moved(array, Y, 1)
    left = moved(array, Y, -1)
    return (
        array, right, left,
        moved(right[:4], Y, 1), moved(left[4:], Y, -1),
    )


def spread_kernel(place, factor, out):
    rows = factor[pl.ds(pl.multiple_of(place[2] * 32, 32), 32)]
    out[...] = jnp.broadcast_to(rows, out.shape)


def state_kernel(weights, first, second, out):
    out[0, :192] = weights[...].reshape(192, 128).astype(BF)
    moments = jnp.concatenate([first[...].reshape(24, 128), second[...].reshape(24, 128)])
    out[0, 192:] = moments.astype(BF)


def assemble(place, mine, other, factor):
    for z in range(8):
        for y in range(4):
            row = z * 256 + y * 64
            factor[pl.ds(row + pl.multiple_of(place[2] * 32, 32), 32)] = mine[y, z]
            factor[pl.ds(row + pl.multiple_of(32 - place[2] * 32, 32), 32)] = other[y, z]


def partial_kernel(place, gradient_a, gradient_b, mine, other, out, factor, held, sem):
    copy = pltpu.make_async_copy(gradient_b, held, sem)
    copy.start()
    assemble(place, mine, other, factor)
    projected = jnp.dot(gradient_a[...], factor[:1024], preferred_element_type=F32)
    copy.wait()
    projected += jnp.dot(held[...], factor[1024:], preferred_element_type=F32)
    rows = [projected[m * 128 : (m + 1) * 128].T.reshape(32, 8, 128) for m in range(3)]
    out[...] = jnp.concatenate(rows, axis=1).astype(BF)


def square_kernel(projected, out):
    values = projected[...].astype(F32).reshape(96, 8, 128)
    out[...] = jnp.broadcast_to(jnp.sum(values * values, axis=0), out.shape)


def moments(clip, projected, first, second):
    clipped = clip * projected
    new_first = 0.9 * first + 0.1 * clipped
    new_second = 0.95 * second + 0.05 * clipped * clipped
    return new_first, new_second, new_first / (jnp.sqrt(new_second) + 1e-08)


def final_kernel(
    place, squares, projected, own, state, right, left, across_a, across_b,
    first, second, weights, factor, own_factor,
    update_out, weights_out, copies_out, first_out, second_out,
    update, new_weights, copies, new_first, new_second, normed, change, own_sems, sems,
):
    total = jnp.sum(jnp.sum(squares[...], axis=0), keepdims=True)
    root_mean = jnp.sqrt(total / (3 * RANK * MW) + 1e-06)
    clip = jnp.minimum(1.0, 0.25 / root_mean)

    def blocks_of(j):
        across = across_a.at[j] if j < 4 else across_b.at[j - 4]
        z = place[0] ^ (j // 4 + (j // 2 % 2) * 2 + (j % 2) * 4)
        return [
            (z * 4 + (place[1] + 4 - i) % 4, block)
            for i, block in enumerate((state.at[j], right.at[j], across, left.at[j]))
        ]

    blocks = [blocks_of(j) for j in range(8)]
    for m in range(3):
        own_first, own_second, _ = moments(
            clip, own[m * 8 : (m + 1) * 8], first[m], second[m]
        )
        new_first[m] = own_first
        new_second[m] = own_second
    for j in range(8):
        for at, block in blocks[j]:
            _, _, values = moments(
                clip,
                projected[at].astype(F32),
                block[192:216].astype(F32),
                block[216:240].astype(F32),
            )
            for m in range(3):
                normed[pl.ds(pl.multiple_of(at * 8, 8), 8), m * 128 : (m + 1) * 128] = values[
                    m * 8 : (m + 1) * 8
                ]
    values = normed[...].astype(BF)
    own_change = jnp.dot(own_factor[...], values, preferred_element_type=F32)
    for m in range(3):
        part = own_change[:, m * 128 : (m + 1) * 128]
        update[m] = part
        new_weights[m] = weights[m] - 0.02 * part
    sent = [
        pltpu.make_async_copy(source, target, own_sems.at[k])
        for k, (source, target) in enumerate(
            (
                (update, update_out), (new_weights, weights_out),
                (new_first, first_out), (new_second, second_out),
            )
        )
    ]
    for copy in sent:
        copy.start()
    for q in range(4):
        base = pl.multiple_of(blocks[q][0][0] // 8 * 512, 512)
        change[q % 2] = jnp.dot(
            factor[pl.ds(base, 512)], values, preferred_element_type=F32
        )
        for at, block in blocks[q] + blocks[q + 4]:
            rows = pl.ds(pl.multiple_of(at * 64, 64), 64)
            inner = pl.ds(pl.multiple_of(at * 64 - base, 64), 64)
            for m in range(3):
                before = block[m * 64 : (m + 1) * 64].astype(F32)
                part = change[q % 2, inner, m * 128 : (m + 1) * 128]
                copies[m, rows] = (before - 0.02 * part).astype(BF)
        for m in range(3):
            rows = pl.ds(base, 512)
            copy = pltpu.make_async_copy(
                copies.at[m, rows], copies_out.at[m, rows], sems.at[q, m]
            )
            copy.start()
            sent.append(copy)
    for copy in sent:
        copy.wait()


def step(inputs, cotangents, factor, weights, first_moment, second_moment):
    place = jnp.stack([lax.axis_index(axis) for axis in (Z, Y, CORE)]).astype(jnp.int32)
    smem = pl.BlockSpec(memory_space=pltpu.SMEM)
    hbm = pl.BlockSpec(memory_space=pl.ANY)
    half = pl.pallas_call(
        spread_kernel,
        out_shape=jax.ShapeDtypeStruct((8, 32, RANK), BF),
        in_specs=[smem, VMEM],
        out_specs=VMEM,
        compiler_params=pltpu.CompilerParams(vmem_limit_bytes=60 << 20),
    )(place, factor)
    half = lax.all_to_all(half, Z, split_axis=0, concat_axis=0, tiled=True)
    half = sent_to_all(half, Y)
    other_half = moved(half, CORE, 1)
    state = pl.pallas_call(
        state_kernel,
        out_shape=jax.ShapeDtypeStruct((1, 240, 128), BF),
        in_specs=[VMEM] * 3,
        out_specs=VMEM,
        compiler_params=pltpu.CompilerParams(vmem_limit_bytes=60 << 20),
    )(weights, first_moment, second_moment)
    state_z = gathered_z(state)
    states = gathered_y(state_z)


    def gradient_of(part):
        return (
            jnp.einsum("mtc,td->mcd", cotangents, part, preferred_element_type=F32)
            .astype(BF)
            .reshape(384, -1)
        )

    gradient_a = gradient_of(inputs[:, :1024])
    gradient_b = gradient_of(inputs[:, 1024:])
    partial_value = pl.pallas_call(
        partial_kernel,
        out_shape=jax.ShapeDtypeStruct((32, 24, 128), BF),
        in_specs=[smem, VMEM, hbm, VMEM, VMEM],
        out_specs=VMEM,
        scratch_shapes=[
            pltpu.VMEM((2048, RANK), BF),
            pltpu.VMEM((384, 1024), BF),
            pltpu.SemaphoreType.DMA,
        ],
        compiler_params=pltpu.CompilerParams(vmem_limit_bytes=12 << 20),
    )(place, gradient_a, gradient_b, half, other_half)
    factor_all = pl.pallas_call(
        assemble,
        out_shape=jax.ShapeDtypeStruct((2048, RANK), BF),
        in_specs=[smem] + [VMEM] * 2,
        out_specs=VMEM,
        compiler_params=pltpu.CompilerParams(vmem_limit_bytes=8 << 20),
    )(place, half, other_half)
    arrived = lax.all_to_all(partial_value, FS, split_axis=0, concat_axis=0, tiled=True)
    projected = arrived.astype(F32).sum(axis=0)
    projected_all = sent_to_all(projected.astype(BF), FS)
    squares = pl.pallas_call(
        square_kernel,
        out_shape=jax.ShapeDtypeStruct((8, 8, 128), F32),
        in_specs=[VMEM],
        out_specs=VMEM,
        compiler_params=pltpu.CompilerParams(vmem_limit_bytes=4 << 20),
    )(projected_all)
    squares = lax.all_to_all(squares, TP, split_axis=0, concat_axis=0, tiled=True)
    return pl.pallas_call(
        final_kernel,
        out_shape=(
            jax.ShapeDtypeStruct((3, 64, 128), F32),
            jax.ShapeDtypeStruct((3, 64, 128), F32),
            jax.ShapeDtypeStruct((3, 2048, 128), BF),
            jax.ShapeDtypeStruct((3, 8, 128), F32),
            jax.ShapeDtypeStruct((3, 8, 128), F32),
        ),
        in_specs=[smem] + [VMEM] * 13,
        out_specs=(hbm,) * 5,
        scratch_shapes=[
            pltpu.VMEM((3, 64, 128), F32),
            pltpu.VMEM((3, 64, 128), F32),
            pltpu.VMEM((3, 2048, 128), BF),
            pltpu.VMEM((3, 8, 128), F32),
            pltpu.VMEM((3, 8, 128), F32),
            pltpu.VMEM((RANK, 384), F32),
            pltpu.VMEM((2, 512, 384), F32),
            pltpu.SemaphoreType.DMA((4,)),
            pltpu.SemaphoreType.DMA((4, 3)),
        ],
        compiler_params=pltpu.CompilerParams(vmem_limit_bytes=24 << 20),
    )(
        place, squares, projected_all, projected, *states, first_moment, second_moment,
        weights, factor_all, factor,
    )


def solution(mesh):
    torus = Mesh(mesh.devices.reshape(8, 4, 4, 2), ("fs_0", "fs_1", "tp_0", "tp_1"))
    return jax.shard_map(
        step,
        mesh=torus,
        in_specs=(
            P(FS, None),
            P(None, FS, TP),
            P(FS, None),
            P(None, FS, TP),
            P(None, FS, TP),
            P(None, FS, TP),
        ),
        out_specs=(
            P(None, FS, TP),
            P(None, FS, TP),
            P(None, None, TP),
            P(None, FS, TP),
            P(None, FS, TP),
        ),
        check_vma=False,
    )
```

time: 104 us -> 99.2 us (0.954)
  starting transfers between devices: 56.1 us -> 47.7 us
  local copies, waits for them, and re-layouts: 13.1 us -> 7.86 us
  Pallas kernels: 5.17 us -> 10 us
  waiting for transfers between devices: 18.9 us -> 20.8 us
  other arithmetic: 1.88 us -> 3.19 us
  matrix products: 6.86 us -> 7.99 us
    ppermute x12 -> x5, starting transfers between devices: 21 us -> 10.5 us  [moved(): lax.ppermute(array, axis, [(i, (i + shift) % size) for i in range(size)])]
    all_to_all x0 -> x1, starting transfers between devices: none -> 9 us  [step(): half = lax.all_to_all(half, Z, split_axis=0, concat_axis=0, tiled=True)]
    ppermute x0 -> x3, starting transfers between devices: none -> 7.43 us  [swapped(): return lax.ppermute(array, axis, [(i, i ^ bit) for i in range(size)])]
    all_to_all x1, starting transfers between devices: 10.7 us -> 5.26 us  [step(): lax.all_to_all(partial_value, FS, split_axis=0, concat_axis=0, tiled=True)]
    pallas_call x1 -> x4, Pallas kernels: 0.72 us -> 5.69 us  [the longest x1 2.1 us: step(): pl.pallas_call(partial_kernel, out_shape=jax.ShapeDtypeStruct((32, 24, 12...]
    all_to_all x3 -> x2, starting transfers between devices: 13.2 us -> 8.29 us  [sent_to_all(): return lax.all_to_all(copies, axis, split_axis=0, concat_axis=0, tiled=True)]
    unnamed x26, local copies, waits for them, and re-layouts: 8.75 us -> 3.93 us
    all_to_all x1, starting transfers between devices: 11.2 us -> 7.26 us  [step(): lax.all_to_all(squares, TP, split_axis=0, concat_axis=0, tiled=True)]
  transfers between devices with their start and end apart: 17 -> 13, of which waited for: 7 -> 5; matrix products, arithmetic and copies ran while one was open for 15% -> 15% of each run, Pallas kernels for 1% -> 5%
where the time goes in v4:
time: 99.2 us; the launch traced here: 98.4 us
  starting transfers between devices  47.7 us (48%)
  waiting for transfers between devices  20.8 us (21%)
  Pallas kernels  10 us (10%)
  matrix products  7.99 us (8%)
  local copies, waits for them, and re-layouts  7.86 us (8%)
  other arithmetic  3.19 us (3%)
    ppermute x5, starting transfers between devices, moved(): lax.ppermute(array, axis, [(i, (i + shift) % size) for i in range(size)])  10.5 us
    all_to_all x1, starting transfers between devices, step(): half = lax.all_to_all(half, Z, split_axis=0, concat_axis=0, tiled=True)  9 us
    all_to_all x2, starting transfers between devices, sent_to_all(): return lax.all_to_all(copies, axis, split_axis=0, concat_axis=0, tiled=True)  8.29 us
    dot_general x2, matrix products, gradient_of(): jnp.einsum('mtc,td->mcd', cotangents, part, preferred_element_type=F32)  7.99 us
    ppermute x3, starting transfers between devices, swapped(): return lax.ppermute(array, axis, [(i, i ^ bit) for i in range(size)])  7.43 us
    all_to_all x1, starting transfers between devices, step(): lax.all_to_all(squares, TP, split_axis=0, concat_axis=0, tiled=True)  7.26 us
    all_to_all x2, waiting for transfers between devices, sent_to_all(): return lax.all_to_all(copies, axis, split_axis=0, concat_axis=0, tiled=True)  7.16 us
    all_to_all x1, waiting for transfers between devices, step(): lax.all_to_all(partial_value, FS, split_axis=0, concat_axis=0, tiled=True)  7.06 us
  transfers between devices with their start and end apart: 13, of which 5 were waited for; matrix products, arithmetic and copies ran while one was open for 15% of the time, Pallas kernels for 5%

profile of v4, /device:TPU:1, one launch (start us, length us, event | category | flops | bytes accessed | tf_op | source)
XLA Modules:
  0.0 98.4 jit_solution(1566884636456070455)
XLA Ops:
  1.2 1.4 %shard_map.101 = bf16[8,32,256]{2,1,0:T(8,128)(2,1)} custom-call(s32[3]{0:T(128)} %pad_add_fusion.place, bf16[64,256]{1,0:T(8,128)(2,1)} %own_factor.1), custom_call_target="tpu_custom_call" | custom-call | tf_op jit(solution)/shard_map/pallas_call | solution.py:173
  2.7 9.0 %all-to-all-start = ((bf16[8,32,256]{2,1,0:T(8,128)(2,1)}), bf16[8,32,256]{2,1,0:T(8,128)(2,1)S(1)}, u32[]{:S(2)}, u32[]{:S(2)}) async-start(bf16[8,32,256]{2,1,0:T(8,128)(2,1)} %shard_map.101), calls=%async_computation | async-start | bytes 262144 | tf_op jit(solution)/shard_map/all_to_all | solution.py:180
  11.7 1.5 %shard_map.104 = bf16[1,240,128]{2,1,0:T(8,128)(2,1)} custom-call(f32[3,64,128]{2,1,0:T(8,128)} %weights.3, f32[3,8,128]{2,1,0:T(8,128)} %first.3, f32[3,8,128]{2,1,0:T(8,128)} %second.3), custom_call_target="tpu_custom_call" | custom-call | tf_op jit(solution)/shard_map/pallas_call | solution.py:183
  13.2 5.4 %collective-permute-start.1 = (bf16[1,240,128]{2,1,0:T(8,128)(2,1)}, bf16[1,240,128]{2,1,0:T(8,128)(2,1)S(1)}, u32[]{:S(2)}, u32[]{:S(2)}) collective-permute-start(bf16[1,240,128]{2,1,0:T(8,128)(2,1)} %shard_map.104), channel_id=1, source_target_pairs={{0,128},{32,160},{64,192},{96,224},{128,0},{160,32},{192,64},{224,... | collective-permute-start | bytes 184328 | tf_op jit(solution)/shard_map/ppermute | solution.py:32
  18.6 3.5 %collective-permute-done.1 = bf16[1,240,128]{2,1,0:T(8,128)(2,1)S(1)} collective-permute-done((bf16[1,240,128]{2,1,0:T(8,128)(2,1)}, bf16[1,240,128]{2,1,0:T(8,128)(2,1)S(1)}, u32[]{:S(2)}, u32[]{:S(2)}) %collective-permute-start.1) | collective-permute-done | bytes 61472 | tf_op jit(solution)/shard_map/ppermute | solution.py:32
  22.1 0.8 pad_maximum_fusion.2
  22.9 0.9 collective-permute-start.2
  23.8 0.9 broadcast_in_dim.6
  24.7 4.2 %all-to-all-start.1 = ((bf16[4,8,32,256]{3,2,1,0:T(8,128)(2,1)}), bf16[4,8,32,256]{3,2,1,0:T(8,128)(2,1)S(1)}, u32[]{:S(2)}, u32[]{:S(2)}) async-start(bf16[4,8,32,256]{3,2,1,0:T(8,128)(2,1)} %broadcast_in_dim.6), calls=%async_computation.1 | async-start | bytes 1048576 | tf_op jit(solution)/shard_map/all_to_all | solution.py:22
  28.8 4.0 %fusion.9 = bf16[3,128,1024]{2,1,0:T(8,128)(2,1)S(1)} fusion(bf16[3,2048,128]{2,1,0:T(8,128)(2,1)S(1)} %copy-done, bf16[2048,2048]{1,0:T(8,128)(2,1)} %param.6), kind=kOutput, calls=%fused_computation.7 | convolution fusion | flops 1611005952 | bytes 6553600 | tf_op jit(solution)/shard_map/mtc,td->mcd/dot_general | solution.py:196
  32.9 2.9 %all-to-all-done.1.mine = bf16[4,8,32,256]{3,2,1,0:T(8,128)(2,1)S(1)} async-done(((bf16[4,8,32,256]{3,2,1,0:T(8,128)(2,1)}), bf16[4,8,32,256]{3,2,1,0:T(8,128)(2,1)S(1)}, u32[]{:S(2)}, u32[]{:S(2)}) %all-to-all-start.1) | async-done | bytes 524320 | tf_op jit(solution)/shard_map/all_to_all | solution.py:22
  35.8 4.7 %collective-permute-start = (bf16[4,8,32,256]{3,2,1,0:T(8,128)(2,1)S(1)}, bf16[4,8,32,256]{3,2,1,0:T(8,128)(2,1)S(1)}, u32[]{:S(2)}, u32[]{:S(2)}) collective-permute-start(bf16[4,8,32,256]{3,2,1,0:T(8,128)(2,1)S(1)} %all-to-all-done.1.mine), channel_id=1, source_target_pairs={{0,1},{1,0},{2,3},{3,2},{4,5},{5,4},{6,7},{7,6},{8,9},{9,8},{10,11... | collective-permute-start | bytes 1572872 | tf_op jit(solution)/shard_map/ppermute | solution.py:27
  40.4 0.7 pad_maximum_fusion.1
  41.2 1.2 %collective-permute-start.3 = (bf16[4,240,128]{2,1,0:T(8,128)(2,1)}, bf16[4,240,128]{2,1,0:T(8,128)(2,1)}, u32[]{:S(2)}, u32[]{:S(2)}) collective-permute-start(bf16[4,240,128]{2,1,0:T(8,128)(2,1)} %pad_maximum_fusion.1), channel_id=1, source_target_pairs={{0,32},{32,0},{64,96},{96,64},{128,160},{160,128},{192,224},{224,1... | collective-permute-start | bytes 737288 | tf_op jit(solution)/shard_map/ppermute | solution.py:32
  42.3 4.0 %fusion.6 = bf16[3,128,1024]{2,1,0:T(8,128)(2,1)S(1)} fusion(bf16[3,2048,128]{2,1,0:T(8,128)(2,1)S(1)} %copy-done, bf16[2048,2048]{1,0:T(8,128)(2,1)} %param.6), kind=kOutput, calls=%fused_computation.6 | convolution fusion | flops 1611005952 | bytes 6553600 | tf_op jit(solution)/shard_map/mtc,td->mcd/dot_general | solution.py:196
  46.4 2.1 %shard_map.102 = bf16[32,24,128]{2,1,0:T(8,128)(2,1)} custom-call(s32[3]{0:T(128)S(1)} %copy-done.11, bf16[384,1024]{1,0:T(8,128)(2,1)S(1)} %bitcast.18, bf16[384,1024]{1,0:T(8,128)(2,1)S(1)} %bitcast.17, bf16[4,8,32,256]{3,2,1,0:T(8,128)(2,1)S(1)} %all-to-all-done.1.mine, bf16[4,8,32,256]{3,2,1,0:T(8,128)(2,1)S(1)} %collective-permute-done.other), custom_call_target="tpu_custom_call" | custom-call | tf_op jit(solution)/shard_map/pallas_call | solution.py:203
  48.5 0.8 copy-done.1
  49.3 5.3 %all-to-all-start.2 = ((bf16[32,24,128]{2,1,0:T(8,128)(2,1)}), bf16[32,24,128]{2,1,0:T(8,128)(2,1)S(1)}, u32[]{:S(2)}, u32[]{:S(2)}) async-start(bf16[32,24,128]{2,1,0:T(8,128)(2,1)} %shard_map.102), calls=%async_computation.2 | async-start | bytes 393216 | tf_op jit(solution)/shard_map/all_to_all | solution.py:222
  54.5 1.0 %pad_maximum_fusion.state = bf16[8,240,128]{2,1,0:T(8,128)(2,1)S(1)} fusion(bf16[4,240,128]{2,1,0:T(8,128)(2,1)} %collective-permute-done.3, bf16[2,240,128]{2,1,0:T(8,128)(2,1)S(1)} %collective-permute-done.2, bf16[1,240,128]{2,1,0:T(8,128)(2,1)S(1)} %collective-permute-done.1, bf16[1,240,128]{2,1,0:T(8,128)(2,1)S(1)} %copy-done.12), kind=kLoop, calls=%fused_computation.8 | loop fusion | flops 737280 | bytes 983040 | tf_op jit(solution)/shard_map/concatenate | solution.py:37
  55.6 2.5 %collective-permute-start.5 = (bf16[8,240,128]{2,1,0:T(8,128)(2,1)S(1)}, bf16[8,240,128]{2,1,0:T(8,128)(2,1)S(1)}, u32[]{:S(2)}, u32[]{:S(2)}) collective-permute-start(bf16[8,240,128]{2,1,0:T(8,128)(2,1)S(1)} %pad_maximum_fusion.state), channel_id=1, source_target_pairs={{0,24},{8,0},{16,8},{24,16},{1,25},{9,1},{17,9},{25,17},{2,26},{10... | collective-permute-start | bytes 1474568 | tf_op jit(solution)/shard_map/ppermute | solution.py:27
  58.1 7.1 %all-to-all-done.2 = bf16[32,24,128]{2,1,0:T(8,128)(2,1)S(1)} async-done(((bf16[32,24,128]{2,1,0:T(8,128)(2,1)}), bf16[32,24,128]{2,1,0:T(8,128)(2,1)S(1)}, u32[]{:S(2)}, u32[]{:S(2)}) %all-to-all-start.2) | async-done | bytes 196640 | tf_op jit(solution)/shard_map/all_to_all | solution.py:222
  65.9 4.1 %all-to-all-start.3 = ((bf16[32,24,128]{2,1,0:T(8,128)(2,1)}), bf16[32,24,128]{2,1,0:T(8,128)(2,1)S(1)}, u32[]{:S(2)}, u32[]{:S(2)}) async-start(bf16[32,24,128]{2,1,0:T(8,128)(2,1)} %broadcast_in_dim.7), calls=%async_computation.3 | async-start | bytes 393216 | tf_op jit(solution)/shard_map/all_to_all | solution.py:22
  70.8 3.3 %collective-permute-start.7 = (bf16[4,240,128]{2,1,0:T(8,128)(2,1)}, bf16[4,240,128]{2,1,0:T(8,128)(2,1)}, u32[]{:S(2)}, u32[]{:S(2)}) collective-permute-start(bf16[4,240,128]{2,1,0:T(8,128)(2,1)} %slice.17), channel_id=1, source_target_pairs={{0,24},{8,0},{16,8},{24,16},{1,25},{9,1},{17,9},{25,17},{2,26},{10... | collective-permute-start | bytes 737288 | tf_op jit(solution)/shard_map/ppermute | solution.py:27
  74.1 1.7 %slice.16 = bf16[4,240,128]{2,1,0:T(8,128)(2,1)} slice(bf16[8,240,128]{2,1,0:T(8,128)(2,1)} %collective-permute-done.4.right), slice={[0:4], [0:240], [0:128]} | slice | bytes 491520 | tf_op jit(solution)/shard_map/slice | solution.py:46
  75.8 4.2 %all-to-all-done.3.projected = bf16[32,24,128]{2,1,0:T(8,128)(2,1)S(1)} async-done(((bf16[32,24,128]{2,1,0:T(8,128)(2,1)}), bf16[32,24,128]{2,1,0:T(8,128)(2,1)S(1)}, u32[]{:S(2)}, u32[]{:S(2)}) %all-to-all-start.3) | async-done | bytes 196640 | tf_op jit(solution)/shard_map/all_to_all | solution.py:22
  80.0 0.7 shard_map.103
  80.7 7.3 %all-to-all-start.4 = ((f32[8,8,128]{2,1,0:T(8,128)}), f32[8,8,128]{2,1,0:T(8,128)S(1)}, u32[]{:S(2)}, u32[]{:S(2)}) async-start(f32[8,8,128]{2,1,0:T(8,128)} %shard_map.103), calls=%async_computation.4 | async-start | bytes 65536 | tf_op jit(solution)/shard_map/all_to_all | solution.py:232
  88.0 1.0 %copy-done.2 = bf16[4,8,32,256]{3,2,1,0:T(8,128)(2,1)S(1)} copy-done((bf16[4,8,32,256]{3,2,1,0:T(8,128)(2,1)S(1)}, bf16[4,8,32,256]{3,2,1,0:T(8,128)(2,1)}, u32[]{:S(2)}) %copy-start.2) | copy-done | bytes 524312
  89.7 3.0 %all-to-all-done.4.squares = f32[8,8,128]{2,1,0:T(8,128)S(1)} async-done(((f32[8,8,128]{2,1,0:T(8,128)}), f32[8,8,128]{2,1,0:T(8,128)S(1)}, u32[]{:S(2)}, u32[]{:S(2)}) %all-to-all-start.4) | async-done | bytes 32800 | tf_op jit(solution)/shard_map/all_to_all | solution.py:232
  92.7 1.0 %copy-done.4 = bf16[8,240,128]{2,1,0:T(8,128)(2,1)S(1)} copy-done((bf16[8,240,128]{2,1,0:T(8,128)(2,1)S(1)}, bf16[8,240,128]{2,1,0:T(8,128)(2,1)}, u32[]{:S(2)}) %copy-start.4) | copy-done | bytes 491544
  93.8 1.0 %copy-done.6 = bf16[8,240,128]{2,1,0:T(8,128)(2,1)S(1)} copy-done((bf16[8,240,128]{2,1,0:T(8,128)(2,1)S(1)}, bf16[8,240,128]{2,1,0:T(8,128)(2,1)}, u32[]{:S(2)}) %copy-start.6) | copy-done | bytes 491544
  94.8 3.6 %shard_map.106 = (f32[3,64,128]{2,1,0:T(8,128)}, f32[3,64,128]{2,1,0:T(8,128)}, bf16[3,2048,128]{2,1,0:T(8,128)(2,1)}, f32[3,8,128]{2,1,0:T(8,128)}, f32[3,8,128]{2,1,0:T(8,128)}) custom-call(s32[3]{0:T(128)S(1)} %copy-done.11, f32[8,8,128]{2,1,0:T(8,128)S(1)} %all-to-all-done.4.squares, bf16[32,24,128]{2,1,0:T(8,128)(2,1)S(1)} %all-to-all-done.3.projected, ...), custom_call_target="tpu_custom_call" | custom-call | tf_op jit(solution)/shard_map/pallas_call | solution.py:233
  (38 shorter events, 2.8 us)
Async XLA Ops:
  0.6 28.2 %copy-start = (bf16[3,2048,128]{2,1,0:T(8,128)(2,1)S(1)}, bf16[3,2048,128]{2,1,0:T(8,128)(2,1)}, u32[]{:S(2)}) copy-start(bf16[3,2048,128]{2,1,0:T(8,128)(2,1)} %param.7) | copy-start | bytes 4718596
  2.7 21.1 %all-to-all-start = ((bf16[8,32,256]{2,1,0:T(8,128)(2,1)}), bf16[8,32,256]{2,1,0:T(8,128)(2,1)S(1)}, u32[]{:S(2)}, u32[]{:S(2)}) async-start(bf16[8,32,256]{2,1,0:T(8,128)(2,1)} %shard_map.101), calls=%async_computation | async-start | bytes 262144 | tf_op jit(solution)/shard_map/all_to_all | solution.py:180
  13.2 8.9 %collective-permute-start.1 = (bf16[1,240,128]{2,1,0:T(8,128)(2,1)}, bf16[1,240,128]{2,1,0:T(8,128)(2,1)S(1)}, u32[]{:S(2)}, u32[]{:S(2)}) collective-permute-start(bf16[1,240,128]{2,1,0:T(8,128)(2,1)} %shard_map.104), channel_id=1, source_target_pairs={{0,128},{32,160},{64,192},{96,224},{128,0},{160,32},{192,64},{224,... | collective-permute-start | bytes 184328 | tf_op jit(solution)/shard_map/ppermute | solution.py:32
  22.9 17.5 %collective-permute-start.2 = (bf16[2,240,128]{2,1,0:T(8,128)(2,1)S(1)}, bf16[2,240,128]{2,1,0:T(8,128)(2,1)S(1)}, u32[]{:S(2)}, u32[]{:S(2)}) collective-permute-start(bf16[2,240,128]{2,1,0:T(8,128)(2,1)S(1)} %pad_maximum_fusion.2), channel_id=1, source_target_pairs={{0,64},{32,96},{64,0},{96,32},{128,192},{160,224},{192,128},{224,1... | collective-permute-start | bytes 368648 | tf_op jit(solution)/shard_map/ppermute | solution.py:32
  24.7 11.1 %all-to-all-start.1 = ((bf16[4,8,32,256]{3,2,1,0:T(8,128)(2,1)}), bf16[4,8,32,256]{3,2,1,0:T(8,128)(2,1)S(1)}, u32[]{:S(2)}, u32[]{:S(2)}) async-start(bf16[4,8,32,256]{3,2,1,0:T(8,128)(2,1)} %broadcast_in_dim.6), calls=%async_computation.1 | async-start | bytes 1048576 | tf_op jit(solution)/shard_map/all_to_all | solution.py:22
  28.8 11.6 %copy-start.12 = (bf16[1,240,128]{2,1,0:T(8,128)(2,1)S(1)}, bf16[1,240,128]{2,1,0:T(8,128)(2,1)}, u32[]{:S(2)}) copy-start(bf16[1,240,128]{2,1,0:T(8,128)(2,1)} %shard_map.104) | copy-start | bytes 184324
  35.8 10.6 %collective-permute-start = (bf16[4,8,32,256]{3,2,1,0:T(8,128)(2,1)S(1)}, bf16[4,8,32,256]{3,2,1,0:T(8,128)(2,1)S(1)}, u32[]{:S(2)}, u32[]{:S(2)}) collective-permute-start(bf16[4,8,32,256]{3,2,1,0:T(8,128)(2,1)S(1)} %all-to-all-done.1.mine), channel_id=1, source_target_pairs={{0,1},{1,0},{2,3},{3,2},{4,5},{5,4},{6,7},{7,6},{8,9},{9,8},{10,11... | collective-permute-start | bytes 1572872 | tf_op jit(solution)/shard_map/ppermute | solution.py:27
  41.2 5.2 %copy-start.11 = (s32[3]{0:T(128)S(1)}, s32[3]{0:T(128)}, u32[]{:S(2)}) copy-start(s32[3]{0:T(128)} %pad_add_fusion.place) | copy-start | bytes 40
  41.2 13.4 %collective-permute-start.3 = (bf16[4,240,128]{2,1,0:T(8,128)(2,1)}, bf16[4,240,128]{2,1,0:T(8,128)(2,1)}, u32[]{:S(2)}, u32[]{:S(2)}) collective-permute-start(bf16[4,240,128]{2,1,0:T(8,128)(2,1)} %pad_maximum_fusion.1), channel_id=1, source_target_pairs={{0,32},{32,0},{64,96},{96,64},{128,160},{160,128},{192,224},{224,1... | collective-permute-start | bytes 737288 | tf_op jit(solution)/shard_map/ppermute | solution.py:32
  48.5 0.8 copy-start.1
  49.3 15.9 %all-to-all-start.2 = ((bf16[32,24,128]{2,1,0:T(8,128)(2,1)}), bf16[32,24,128]{2,1,0:T(8,128)(2,1)S(1)}, u32[]{:S(2)}, u32[]{:S(2)}) async-start(bf16[32,24,128]{2,1,0:T(8,128)(2,1)} %shard_map.102), calls=%async_computation.2 | async-start | bytes 393216 | tf_op jit(solution)/shard_map/all_to_all | solution.py:222
  55.5 25.2 %copy-start.3 = (bf16[8,240,128]{2,1,0:T(8,128)(2,1)}, bf16[8,240,128]{2,1,0:T(8,128)(2,1)S(1)}, u32[]{:S(2)}) copy-start(bf16[8,240,128]{2,1,0:T(8,128)(2,1)S(1)} %pad_maximum_fusion.state) | copy-start | bytes 1474564
  55.6 14.5 %collective-permute-start.5 = (bf16[8,240,128]{2,1,0:T(8,128)(2,1)S(1)}, bf16[8,240,128]{2,1,0:T(8,128)(2,1)S(1)}, u32[]{:S(2)}, u32[]{:S(2)}) collective-permute-start(bf16[8,240,128]{2,1,0:T(8,128)(2,1)S(1)} %pad_maximum_fusion.state), channel_id=1, source_target_pairs={{0,24},{8,0},{16,8},{24,16},{1,25},{9,1},{17,9},{25,17},{2,26},{10... | collective-permute-start | bytes 1474568 | tf_op jit(solution)/shard_map/ppermute | solution.py:27
  58.1 16.0 %collective-permute-start.4 = (bf16[8,240,128]{2,1,0:T(8,128)(2,1)S(1)}, bf16[8,240,128]{2,1,0:T(8,128)(2,1)}, u32[]{:S(2)}, u32[]{:S(2)}) collective-permute-start(bf16[8,240,128]{2,1,0:T(8,128)(2,1)S(1)} %pad_maximum_fusion.state), channel_id=1, source_target_pairs={{0,8},{8,16},{16,24},{24,0},{1,9},{9,17},{17,25},{25,1},{2,10},{10... | collective-permute-start | bytes 1474568 | tf_op jit(solution)/shard_map/ppermute | solution.py:27
  65.9 14.1 %all-to-all-start.3 = ((bf16[32,24,128]{2,1,0:T(8,128)(2,1)}), bf16[32,24,128]{2,1,0:T(8,128)(2,1)S(1)}, u32[]{:S(2)}, u32[]{:S(2)}) async-start(bf16[32,24,128]{2,1,0:T(8,128)(2,1)} %broadcast_in_dim.7), calls=%async_computation.3 | async-start | bytes 393216 | tf_op jit(solution)/shard_map/all_to_all | solution.py:22
  70.0 22.7 %copy-start.7 = (f32[3,64,128]{2,1,0:T(8,128)S(1)}, f32[3,64,128]{2,1,0:T(8,128)}, u32[]{:S(2)}) copy-start(f32[3,64,128]{2,1,0:T(8,128)} %weights.3) | copy-start | bytes 294916
  70.0 22.7 %copy-start.8 = (bf16[64,256]{1,0:T(8,128)(2,1)S(1)}, bf16[64,256]{1,0:T(8,128)(2,1)}, u32[]{:S(2)}) copy-start(bf16[64,256]{1,0:T(8,128)(2,1)} %own_factor.1) | copy-start | bytes 98308
  70.0 22.7 %copy-start.9 = (f32[3,8,128]{2,1,0:T(8,128)S(1)}, f32[3,8,128]{2,1,0:T(8,128)}, u32[]{:S(2)}) copy-start(f32[3,8,128]{2,1,0:T(8,128)} %first.3) | copy-start | bytes 36868
  70.1 22.7 %copy-start.10 = (f32[3,8,128]{2,1,0:T(8,128)S(1)}, f32[3,8,128]{2,1,0:T(8,128)}, u32[]{:S(2)}) copy-start(f32[3,8,128]{2,1,0:T(8,128)} %second.3) | copy-start | bytes 36868
  70.1 10.6 %copy-start.5 = (bf16[8,240,128]{2,1,0:T(8,128)(2,1)}, bf16[8,240,128]{2,1,0:T(8,128)(2,1)S(1)}, u32[]{:S(2)}) copy-start(bf16[8,240,128]{2,1,0:T(8,128)(2,1)S(1)} %collective-permute-done.5.left) | copy-start | bytes 1474564
  70.8 18.9 %collective-permute-start.7 = (bf16[4,240,128]{2,1,0:T(8,128)(2,1)}, bf16[4,240,128]{2,1,0:T(8,128)(2,1)}, u32[]{:S(2)}, u32[]{:S(2)}) collective-permute-start(bf16[4,240,128]{2,1,0:T(8,128)(2,1)} %slice.17), channel_id=1, source_target_pairs={{0,24},{8,0},{16,8},{24,16},{1,25},{9,1},{17,9},{25,17},{2,26},{10... | collective-permute-start | bytes 737288 | tf_op jit(solution)/shard_map/ppermute | solution.py:27
  75.8 13.9 %collective-permute-start.6 = (bf16[4,240,128]{2,1,0:T(8,128)(2,1)}, bf16[4,240,128]{2,1,0:T(8,128)(2,1)}, u32[]{:S(2)}, u32[]{:S(2)}) collective-permute-start(bf16[4,240,128]{2,1,0:T(8,128)(2,1)} %slice.16), channel_id=1, source_target_pairs={{0,8},{8,16},{16,24},{24,0},{1,9},{9,17},{17,25},{25,1},{2,10},{10... | collective-permute-start | bytes 737288 | tf_op jit(solution)/shard_map/ppermute | solution.py:27
  80.7 12.0 %all-to-all-start.4 = ((f32[8,8,128]{2,1,0:T(8,128)}), f32[8,8,128]{2,1,0:T(8,128)S(1)}, u32[]{:S(2)}, u32[]{:S(2)}) async-start(f32[8,8,128]{2,1,0:T(8,128)} %shard_map.103), calls=%async_computation.4 | async-start | bytes 65536 | tf_op jit(solution)/shard_map/all_to_all | solution.py:232
  88.0 1.0 %copy-start.2 = (bf16[4,8,32,256]{3,2,1,0:T(8,128)(2,1)S(1)}, bf16[4,8,32,256]{3,2,1,0:T(8,128)(2,1)}, u32[]{:S(2)}) copy-start(bf16[4,8,32,256]{3,2,1,0:T(8,128)(2,1)} %copy-done.1) | copy-start | bytes 1572868
  92.7 1.0 %copy-start.4 = (bf16[8,240,128]{2,1,0:T(8,128)(2,1)S(1)}, bf16[8,240,128]{2,1,0:T(8,128)(2,1)}, u32[]{:S(2)}) copy-start(bf16[8,240,128]{2,1,0:T(8,128)(2,1)} %copy-done.3) | copy-start | bytes 1474564
  93.8 1.0 %copy-start.6 = (bf16[8,240,128]{2,1,0:T(8,128)(2,1)S(1)}, bf16[8,240,128]{2,1,0:T(8,128)(2,1)}, u32[]{:S(2)}) copy-start(bf16[8,240,128]{2,1,0:T(8,128)(2,1)} %copy-done.5) | copy-start | bytes 1474564

commit v5 on v4

--- a/solution.py
+++ b/solution.py
@@ -12,6 +12,8 @@
 FS = ("fs_0", "fs_1")
 TP = ("tp_0", "tp_1")
 CORE = "tp_1"
+AWAY = (0, 7, 6, 5, 2, 1, 4, 3)
+CUT = 1024
 BF = jnp.bfloat16
 F32 = jnp.float32
 VMEM = pl.BlockSpec(memory_space=pltpu.VMEM)
@@ -27,15 +29,11 @@
     return lax.ppermute(array, axis, [(i, (i + shift) % size) for i in range(size)])
 
 
-def swapped(array, axis, bit):
-    size = lax.axis_size(axis)
-    return lax.ppermute(array, axis, [(i, i ^ bit) for i in range(size)])
-
-
 def gathered_z(array):
-    for bit in (4, 2, 1):
-        array = jnp.concatenate([array, swapped(array, Z, bit)])
-    return array
+    pair = jnp.concatenate([array, moved(array, Z, 1)])
+    below = moved(pair, Z, 2)
+    above = moved(pair, Z, -2)
+    return jnp.concatenate([pair, below, above, moved(above, Z, -2)])
 
 
 def gathered_y(array):
@@ -58,23 +56,41 @@
     out[0, 192:] = moments.astype(BF)
 
 
-def assemble(place, mine, other, factor):
+def partial_kernel(
+    place, gradient, cotangents, inputs, mine, other,
+    out, factor_out, factor, held, seen, turned, mapped, sems, factor_sem,
+):
+    copies = [
+        pltpu.make_async_copy(
+            inputs.at[pl.ds(n * 512, 512), pl.ds(CUT, 2048 - CUT)], held.at[n], sems.at[n]
+        )
+        for n in range(4)
+    ]
+    copies += [
+        pltpu.make_async_copy(cotangents.at[m], seen.at[m], sems.at[4 + m]) for m in range(3)
+    ]
+    for copy in copies[4:] + copies[:4]:
+        copy.start()
     for z in range(8):
         for y in range(4):
             row = z * 256 + y * 64
             factor[pl.ds(row + pl.multiple_of(place[2] * 32, 32), 32)] = mine[y, z]
             factor[pl.ds(row + pl.multiple_of(32 - place[2] * 32, 32), 32)] = other[y, z]
-
-
-def partial_kernel(place, gradient_a, gradient_b, mine, other, out, factor, held, sem):
-    copy = pltpu.make_async_copy(gradient_b, held, sem)
-    copy.start()
-    assemble(place, mine, other, factor)
-    projected = jnp.dot(gradient_a[...], factor[:1024], preferred_element_type=F32)
-    copy.wait()
-    projected += jnp.dot(held[...], factor[1024:], preferred_element_type=F32)
+    factor_copy = pltpu.make_async_copy(factor, factor_out, factor_sem)
+    factor_copy.start()
+    projected = jnp.dot(gradient[...], factor[:CUT], preferred_element_type=F32)
+    for m in range(3):
+        copies[4 + m].wait()
+        turned[m * 128 : (m + 1) * 128] = seen[m].T
+    for n in range(4):
+        copies[n].wait()
+        mapped[n * 512 : (n + 1) * 512] = jnp.dot(
+            held[n], factor[CUT:], preferred_element_type=F32
+        ).astype(BF)
+    projected += jnp.dot(turned[...], mapped[...], preferred_element_type=F32)
     rows = [projected[m * 128 : (m + 1) * 128].T.reshape(32, 8, 128) for m in range(3)]
     out[...] = jnp.concatenate(rows, axis=1).astype(BF)
+    factor_copy.wait()
 
 
 def square_kernel(projected, out):
@@ -101,7 +117,7 @@
 
     def blocks_of(j):
         across = across_a.at[j] if j < 4 else across_b.at[j - 4]
-        z = place[0] ^ (j // 4 + (j // 2 % 2) * 2 + (j % 2) * 4)
+        z = (place[0] + AWAY[j]) % 8
         return [
             (z * 4 + (place[1] + 4 - i) % 4, block)
             for i, block in enumerate((state.at[j], right.at[j], across, left.at[j]))
@@ -144,24 +160,26 @@
     for copy in sent:
         copy.start()
     for q in range(4):
-        base = pl.multiple_of(blocks[q][0][0] // 8 * 512, 512)
+        places = [(place[0] + AWAY[2 * q + k]) % 8 * 256 for k in range(2)]
+        chunks = [factor[pl.ds(pl.multiple_of(at, 256), 256)] for at in places]
         change[q % 2] = jnp.dot(
-            factor[pl.ds(base, 512)], values, preferred_element_type=F32
-        )
-        for at, block in blocks[q] + blocks[q + 4]:
-            rows = pl.ds(pl.multiple_of(at * 64, 64), 64)
-            inner = pl.ds(pl.multiple_of(at * 64 - base, 64), 64)
+            jnp.concatenate(chunks), values, preferred_element_type=F32
+        )
+        for k in range(2):
+            for at, block in blocks[2 * q + k]:
+                rows = pl.ds(pl.multiple_of(at * 64, 64), 64)
+                inner = pl.ds(pl.multiple_of(k * 256 + at % 4 * 64, 64), 64)
+                for m in range(3):
+                    before = block[m * 64 : (m + 1) * 64].astype(F32)
+                    part = change[q % 2, inner, m * 128 : (m + 1) * 128]
+                    copies[m, rows] = (before - 0.02 * part).astype(BF)
+            rows = pl.ds(pl.multiple_of(places[k], 256), 256)
             for m in range(3):
-                before = block[m * 64 : (m + 1) * 64].astype(F32)
-                part = change[q % 2, inner, m * 128 : (m + 1) * 128]
-                copies[m, rows] = (before - 0.02 * part).astype(BF)
-        for m in range(3):
-            rows = pl.ds(base, 512)
-            copy = pltpu.make_async_copy(
-                copies.at[m, rows], copies_out.at[m, rows], sems.at[q, m]
-            )
-            copy.start()
-            sent.append(copy)
+                copy = pltpu.make_async_copy(
+                    copies.at[m, rows], copies_out.at[m, rows], sems.at[2 * q + k, m]
+                )
+                copy.start()
+                sent.append(copy)
     for copy in sent:
         copy.wait()
 
@@ -191,34 +209,27 @@
     states = gathered_y(state_z)
 
 
-    def gradient_of(part):
-        return (
-            jnp.einsum("mtc,td->mcd", cotangents, part, preferred_element_type=F32)
-            .astype(BF)
-            .reshape(384, -1)
-        )
-
-    gradient_a = gradient_of(inputs[:, :1024])
-    gradient_b = gradient_of(inputs[:, 1024:])
-    partial_value = pl.pallas_call(
+    gradient = (
+        jnp.einsum("mtc,td->mcd", cotangents, inputs[:, :CUT], preferred_element_type=F32)
+        .astype(BF)
+        .reshape(384, CUT)
+    )
+    partial_value, factor_all = pl.pallas_call(
         partial_kernel,
-        out_shape=jax.ShapeDtypeStruct((32, 24, 128), BF),
-        in_specs=[smem, VMEM, hbm, VMEM, VMEM],
-        out_specs=VMEM,
+        out_shape=(jax.ShapeDtypeStruct((32, 24, 128), BF), jax.ShapeDtypeStruct((2048, RANK), BF)),
+        in_specs=[smem, VMEM, hbm, hbm, VMEM, VMEM],
+        out_specs=(VMEM, hbm),
         scratch_shapes=[
             pltpu.VMEM((2048, RANK), BF),
-            pltpu.VMEM((384, 1024), BF),
+            pltpu.VMEM((4, 512, 2048 - CUT), BF),
+            pltpu.VMEM((3, 2048, 128), BF),
+            pltpu.VMEM((384, 2048), BF),
+            pltpu.VMEM((2048, RANK), BF),
+            pltpu.SemaphoreType.DMA((7,)),
             pltpu.SemaphoreType.DMA,
         ],
-        compiler_params=pltpu.CompilerParams(vmem_limit_bytes=12 << 20),
-    )(place, gradient_a, gradient_b, half, other_half)
-    factor_all = pl.pallas_call(
-        assemble,
-        out_shape=jax.ShapeDtypeStruct((2048, RANK), BF),
-        in_specs=[smem] + [VMEM] * 2,
-        out_specs=VMEM,
-        compiler_params=pltpu.CompilerParams(vmem_limit_bytes=8 << 20),
-    )(place, half, other_half)
+        compiler_params=pltpu.CompilerParams(vmem_limit_bytes=50 << 20),
+    )(place, gradient, cotangents, inputs, half, other_half)
     arrived = lax.all_to_all(partial_value, FS, split_axis=0, concat_axis=0, tiled=True)
     projected = arrived.astype(F32).sum(axis=0)
     projected_all = sent_to_all(projected.astype(BF), FS)
@@ -250,7 +261,7 @@
             pltpu.VMEM((RANK, 384), F32),
             pltpu.VMEM((2, 512, 384), F32),
             pltpu.SemaphoreType.DMA((4,)),
-            pltpu.SemaphoreType.DMA((4, 3)),
+            pltpu.SemaphoreType.DMA((8, 3)),
         ],
         compiler_params=pltpu.CompilerParams(vmem_limit_bytes=24 << 20),
     )(

time: 99.2 us -> 104 us (1.048)
  blocking collectives: 0 us -> 16.8 us
  starting transfers between devices: 47.7 us -> 34.7 us
  waiting for transfers between devices: 20.8 us -> 29.3 us
  local copies, waits for them, and re-layouts: 7.86 us -> 3.08 us
  matrix products: 7.99 us -> 4.47 us
  Pallas kernels: 10 us -> 13.3 us
  other arithmetic: 3.19 us -> 0.65 us
    all_to_all x0 -> x1, blocking collectives: none -> 16.8 us  [step(): half = lax.all_to_all(half, Z, split_axis=0, concat_axis=0, tiled=True)]
    all_to_all x1 -> x0, starting transfers between devices: 9 us -> none  [step(): half = lax.all_to_all(half, Z, split_axis=0, concat_axis=0, tiled=True)]
    ppermute x3 -> x0, starting transfers between devices: 7.43 us -> none  [swapped(): return lax.ppermute(array, axis, [(i, i ^ bit) for i in range(size)])]
    ppermute x5 -> x9, waiting for transfers between devices: 0.01 us -> 6.41 us  [moved(): lax.ppermute(array, axis, [(i, (i + shift) % size) for i in range(size)])]
    unnamed x26 -> x16, local copies, waits for them, and re-layouts: 3.93 us -> 0.09 us
    all_to_all x2, waiting for transfers between devices: 7.16 us -> 10.9 us  [sent_to_all(): return lax.all_to_all(copies, axis, split_axis=0, concat_axis=0, tiled=True)]
    pallas_call x2 -> x1, Pallas kernels: 2.72 us -> 6.47 us  [step(): pl.pallas_call(partial_kernel, out_shape=(jax.ShapeDtypeStruct((32, 24, 1...]
    dot_general x2 -> x1, matrix products: 7.99 us -> 4.47 us  [step(): jnp.einsum('mtc,td->mcd', cotangents, inputs[:, :CUT], preferred_element_...]
  transfers between devices with their start and end apart: 13 -> 13, of which waited for: 5 -> 5; matrix products, arithmetic and copies ran while one was open for 15% -> 7% of each run, Pallas kernels for 5% -> 8%
where the time goes in v5:
time: 104 us; the launch traced here: 103 us
  starting transfers between devices  34.7 us (33%)
  waiting for transfers between devices  29.3 us (28%)
  blocking collectives  16.8 us (16%)
  Pallas kernels  13.3 us (13%)
  matrix products  4.47 us (4%)
  local copies, waits for them, and re-layouts  3.08 us (3%)
    all_to_all x1, blocking collectives, step(): half = lax.all_to_all(half, Z, split_axis=0, concat_axis=0, tiled=True)  16.8 us
    ppermute x9, starting transfers between devices, moved(): lax.ppermute(array, axis, [(i, (i + shift) % size) for i in range(size)])  13.3 us
    all_to_all x2, waiting for transfers between devices, sent_to_all(): return lax.all_to_all(copies, axis, split_axis=0, concat_axis=0, tiled=True)  10.9 us
    all_to_all x2, starting transfers between devices, sent_to_all(): return lax.all_to_all(copies, axis, split_axis=0, concat_axis=0, tiled=True)  8.79 us
    all_to_all x1, starting transfers between devices, step(): lax.all_to_all(squares, TP, split_axis=0, concat_axis=0, tiled=True)  7.59 us
    all_to_all x1, waiting for transfers between devices, step(): lax.all_to_all(partial_value, FS, split_axis=0, concat_axis=0, tiled=True)  7.29 us
    pallas_call x1, Pallas kernels, step(): pl.pallas_call(partial_kernel, out_shape=(jax.ShapeDtypeStruct((32, 24, 1...  6.47 us
    ppermute x9, waiting for transfers between devices, moved(): lax.ppermute(array, axis, [(i, (i + shift) % size) for i in range(size)])  6.41 us
  transfers between devices with their start and end apart: 13, of which 5 were waited for; matrix products, arithmetic and copies ran while one was open for 7% of the time, Pallas kernels for 8%

profile of v5, /device:TPU:1, one launch (start us, length us, event | category | flops | bytes accessed | tf_op | source)
XLA Modules:
  0.0 103.0 jit_solution(1066526084579908066)
XLA Ops:
  0.6 0.6 pad_add_fusion.place
  1.2 1.4 %shard_map.101 = bf16[8,32,256]{2,1,0:T(8,128)(2,1)} custom-call(s32[3]{0:T(128)} %pad_add_fusion.place, bf16[64,256]{1,0:T(8,128)(2,1)} %own_factor.1), custom_call_target="tpu_custom_call" | custom-call | tf_op jit(solution)/shard_map/pallas_call | solution.py:191
  2.7 16.8 %all_to_all.25 = bf16[8,32,256]{2,1,0:T(8,128)(2,1)S(1)} all-to-all(bf16[8,32,256]{2,1,0:T(8,128)(2,1)} %shard_map.101), channel_id=1, replica_groups=mesh['fs_0'=8,'fs_1'=4,'tp_0'=4,'tp_1'=2] {'fs_0'}, dimensions={0} | all-to-all | bytes 262144 | tf_op jit(solution)/shard_map/all_to_all | solution.py:198
  19.4 0.9 broadcast_in_dim.6
  20.3 4.2 %all-to-all-start.1 = ((bf16[4,8,32,256]{3,2,1,0:T(8,128)(2,1)}), bf16[4,8,32,256]{3,2,1,0:T(8,128)(2,1)S(1)}, u32[]{:S(2)}, u32[]{:S(2)}) async-start(bf16[4,8,32,256]{3,2,1,0:T(8,128)(2,1)} %broadcast_in_dim.6), calls=%async_computation.1 | async-start | bytes 1048576 | tf_op jit(solution)/shard_map/all_to_all | solution.py:24
  24.4 1.5 %shard_map.104 = bf16[1,240,128]{2,1,0:T(8,128)(2,1)} custom-call(f32[3,64,128]{2,1,0:T(8,128)} %weights.3, f32[3,8,128]{2,1,0:T(8,128)} %first.3, f32[3,8,128]{2,1,0:T(8,128)} %second.3), custom_call_target="tpu_custom_call" | custom-call | tf_op jit(solution)/shard_map/pallas_call | solution.py:201
  26.0 0.5 collective-permute-start.1
  26.5 4.9 %all-to-all-done.1.mine = bf16[4,8,32,256]{3,2,1,0:T(8,128)(2,1)S(1)} async-done(((bf16[4,8,32,256]{3,2,1,0:T(8,128)(2,1)}), bf16[4,8,32,256]{3,2,1,0:T(8,128)(2,1)S(1)}, u32[]{:S(2)}, u32[]{:S(2)}) %all-to-all-start.1) | async-done | bytes 524320 | tf_op jit(solution)/shard_map/all_to_all | solution.py:24
  31.4 3.7 %collective-permute-start = (bf16[4,8,32,256]{3,2,1,0:T(8,128)(2,1)S(1)}, bf16[4,8,32,256]{3,2,1,0:T(8,128)(2,1)S(1)}, u32[]{:S(2)}, u32[]{:S(2)}) collective-permute-start(bf16[4,8,32,256]{3,2,1,0:T(8,128)(2,1)S(1)} %all-to-all-done.1.mine), channel_id=1, source_target_pairs={{0,1},{1,0},{2,3},{3,2},{4,5},{5,4},{6,7},{7,6},{8,9},{9,8},{10,11... | collective-permute-start | bytes 1572872 | tf_op jit(solution)/shard_map/ppermute | solution.py:29
  35.1 4.5 %fusion.3 = bf16[3,128,1024]{2,1,0:T(8,128)(2,1)S(1)} fusion(bf16[3,2048,128]{2,1,0:T(8,128)(2,1)} %cotangents.1, bf16[2048,2048]{1,0:T(8,128)(2,1)} %inputs.1), kind=kOutput, calls=%fused_computation.3 | convolution fusion | flops 1611005952 | bytes 6553600 | tf_op jit(solution)/shard_map/mtc,td->mcd/dot_general | solution.py:213
  39.6 0.9 collective-permute-start.3
  40.5 1.6 %collective-permute-start.2 = (bf16[2,240,128]{2,1,0:T(8,128)(2,1)S(1)}, bf16[2,240,128]{2,1,0:T(8,128)(2,1)S(1)}, u32[]{:S(2)}, u32[]{:S(2)}) collective-permute-start(bf16[2,240,128]{2,1,0:T(8,128)(2,1)S(1)} %pad_maximum_fusion), channel_id=1, source_target_pairs={{0,64},{32,96},{64,128},{96,160},{128,192},{160,224},{192,0},{224,... | collective-permute-start | bytes 368648 | tf_op jit(solution)/shard_map/ppermute | solution.py:29
  42.1 6.4 %collective-permute-done.3 = bf16[2,240,128]{2,1,0:T(8,128)(2,1)S(1)} collective-permute-done((bf16[2,240,128]{2,1,0:T(8,128)(2,1)S(1)}, bf16[2,240,128]{2,1,0:T(8,128)(2,1)S(1)}, u32[]{:S(2)}, u32[]{:S(2)}) %collective-permute-start.3) | collective-permute-done | bytes 122912 | tf_op jit(solution)/shard_map/ppermute | solution.py:29
  48.5 1.7 %collective-permute-start.4 = (bf16[2,240,128]{2,1,0:T(8,128)(2,1)S(1)}, bf16[2,240,128]{2,1,0:T(8,128)(2,1)S(1)}, u32[]{:S(2)}, u32[]{:S(2)}) collective-permute-start(bf16[2,240,128]{2,1,0:T(8,128)(2,1)S(1)} %collective-permute-done.3), channel_id=1, source_target_pairs={{0,192},{32,224},{64,0},{96,32},{128,64},{160,96},{192,128},{224,1... | collective-permute-start | bytes 368648 | tf_op jit(solution)/shard_map/ppermute | solution.py:29
  50.3 6.5 %shard_map.102 = (bf16[32,24,128]{2,1,0:T(8,128)(2,1)}, bf16[2048,256]{1,0:T(8,128)(2,1)S(1)}) custom-call(s32[3]{0:T(128)S(1)} %copy-done.4, bf16[384,1024]{1,0:T(8,128)(2,1)S(1)} %bitcast.10, bf16[3,2048,128]{2,1,0:T(8,128)(2,1)} %cotangents.1, bf16[2048,2048]{1,0:T(8,128)(2,1)} %inputs.1, bf16[4,8,32,256]{3,2,1,0:T(8,128)(2,1)S(1)} %all-to-all-done.1.mine, ...), custom_call_target="tpu_custom_call" | custom-call | tf_op jit(solution)/shard_map/pallas_call | solution.py:217
  56.7 0.0 copy-start
  56.7 0.0 copy-start.1
  56.8 0.0 copy-start.2
  56.8 0.0 copy-start.3
  56.8 5.0 %all-to-all-start.2 = ((bf16[32,24,128]{2,1,0:T(8,128)(2,1)}), bf16[32,24,128]{2,1,0:T(8,128)(2,1)S(1)}, u32[]{:S(2)}, u32[]{:S(2)}) async-start(bf16[32,24,128]{2,1,0:T(8,128)(2,1)} %get-tuple-element.7), calls=%async_computation.2 | async-start | bytes 393216 | tf_op jit(solution)/shard_map/all_to_all | solution.py:233
  61.8 2.5 %collective-permute-start.6 = (bf16[8,240,128]{2,1,0:T(8,128)(2,1)S(1)}, bf16[8,240,128]{2,1,0:T(8,128)(2,1)S(1)}, u32[]{:S(2)}, u32[]{:S(2)}) collective-permute-start(bf16[8,240,128]{2,1,0:T(8,128)(2,1)S(1)} %constant_dynamic-update-slice_fusion.state), channel_id=1, source_target_pairs={{0,24},{8,0},{16,8},{24,16},{1,25},{9,1},{17,9},{25,17},{2,26},{10... | collective-permute-start | bytes 1474568 | tf_op jit(solution)/shard_map/ppermute | solution.py:29
  64.3 7.3 %all-to-all-done.2 = bf16[32,24,128]{2,1,0:T(8,128)(2,1)S(1)} async-done(((bf16[32,24,128]{2,1,0:T(8,128)(2,1)}), bf16[32,24,128]{2,1,0:T(8,128)(2,1)S(1)}, u32[]{:S(2)}, u32[]{:S(2)}) %all-to-all-start.2) | async-done | bytes 196640 | tf_op jit(solution)/shard_map/all_to_all | solution.py:233
  71.7 0.7 broadcast_in_dim.7
  72.4 4.6 %all-to-all-start.3 = ((bf16[32,24,128]{2,1,0:T(8,128)(2,1)}), bf16[32,24,128]{2,1,0:T(8,128)(2,1)S(1)}, u32[]{:S(2)}, u32[]{:S(2)}) async-start(bf16[32,24,128]{2,1,0:T(8,128)(2,1)} %broadcast_in_dim.7), calls=%async_computation.3 | async-start | bytes 393216 | tf_op jit(solution)/shard_map/all_to_all | solution.py:24
  77.0 0.7 slice.13
  77.7 2.4 %collective-permute-start.8 = (bf16[4,240,128]{2,1,0:T(8,128)(2,1)}, bf16[4,240,128]{2,1,0:T(8,128)(2,1)S(1)}, u32[]{:S(2)}, u32[]{:S(2)}) collective-permute-start(bf16[4,240,128]{2,1,0:T(8,128)(2,1)} %slice.13), channel_id=1, source_target_pairs={{0,24},{8,0},{16,8},{24,16},{1,25},{9,1},{17,9},{25,17},{2,26},{10... | collective-permute-start | bytes 737288 | tf_op jit(solution)/shard_map/ppermute | solution.py:29
  80.2 0.7 slice.12
  80.9 6.0 %all-to-all-done.3.projected = bf16[32,24,128]{2,1,0:T(8,128)(2,1)S(1)} async-done(((bf16[32,24,128]{2,1,0:T(8,128)(2,1)}), bf16[32,24,128]{2,1,0:T(8,128)(2,1)S(1)}, u32[]{:S(2)}, u32[]{:S(2)}) %all-to-all-start.3) | async-done | bytes 196640 | tf_op jit(solution)/shard_map/all_to_all | solution.py:24
  86.9 0.7 shard_map.103
  87.6 7.6 %all-to-all-start.4 = ((f32[8,8,128]{2,1,0:T(8,128)}), f32[8,8,128]{2,1,0:T(8,128)S(1)}, u32[]{:S(2)}, u32[]{:S(2)}) async-start(f32[8,8,128]{2,1,0:T(8,128)} %shard_map.103), calls=%async_computation.4 | async-start | bytes 65536 | tf_op jit(solution)/shard_map/all_to_all | solution.py:243
  95.2 4.7 %all-to-all-done.4.squares = f32[8,8,128]{2,1,0:T(8,128)S(1)} async-done(((f32[8,8,128]{2,1,0:T(8,128)}), f32[8,8,128]{2,1,0:T(8,128)S(1)}, u32[]{:S(2)}, u32[]{:S(2)}) %all-to-all-start.4) | async-done | bytes 32800 | tf_op jit(solution)/shard_map/all_to_all | solution.py:243
  99.9 3.1 %shard_map.105 = (f32[3,64,128]{2,1,0:T(8,128)}, f32[3,64,128]{2,1,0:T(8,128)}, bf16[3,2048,128]{2,1,0:T(8,128)(2,1)}, f32[3,8,128]{2,1,0:T(8,128)}, f32[3,8,128]{2,1,0:T(8,128)}) custom-call(s32[3]{0:T(128)S(1)} %copy-done.4, f32[8,8,128]{2,1,0:T(8,128)S(1)} %all-to-all-done.4.squares, bf16[32,24,128]{2,1,0:T(8,128)(2,1)S(1)} %all-to-all-done.3.projected, ...), custom_call_target="tpu_custom_call" | custom-call | tf_op jit(solution)/shard_map/pallas_call | solution.py:244
  (26 shorter events, 0.2 us)
Async XLA Ops:
  20.3 11.1 %all-to-all-start.1 = ((bf16[4,8,32,256]{3,2,1,0:T(8,128)(2,1)}), bf16[4,8,32,256]{3,2,1,0:T(8,128)(2,1)S(1)}, u32[]{:S(2)}, u32[]{:S(2)}) async-start(bf16[4,8,32,256]{3,2,1,0:T(8,128)(2,1)} %broadcast_in_dim.6), calls=%async_computation.1 | async-start | bytes 1048576 | tf_op jit(solution)/shard_map/all_to_all | solution.py:24
  26.0 13.6 %copy-start.5 = (bf16[1,240,128]{2,1,0:T(8,128)(2,1)S(1)}, bf16[1,240,128]{2,1,0:T(8,128)(2,1)}, u32[]{:S(2)}) copy-start(bf16[1,240,128]{2,1,0:T(8,128)(2,1)} %shard_map.104) | copy-start | bytes 184324
  26.0 24.3 %copy-start.4 = (s32[3]{0:T(128)S(1)}, s32[3]{0:T(128)}, u32[]{:S(2)}) copy-start(s32[3]{0:T(128)} %pad_add_fusion.place) | copy-start | bytes 40
  26.0 13.6 %collective-permute-start.1 = (bf16[1,240,128]{2,1,0:T(8,128)(2,1)}, bf16[1,240,128]{2,1,0:T(8,128)(2,1)S(1)}, u32[]{:S(2)}, u32[]{:S(2)}) collective-permute-start(bf16[1,240,128]{2,1,0:T(8,128)(2,1)} %shard_map.104), channel_id=1, source_target_pairs={{0,32},{32,64},{64,96},{96,128},{128,160},{160,192},{192,224},{224... | collective-permute-start | bytes 184328 | tf_op jit(solution)/shard_map/ppermute | solution.py:29
  31.4 18.8 %collective-permute-start = (bf16[4,8,32,256]{3,2,1,0:T(8,128)(2,1)S(1)}, bf16[4,8,32,256]{3,2,1,0:T(8,128)(2,1)S(1)}, u32[]{:S(2)}, u32[]{:S(2)}) collective-permute-start(bf16[4,8,32,256]{3,2,1,0:T(8,128)(2,1)S(1)} %all-to-all-done.1.mine), channel_id=1, source_target_pairs={{0,1},{1,0},{2,3},{3,2},{4,5},{5,4},{6,7},{7,6},{8,9},{9,8},{10,11... | collective-permute-start | bytes 1572872 | tf_op jit(solution)/shard_map/ppermute | solution.py:29
  39.6 8.9 %collective-permute-start.3 = (bf16[2,240,128]{2,1,0:T(8,128)(2,1)S(1)}, bf16[2,240,128]{2,1,0:T(8,128)(2,1)S(1)}, u32[]{:S(2)}, u32[]{:S(2)}) collective-permute-start(bf16[2,240,128]{2,1,0:T(8,128)(2,1)S(1)} %pad_maximum_fusion), channel_id=1, source_target_pairs={{0,192},{32,224},{64,0},{96,32},{128,64},{160,96},{192,128},{224,1... | collective-permute-start | bytes 368648 | tf_op jit(solution)/shard_map/ppermute | solution.py:29
  40.5 9.7 %collective-permute-start.2 = (bf16[2,240,128]{2,1,0:T(8,128)(2,1)S(1)}, bf16[2,240,128]{2,1,0:T(8,128)(2,1)S(1)}, u32[]{:S(2)}, u32[]{:S(2)}) collective-permute-start(bf16[2,240,128]{2,1,0:T(8,128)(2,1)S(1)} %pad_maximum_fusion), channel_id=1, source_target_pairs={{0,64},{32,96},{64,128},{96,160},{128,192},{160,224},{192,0},{224,... | collective-permute-start | bytes 368648 | tf_op jit(solution)/shard_map/ppermute | solution.py:29
  48.5 13.3 %collective-permute-start.4 = (bf16[2,240,128]{2,1,0:T(8,128)(2,1)S(1)}, bf16[2,240,128]{2,1,0:T(8,128)(2,1)S(1)}, u32[]{:S(2)}, u32[]{:S(2)}) collective-permute-start(bf16[2,240,128]{2,1,0:T(8,128)(2,1)S(1)} %collective-permute-done.3), channel_id=1, source_target_pairs={{0,192},{32,224},{64,0},{96,32},{128,64},{160,96},{192,128},{224,1... | collective-permute-start | bytes 368648 | tf_op jit(solution)/shard_map/ppermute | solution.py:29
  56.7 43.2 %copy-start = (f32[3,64,128]{2,1,0:T(8,128)S(1)}, f32[3,64,128]{2,1,0:T(8,128)}, u32[]{:S(2)}) copy-start(f32[3,64,128]{2,1,0:T(8,128)} %weights.3) | copy-start | bytes 294916
  56.7 43.2 %copy-start.1 = (bf16[64,256]{1,0:T(8,128)(2,1)S(1)}, bf16[64,256]{1,0:T(8,128)(2,1)}, u32[]{:S(2)}) copy-start(bf16[64,256]{1,0:T(8,128)(2,1)} %own_factor.1) | copy-start | bytes 98308
  56.8 43.2 %copy-start.2 = (f32[3,8,128]{2,1,0:T(8,128)S(1)}, f32[3,8,128]{2,1,0:T(8,128)}, u32[]{:S(2)}) copy-start(f32[3,8,128]{2,1,0:T(8,128)} %first.3) | copy-start | bytes 36868
  56.8 43.1 %copy-start.3 = (f32[3,8,128]{2,1,0:T(8,128)S(1)}, f32[3,8,128]{2,1,0:T(8,128)}, u32[]{:S(2)}) copy-start(f32[3,8,128]{2,1,0:T(8,128)} %second.3) | copy-start | bytes 36868
  56.8 14.8 %all-to-all-start.2 = ((bf16[32,24,128]{2,1,0:T(8,128)(2,1)}), bf16[32,24,128]{2,1,0:T(8,128)(2,1)S(1)}, u32[]{:S(2)}, u32[]{:S(2)}) async-start(bf16[32,24,128]{2,1,0:T(8,128)(2,1)} %get-tuple-element.7), calls=%async_computation.2 | async-start | bytes 393216 | tf_op jit(solution)/shard_map/all_to_all | solution.py:233
  61.8 15.2 %collective-permute-start.6 = (bf16[8,240,128]{2,1,0:T(8,128)(2,1)S(1)}, bf16[8,240,128]{2,1,0:T(8,128)(2,1)S(1)}, u32[]{:S(2)}, u32[]{:S(2)}) collective-permute-start(bf16[8,240,128]{2,1,0:T(8,128)(2,1)S(1)} %constant_dynamic-update-slice_fusion.state), channel_id=1, source_target_pairs={{0,24},{8,0},{16,8},{24,16},{1,25},{9,1},{17,9},{25,17},{2,26},{10... | collective-permute-start | bytes 1474568 | tf_op jit(solution)/shard_map/ppermute | solution.py:29
  64.3 15.8 %collective-permute-start.5 = (bf16[8,240,128]{2,1,0:T(8,128)(2,1)S(1)}, bf16[8,240,128]{2,1,0:T(8,128)(2,1)S(1)}, u32[]{:S(2)}, u32[]{:S(2)}) collective-permute-start(bf16[8,240,128]{2,1,0:T(8,128)(2,1)S(1)} %constant_dynamic-update-slice_fusion.state), channel_id=1, source_target_pairs={{0,8},{8,16},{16,24},{24,0},{1,9},{9,17},{17,25},{25,1},{2,10},{10... | collective-permute-start | bytes 1474568 | tf_op jit(solution)/shard_map/ppermute | solution.py:29
  72.4 14.5 %all-to-all-start.3 = ((bf16[32,24,128]{2,1,0:T(8,128)(2,1)}), bf16[32,24,128]{2,1,0:T(8,128)(2,1)S(1)}, u32[]{:S(2)}, u32[]{:S(2)}) async-start(bf16[32,24,128]{2,1,0:T(8,128)(2,1)} %broadcast_in_dim.7), calls=%async_computation.3 | async-start | bytes 393216 | tf_op jit(solution)/shard_map/all_to_all | solution.py:24
  77.7 17.5 %collective-permute-start.8 = (bf16[4,240,128]{2,1,0:T(8,128)(2,1)}, bf16[4,240,128]{2,1,0:T(8,128)(2,1)S(1)}, u32[]{:S(2)}, u32[]{:S(2)}) collective-permute-start(bf16[4,240,128]{2,1,0:T(8,128)(2,1)} %slice.13), channel_id=1, source_target_pairs={{0,24},{8,0},{16,8},{24,16},{1,25},{9,1},{17,9},{25,17},{2,26},{10... | collective-permute-start | bytes 737288 | tf_op jit(solution)/shard_map/ppermute | solution.py:29
  80.9 14.3 %collective-permute-start.7 = (bf16[4,240,128]{2,1,0:T(8,128)(2,1)}, bf16[4,240,128]{2,1,0:T(8,128)(2,1)S(1)}, u32[]{:S(2)}, u32[]{:S(2)}) collective-permute-start(bf16[4,240,128]{2,1,0:T(8,128)(2,1)} %slice.12), channel_id=1, source_target_pairs={{0,8},{8,16},{16,24},{24,0},{1,9},{9,17},{17,25},{25,1},{2,10},{10... | collective-permute-start | bytes 737288 | tf_op jit(solution)/shard_map/ppermute | solution.py:29
  87.6 12.3 %all-to-all-start.4 = ((f32[8,8,128]{2,1,0:T(8,128)}), f32[8,8,128]{2,1,0:T(8,128)S(1)}, u32[]{:S(2)}, u32[]{:S(2)}) async-start(f32[8,8,128]{2,1,0:T(8,128)} %shard_map.103), calls=%async_computation.4 | async-start | bytes 65536 | tf_op jit(solution)/shard_map/all_to_all | solution.py:243

commit v6 on v5

--- a/solution.py
+++ b/solution.py
@@ -45,52 +45,38 @@
     )
 
 
-def spread_kernel(place, factor, out):
-    rows = factor[pl.ds(pl.multiple_of(place[2] * 32, 32), 32)]
-    out[...] = jnp.broadcast_to(rows, out.shape)
-
-
-def state_kernel(weights, first, second, out):
-    out[0, :192] = weights[...].reshape(192, 128).astype(BF)
+def head_kernel(factor, weights, first, second, half, state):
+    rows = factor[pl.ds(pl.multiple_of(lax.axis_index(CORE) * 32, 32), 32)]
+    half[...] = jnp.broadcast_to(rows, half.shape)
+    state[0, :192] = weights[...].reshape(192, 128).astype(BF)
     moments = jnp.concatenate([first[...].reshape(24, 128), second[...].reshape(24, 128)])
-    out[0, 192:] = moments.astype(BF)
+    state[0, 192:] = moments.astype(BF)
 
 
 def partial_kernel(
-    place, gradient, cotangents, inputs, mine, other,
-    out, factor_out, factor, held, seen, turned, mapped, sems, factor_sem,
+    gradient_a, gradient_b, mine, other, out, factor_out, factor, held_a, held_b, sems
 ):
     copies = [
-        pltpu.make_async_copy(
-            inputs.at[pl.ds(n * 512, 512), pl.ds(CUT, 2048 - CUT)], held.at[n], sems.at[n]
-        )
-        for n in range(4)
+        pltpu.make_async_copy(gradient_a, held_a, sems.at[0]),
+        pltpu.make_async_copy(gradient_b, held_b, sems.at[1]),
+        pltpu.make_async_copy(factor, factor_out, sems.at[2]),
     ]
-    copies += [
-        pltpu.make_async_copy(cotangents.at[m], seen.at[m], sems.at[4 + m]) for m in range(3)
-    ]
-    for copy in copies[4:] + copies[:4]:
-        copy.start()
+    copies[0].start()
+    copies[1].start()
+    first = lax.axis_index(CORE) * 32
     for z in range(8):
         for y in range(4):
             row = z * 256 + y * 64
-            factor[pl.ds(row + pl.multiple_of(place[2] * 32, 32), 32)] = mine[y, z]
-            factor[pl.ds(row + pl.multiple_of(32 - place[2] * 32, 32), 32)] = other[y, z]
-    factor_copy = pltpu.make_async_copy(factor, factor_out, factor_sem)
-    factor_copy.start()
-    projected = jnp.dot(gradient[...], factor[:CUT], preferred_element_type=F32)
-    for m in range(3):
-        copies[4 + m].wait()
-        turned[m * 128 : (m + 1) * 128] = seen[m].T
-    for n in range(4):
-        copies[n].wait()
-        mapped[n * 512 : (n + 1) * 512] = jnp.dot(
-            held[n], factor[CUT:], preferred_element_type=F32
-        ).astype(BF)
-    projected += jnp.dot(turned[...], mapped[...], preferred_element_type=F32)
+            factor[pl.ds(row + pl.multiple_of(first, 32), 32)] = mine[y, z]
+            factor[pl.ds(row + pl.multiple_of(32 - first, 32), 32)] = other[y, z]
+    copies[2].start()
+    copies[0].wait()
+    projected = jnp.dot(held_a[...], factor[:CUT], preferred_element_type=F32)
+    copies[1].wait()
+    projected += jnp.dot(held_b[...], factor[CUT:], preferred_element_type=F32)
     rows = [projected[m * 128 : (m + 1) * 128].T.reshape(32, 8, 128) for m in range(3)]
     out[...] = jnp.concatenate(rows, axis=1).astype(BF)
-    factor_copy.wait()
+    copies[2].wait()
 
 
 def square_kernel(projected, out):
@@ -106,11 +92,12 @@
 
 
 def final_kernel(
-    place, squares, projected, own, state, right, left, across_a, across_b,
+    squares, projected, own, state, right, left, across_a, across_b,
     first, second, weights, factor, own_factor,
     update_out, weights_out, copies_out, first_out, second_out,
     update, new_weights, copies, new_first, new_second, normed, change, own_sems, sems,
 ):
+    place = (lax.axis_index(Z), lax.axis_index(Y))
     total = jnp.sum(jnp.sum(squares[...], axis=0), keepdims=True)
     root_mean = jnp.sqrt(total / (3 * RANK * MW) + 1e-06)
     clip = jnp.minimum(1.0, 0.25 / root_mean)
@@ -185,51 +172,49 @@
 
 
 def step(inputs, cotangents, factor, weights, first_moment, second_moment):
-    place = jnp.stack([lax.axis_index(axis) for axis in (Z, Y, CORE)]).astype(jnp.int32)
-    smem = pl.BlockSpec(memory_space=pltpu.SMEM)
     hbm = pl.BlockSpec(memory_space=pl.ANY)
-    half = pl.pallas_call(
-        spread_kernel,
-        out_shape=jax.ShapeDtypeStruct((8, 32, RANK), BF),
-        in_specs=[smem, VMEM],
-        out_specs=VMEM,
+    half, state = pl.pallas_call(
+        head_kernel,
+        out_shape=(
+            jax.ShapeDtypeStruct((8, 32, RANK), BF),
+            jax.ShapeDtypeStruct((1, 240, 128), BF),
+        ),
+        in_specs=[VMEM] * 4,
+        out_specs=(VMEM, VMEM),
         compiler_params=pltpu.CompilerParams(vmem_limit_bytes=60 << 20),
-    )(place, factor)
+    )(factor, weights, first_moment, second_moment)
     half = lax.all_to_all(half, Z, split_axis=0, concat_axis=0, tiled=True)
     half = sent_to_all(half, Y)
     other_half = moved(half, CORE, 1)
-    state = pl.pallas_call(
-        state_kernel,
-        out_shape=jax.ShapeDtypeStruct((1, 240, 128), BF),
-        in_specs=[VMEM] * 3,
-        out_specs=VMEM,
-        compiler_params=pltpu.CompilerParams(vmem_limit_bytes=60 << 20),
-    )(weights, first_moment, second_moment)
     state_z = gathered_z(state)
     states = gathered_y(state_z)
 
 
-    gradient = (
-        jnp.einsum("mtc,td->mcd", cotangents, inputs[:, :CUT], preferred_element_type=F32)
-        .astype(BF)
-        .reshape(384, CUT)
-    )
+    def gradient_of(part):
+        return (
+            jnp.einsum("mtc,td->mcd", cotangents, part, preferred_element_type=F32)
+            .astype(BF)
+            .reshape(384, -1)
+        )
+
+    gradient_a = gradient_of(inputs[:, :CUT])
+    gradient_b = gradient_of(inputs[:, CUT:])
     partial_value, factor_all = pl.pallas_call(
         partial_kernel,
-        out_shape=(jax.ShapeDtypeStruct((32, 24, 128), BF), jax.ShapeDtypeStruct((2048, RANK), BF)),
-        in_specs=[smem, VMEM, hbm, hbm, VMEM, VMEM],
+        out_shape=(
+            jax.ShapeDtypeStruct((32, 24, 128), BF),
+            jax.ShapeDtypeStruct((2048, RANK), BF),
+        ),
+        in_specs=[hbm, hbm, VMEM, VMEM],
         out_specs=(VMEM, hbm),
         scratch_shapes=[
             pltpu.VMEM((2048, RANK), BF),
-            pltpu.VMEM((4, 512, 2048 - CUT), BF),
-            pltpu.VMEM((3, 2048, 128), BF),
-            pltpu.VMEM((384, 2048), BF),
-            pltpu.VMEM((2048, RANK), BF),
-            pltpu.SemaphoreType.DMA((7,)),
-            pltpu.SemaphoreType.DMA,
+            pltpu.VMEM((384, CUT), BF),
+            pltpu.VMEM((384, 2048 - CUT), BF),
+            pltpu.SemaphoreType.DMA((3,)),
         ],
-        compiler_params=pltpu.CompilerParams(vmem_limit_bytes=50 << 20),
-    )(place, gradient, cotangents, inputs, half, other_half)
+        compiler_params=pltpu.CompilerParams(vmem_limit_bytes=60 << 20),
+    )(gradient_a, gradient_b, half, other_half)
     arrived = lax.all_to_all(partial_value, FS, split_axis=0, concat_axis=0, tiled=True)
     projected = arrived.astype(F32).sum(axis=0)
     projected_all = sent_to_all(projected.astype(BF), FS)
@@ -250,7 +235,7 @@
             jax.ShapeDtypeStruct((3, 8, 128), F32),
             jax.ShapeDtypeStruct((3, 8, 128), F32),
         ),
-        in_specs=[smem] + [VMEM] * 13,
+        in_specs=[VMEM] * 13,
         out_specs=(hbm,) * 5,
         scratch_shapes=[
             pltpu.VMEM((3, 64, 128), F32),
@@ -265,7 +250,7 @@
         ],
         compiler_params=pltpu.CompilerParams(vmem_limit_bytes=24 << 20),
     )(
-        place, squares, projected_all, projected, *states, first_moment, second_moment,
+        squares, projected_all, projected, *states, first_moment, second_moment,
         weights, factor_all, factor,
     )
 

time: 104 us -> 97.5 us (0.938)
  blocking collectives: 16.8 us -> 0 us
  starting transfers between devices: 34.7 us -> 46.9 us
  waiting for transfers between devices: 29.3 us -> 23.9 us
  matrix products: 4.47 us -> 9.83 us
  Pallas kernels: 13.3 us -> 10.3 us
  local copies, waits for them, and re-layouts: 3.08 us -> 5.13 us
    all_to_all x1 -> x0, blocking collectives: 16.8 us -> none  [step(): half = lax.all_to_all(half, Z, split_axis=0, concat_axis=0, tiled=True)]
    all_to_all x0 -> x1, starting transfers between devices: none -> 9 us  [step(): half = lax.all_to_all(half, Z, split_axis=0, concat_axis=0, tiled=True)]
    all_to_all x0 -> x1, waiting for transfers between devices: none -> 6.3 us  [step(): half = lax.all_to_all(half, Z, split_axis=0, concat_axis=0, tiled=True)]
    ppermute x9, waiting for transfers between devices: 6.41 us -> 0.2 us  [moved(): lax.ppermute(array, axis, [(i, (i + shift) % size) for i in range(size)])]
    dot_general x1 -> x2, matrix products: 4.47 us -> 9.83 us  [gradient_of(): jnp.einsum('mtc,td->mcd', cotangents, part, preferred_element_type=F32)]
    all_to_all x2, waiting for transfers between devices: 10.9 us -> 5.62 us  [sent_to_all(): return lax.all_to_all(copies, axis, split_axis=0, concat_axis=0, tiled=True)]
    all_to_all x1, starting transfers between devices: 4.96 us -> 7.12 us  [step(): lax.all_to_all(partial_value, FS, split_axis=0, concat_axis=0, tiled=True)]
    pallas_call x1, Pallas kernels: 6.47 us -> 4.32 us  [step(): pl.pallas_call(partial_kernel, out_shape=(jax.ShapeDtypeStruct((32, 24, 1...]
  transfers between devices with their start and end apart: 13 -> 14, of which waited for: 5 -> 5; matrix products, arithmetic and copies ran while one was open for 7% -> 13% of each run, Pallas kernels for 8% -> 5%
where the time goes in v6:
time: 97.5 us; the launch traced here: 96.8 us
  starting transfers between devices  46.9 us (48%)
  waiting for transfers between devices  23.9 us (25%)
  Pallas kernels  10.3 us (11%)
  matrix products  9.83 us (10%)
  local copies, waits for them, and re-layouts  5.13 us (5%)
    ppermute x9, starting transfers between devices, moved(): lax.ppermute(array, axis, [(i, (i + shift) % size) for i in range(size)])  14.3 us
    dot_general x2, matrix products, gradient_of(): jnp.einsum('mtc,td->mcd', cotangents, part, preferred_element_type=F32)  9.83 us
    all_to_all x1, starting transfers between devices, step(): half = lax.all_to_all(half, Z, split_axis=0, concat_axis=0, tiled=True)  9 us
    all_to_all x2, starting transfers between devices, sent_to_all(): return lax.all_to_all(copies, axis, split_axis=0, concat_axis=0, tiled=True)  8.43 us
    all_to_all x1, starting transfers between devices, step(): lax.all_to_all(squares, TP, split_axis=0, concat_axis=0, tiled=True)  8.01 us
    all_to_all x1, starting transfers between devices, step(): lax.all_to_all(partial_value, FS, split_axis=0, concat_axis=0, tiled=True)  7.12 us
    all_to_all x1, waiting for transfers between devices, step(): lax.all_to_all(partial_value, FS, split_axis=0, concat_axis=0, tiled=True)  7.06 us
    all_to_all x1, waiting for transfers between devices, step(): half = lax.all_to_all(half, Z, split_axis=0, concat_axis=0, tiled=True)  6.3 us
  transfers between devices with their start and end apart: 14, of which 5 were waited for; matrix products, arithmetic and copies ran while one was open for 13% of the time, Pallas kernels for 5%

profile of v6, /device:TPU:1, one launch (start us, length us, event | category | flops | bytes accessed | tf_op | source)
XLA Modules:
  0.0 96.8 jit_solution(577751443472446088)
XLA Ops:
  0.6 0.0 copy-start
  0.6 1.7 %shard_map.101 = (bf16[8,32,256]{2,1,0:T(8,128)(2,1)}, bf16[1,240,128]{2,1,0:T(8,128)(2,1)}) custom-call(bf16[64,256]{1,0:T(8,128)(2,1)} %own_factor.1, f32[3,64,128]{2,1,0:T(8,128)} %weights.3, f32[3,8,128]{2,1,0:T(8,128)} %first.3, f32[3,8,128]{2,1,0:T(8,128)} %second.3), custom_call_target="tpu_custom_call" | custom-call | tf_op jit(solution)/shard_map/pallas_call | solution.py:176
  2.3 9.0 %all-to-all-start = ((bf16[8,32,256]{2,1,0:T(8,128)(2,1)}), bf16[8,32,256]{2,1,0:T(8,128)(2,1)S(1)}, u32[]{:S(2)}, u32[]{:S(2)}) async-start(bf16[8,32,256]{2,1,0:T(8,128)(2,1)} %get-tuple-element.9), calls=%async_computation | async-start | bytes 262144 | tf_op jit(solution)/shard_map/all_to_all | solution.py:186
  11.4 1.5 %collective-permute-start.1 = (bf16[1,240,128]{2,1,0:T(8,128)(2,1)}, bf16[1,240,128]{2,1,0:T(8,128)(2,1)S(1)}, u32[]{:S(2)}, u32[]{:S(2)}) collective-permute-start(bf16[1,240,128]{2,1,0:T(8,128)(2,1)} %get-tuple-element.11), channel_id=1, source_target_pairs={{0,32},{32,64},{64,96},{96,128},{128,160},{160,192},{192,224},{224... | collective-permute-start | bytes 184328 | tf_op jit(solution)/shard_map/ppermute | solution.py:29
  12.8 6.3 %all-to-all-done = bf16[8,32,256]{2,1,0:T(8,128)(2,1)S(1)} async-done(((bf16[8,32,256]{2,1,0:T(8,128)(2,1)}), bf16[8,32,256]{2,1,0:T(8,128)(2,1)S(1)}, u32[]{:S(2)}, u32[]{:S(2)}) %all-to-all-start) | async-done | bytes 131104 | tf_op jit(solution)/shard_map/all_to_all | solution.py:186
  19.1 0.9 broadcast_in_dim.6
  20.0 4.2 %all-to-all-start.1 = ((bf16[4,8,32,256]{3,2,1,0:T(8,128)(2,1)}), bf16[4,8,32,256]{3,2,1,0:T(8,128)(2,1)S(1)}, u32[]{:S(2)}, u32[]{:S(2)}) async-start(bf16[4,8,32,256]{3,2,1,0:T(8,128)(2,1)} %broadcast_in_dim.6), calls=%async_computation.1 | async-start | bytes 1048576 | tf_op jit(solution)/shard_map/all_to_all | solution.py:24
  24.2 4.9 %fusion.6 = bf16[3,128,1024]{2,1,0:T(8,128)(2,1)} fusion(bf16[3,2048,128]{2,1,0:T(8,128)(2,1)S(1)} %copy-done, bf16[2048,2048]{1,0:T(8,128)(2,1)} %param.6), kind=kOutput, calls=%fused_computation.6 | convolution fusion | flops 1611005952 | bytes 6553600 | tf_op jit(solution)/shard_map/mtc,td->mcd/dot_general | solution.py:195
  29.1 0.1 collective-permute-start.2
  29.2 3.5 %collective-permute-start.3 = (bf16[2,240,128]{2,1,0:T(8,128)(2,1)S(1)}, bf16[2,240,128]{2,1,0:T(8,128)(2,1)S(1)}, u32[]{:S(2)}, u32[]{:S(2)}) collective-permute-start(bf16[2,240,128]{2,1,0:T(8,128)(2,1)S(1)} %get-tuple-element.13), channel_id=1, source_target_pairs={{0,192},{32,224},{64,0},{96,32},{128,64},{160,96},{192,128},{224,1... | collective-permute-start | bytes 368648 | tf_op jit(solution)/shard_map/ppermute | solution.py:29
  32.8 3.8 %collective-permute-start = (bf16[4,8,32,256]{3,2,1,0:T(8,128)(2,1)S(1)}, bf16[4,8,32,256]{3,2,1,0:T(8,128)(2,1)S(1)}, u32[]{:S(2)}, u32[]{:S(2)}) collective-permute-start(bf16[4,8,32,256]{3,2,1,0:T(8,128)(2,1)S(1)} %all-to-all-done.1.mine), channel_id=1, source_target_pairs={{0,1},{1,0},{2,3},{3,2},{4,5},{5,4},{6,7},{7,6},{8,9},{9,8},{10,11... | collective-permute-start | bytes 1572872 | tf_op jit(solution)/shard_map/ppermute | solution.py:29
  36.5 4.9 %fusion.9 = bf16[3,128,1024]{2,1,0:T(8,128)(2,1)} fusion(bf16[3,2048,128]{2,1,0:T(8,128)(2,1)S(1)} %copy-done, bf16[2048,2048]{1,0:T(8,128)(2,1)} %param.6), kind=kOutput, calls=%fused_computation.7 | convolution fusion | flops 1611005952 | bytes 6553600 | tf_op jit(solution)/shard_map/mtc,td->mcd/dot_general | solution.py:195
  41.5 0.8 copy-done.7
  42.3 4.3 %shard_map.102 = (bf16[32,24,128]{2,1,0:T(8,128)(2,1)}, bf16[2048,256]{1,0:T(8,128)(2,1)}) custom-call(bf16[384,1024]{1,0:T(8,128)(2,1)} %bitcast.14, bf16[384,1024]{1,0:T(8,128)(2,1)} %bitcast.15, bf16[4,8,32,256]{3,2,1,0:T(8,128)(2,1)} %copy-done.6, bf16[4,8,32,256]{3,2,1,0:T(8,128)(2,1)} %copy-done.7), custom_call_target="tpu_custom_call" | custom-call | tf_op jit(solution)/shard_map/pallas_call | solution.py:202
  46.7 0.0 copy-start.3
  46.7 7.1 %all-to-all-start.2 = ((bf16[32,24,128]{2,1,0:T(8,128)(2,1)}), bf16[32,24,128]{2,1,0:T(8,128)(2,1)S(1)}, u32[]{:S(2)}, u32[]{:S(2)}) async-start(bf16[32,24,128]{2,1,0:T(8,128)(2,1)} %get-tuple-element.10), calls=%async_computation.2 | async-start | bytes 393216 | tf_op jit(solution)/shard_map/all_to_all | solution.py:218
  53.9 1.3 %collective-permute-start.5 = (bf16[8,240,128]{2,1,0:T(8,128)(2,1)S(1)}, bf16[8,240,128]{2,1,0:T(8,128)(2,1)S(1)}, u32[]{:S(2)}, u32[]{:S(2)}) collective-permute-start(bf16[8,240,128]{2,1,0:T(8,128)(2,1)S(1)} %constant_dynamic-update-slice_fusion.2.state), channel_id=1, source_target_pairs={{0,8},{8,16},{16,24},{24,0},{1,9},{9,17},{17,25},{25,1},{2,10},{10... | collective-permute-start | bytes 1474568 | tf_op jit(solution)/shard_map/ppermute | solution.py:29
  55.2 1.4 %collective-permute-start.6 = (bf16[8,240,128]{2,1,0:T(8,128)(2,1)S(1)}, bf16[8,240,128]{2,1,0:T(8,128)(2,1)S(1)}, u32[]{:S(2)}, u32[]{:S(2)}) collective-permute-start(bf16[8,240,128]{2,1,0:T(8,128)(2,1)S(1)} %constant_dynamic-update-slice_fusion.2.state), channel_id=1, source_target_pairs={{0,24},{8,0},{16,8},{24,16},{1,25},{9,1},{17,9},{25,17},{2,26},{10... | collective-permute-start | bytes 1474568 | tf_op jit(solution)/shard_map/ppermute | solution.py:29
  56.7 7.1 %all-to-all-done.2 = bf16[32,24,128]{2,1,0:T(8,128)(2,1)S(1)} async-done(((bf16[32,24,128]{2,1,0:T(8,128)(2,1)}), bf16[32,24,128]{2,1,0:T(8,128)(2,1)S(1)}, u32[]{:S(2)}, u32[]{:S(2)}) %all-to-all-start.2) | async-done | bytes 196640 | tf_op jit(solution)/shard_map/all_to_all | solution.py:218
  63.8 0.7 broadcast_in_dim.7
  64.5 4.3 %all-to-all-start.3 = ((bf16[32,24,128]{2,1,0:T(8,128)(2,1)}), bf16[32,24,128]{2,1,0:T(8,128)(2,1)S(1)}, u32[]{:S(2)}, u32[]{:S(2)}) async-start(bf16[32,24,128]{2,1,0:T(8,128)(2,1)} %broadcast_in_dim.7), calls=%async_computation.3 | async-start | bytes 393216 | tf_op jit(solution)/shard_map/all_to_all | solution.py:24
  68.7 0.2 collective-permute-done.5.right
  68.9 0.7 slice.16
  69.6 1.1 %collective-permute-start.7 = (bf16[4,240,128]{2,1,0:T(8,128)(2,1)}, bf16[4,240,128]{2,1,0:T(8,128)(2,1)}, u32[]{:S(2)}, u32[]{:S(2)}) collective-permute-start(bf16[4,240,128]{2,1,0:T(8,128)(2,1)} %slice.16), channel_id=1, source_target_pairs={{0,8},{8,16},{16,24},{24,0},{1,9},{9,17},{17,25},{25,1},{2,10},{10... | collective-permute-start | bytes 737288 | tf_op jit(solution)/shard_map/ppermute | solution.py:29
  70.7 0.7 slice.17
  71.4 1.6 %collective-permute-start.8 = (bf16[4,240,128]{2,1,0:T(8,128)(2,1)}, bf16[4,240,128]{2,1,0:T(8,128)(2,1)}, u32[]{:S(2)}, u32[]{:S(2)}) collective-permute-start(bf16[4,240,128]{2,1,0:T(8,128)(2,1)} %slice.17), channel_id=1, source_target_pairs={{0,24},{8,0},{16,8},{24,16},{1,25},{9,1},{17,9},{25,17},{2,26},{10... | collective-permute-start | bytes 737288 | tf_op jit(solution)/shard_map/ppermute | solution.py:29
  73.0 5.6 %all-to-all-done.3.projected = bf16[32,24,128]{2,1,0:T(8,128)(2,1)S(1)} async-done(((bf16[32,24,128]{2,1,0:T(8,128)(2,1)}), bf16[32,24,128]{2,1,0:T(8,128)(2,1)S(1)}, u32[]{:S(2)}, u32[]{:S(2)}) %all-to-all-start.3) | async-done | bytes 196640 | tf_op jit(solution)/shard_map/all_to_all | solution.py:24
  78.6 0.7 shard_map.103
  79.3 8.0 %all-to-all-start.4 = ((f32[8,8,128]{2,1,0:T(8,128)}), f32[8,8,128]{2,1,0:T(8,128)S(1)}, u32[]{:S(2)}, u32[]{:S(2)}) async-start(f32[8,8,128]{2,1,0:T(8,128)} %shard_map.103), calls=%async_computation.4 | async-start | bytes 65536 | tf_op jit(solution)/shard_map/all_to_all | solution.py:228
  87.4 4.7 %all-to-all-done.4.squares = f32[8,8,128]{2,1,0:T(8,128)S(1)} async-done(((f32[8,8,128]{2,1,0:T(8,128)}), f32[8,8,128]{2,1,0:T(8,128)S(1)}, u32[]{:S(2)}, u32[]{:S(2)}) %all-to-all-start.4) | async-done | bytes 32800 | tf_op jit(solution)/shard_map/all_to_all | solution.py:228
  92.1 1.2 %copy-done.1 = bf16[2048,256]{1,0:T(8,128)(2,1)S(1)} copy-done((bf16[2048,256]{1,0:T(8,128)(2,1)S(1)}, bf16[2048,256]{1,0:T(8,128)(2,1)}, u32[]{:S(2)}) %copy-start.1) | copy-done | bytes 1048600
  93.3 3.5 %shard_map.104 = (f32[3,64,128]{2,1,0:T(8,128)}, f32[3,64,128]{2,1,0:T(8,128)}, bf16[3,2048,128]{2,1,0:T(8,128)(2,1)}, f32[3,8,128]{2,1,0:T(8,128)}, f32[3,8,128]{2,1,0:T(8,128)}) custom-call(f32[8,8,128]{2,1,0:T(8,128)S(1)} %all-to-all-done.4.squares, bf16[32,24,128]{2,1,0:T(8,128)(2,1)S(1)} %all-to-all-done.3.projected, ...), custom_call_target="tpu_custom_call" | custom-call | tf_op jit(solution)/shard_map/pallas_call | solution.py:229
  (31 shorter events, 0.2 us)
Async XLA Ops:
  0.6 23.5 %copy-start = (bf16[3,2048,128]{2,1,0:T(8,128)(2,1)S(1)}, bf16[3,2048,128]{2,1,0:T(8,128)(2,1)}, u32[]{:S(2)}) copy-start(bf16[3,2048,128]{2,1,0:T(8,128)(2,1)} %param.7) | copy-start | bytes 4718596
  2.3 16.8 %all-to-all-start = ((bf16[8,32,256]{2,1,0:T(8,128)(2,1)}), bf16[8,32,256]{2,1,0:T(8,128)(2,1)S(1)}, u32[]{:S(2)}, u32[]{:S(2)}) async-start(bf16[8,32,256]{2,1,0:T(8,128)(2,1)} %get-tuple-element.9), calls=%async_computation | async-start | bytes 262144 | tf_op jit(solution)/shard_map/all_to_all | solution.py:186
  11.4 17.7 %collective-permute-start.1 = (bf16[1,240,128]{2,1,0:T(8,128)(2,1)}, bf16[1,240,128]{2,1,0:T(8,128)(2,1)S(1)}, u32[]{:S(2)}, u32[]{:S(2)}) collective-permute-start(bf16[1,240,128]{2,1,0:T(8,128)(2,1)} %get-tuple-element.11), channel_id=1, source_target_pairs={{0,32},{32,64},{64,96},{96,128},{128,160},{160,192},{192,224},{224... | collective-permute-start | bytes 184328 | tf_op jit(solution)/shard_map/ppermute | solution.py:29
  20.0 12.8 %all-to-all-start.1 = ((bf16[4,8,32,256]{3,2,1,0:T(8,128)(2,1)}), bf16[4,8,32,256]{3,2,1,0:T(8,128)(2,1)S(1)}, u32[]{:S(2)}, u32[]{:S(2)}) async-start(bf16[4,8,32,256]{3,2,1,0:T(8,128)(2,1)} %broadcast_in_dim.6), calls=%async_computation.1 | async-start | bytes 1048576 | tf_op jit(solution)/shard_map/all_to_all | solution.py:24
  24.2 4.9 %copy-start.8 = (bf16[1,240,128]{2,1,0:T(8,128)(2,1)S(1)}, bf16[1,240,128]{2,1,0:T(8,128)(2,1)}, u32[]{:S(2)}) copy-start(bf16[1,240,128]{2,1,0:T(8,128)(2,1)} %get-tuple-element.11) | copy-start | bytes 184324
  29.1 12.4 %collective-permute-start.2 = (bf16[2,240,128]{2,1,0:T(8,128)(2,1)S(1)}, bf16[2,240,128]{2,1,0:T(8,128)(2,1)S(1)}, u32[]{:S(2)}, u32[]{:S(2)}) collective-permute-start(bf16[2,240,128]{2,1,0:T(8,128)(2,1)S(1)} %get-tuple-element.13), channel_id=1, source_target_pairs={{0,64},{32,96},{64,128},{96,160},{128,192},{160,224},{192,0},{224,... | collective-permute-start | bytes 368648 | tf_op jit(solution)/shard_map/ppermute | solution.py:29
  29.2 12.2 %collective-permute-start.3 = (bf16[2,240,128]{2,1,0:T(8,128)(2,1)S(1)}, bf16[2,240,128]{2,1,0:T(8,128)(2,1)S(1)}, u32[]{:S(2)}, u32[]{:S(2)}) collective-permute-start(bf16[2,240,128]{2,1,0:T(8,128)(2,1)S(1)} %get-tuple-element.13), channel_id=1, source_target_pairs={{0,192},{32,224},{64,0},{96,32},{128,64},{160,96},{192,128},{224,1... | collective-permute-start | bytes 368648 | tf_op jit(solution)/shard_map/ppermute | solution.py:29
  32.8 8.7 %copy-start.6 = (bf16[4,8,32,256]{3,2,1,0:T(8,128)(2,1)}, bf16[4,8,32,256]{3,2,1,0:T(8,128)(2,1)S(1)}, u32[]{:S(2)}) copy-start(bf16[4,8,32,256]{3,2,1,0:T(8,128)(2,1)S(1)} %all-to-all-done.1.mine) | copy-start | bytes 1572868
  32.8 8.8 %collective-permute-start = (bf16[4,8,32,256]{3,2,1,0:T(8,128)(2,1)S(1)}, bf16[4,8,32,256]{3,2,1,0:T(8,128)(2,1)S(1)}, u32[]{:S(2)}, u32[]{:S(2)}) collective-permute-start(bf16[4,8,32,256]{3,2,1,0:T(8,128)(2,1)S(1)} %all-to-all-done.1.mine), channel_id=1, source_target_pairs={{0,1},{1,0},{2,3},{3,2},{4,5},{5,4},{6,7},{7,6},{8,9},{9,8},{10,11... | collective-permute-start | bytes 1572872 | tf_op jit(solution)/shard_map/ppermute | solution.py:29
  41.5 12.4 %collective-permute-start.4 = (bf16[2,240,128]{2,1,0:T(8,128)(2,1)S(1)}, bf16[2,240,128]{2,1,0:T(8,128)(2,1)S(1)}, u32[]{:S(2)}, u32[]{:S(2)}) collective-permute-start(bf16[2,240,128]{2,1,0:T(8,128)(2,1)S(1)} %collective-permute-done.3), channel_id=1, source_target_pairs={{0,192},{32,224},{64,0},{96,32},{128,64},{160,96},{192,128},{224,1... | collective-permute-start | bytes 368648 | tf_op jit(solution)/shard_map/ppermute | solution.py:29
  41.5 0.8 copy-start.7
  46.7 45.4 %copy-start.2 = (f32[3,64,128]{2,1,0:T(8,128)S(1)}, f32[3,64,128]{2,1,0:T(8,128)}, u32[]{:S(2)}) copy-start(f32[3,64,128]{2,1,0:T(8,128)} %weights.3) | copy-start | bytes 294916
  46.7 45.4 %copy-start.3 = (bf16[64,256]{1,0:T(8,128)(2,1)S(1)}, bf16[64,256]{1,0:T(8,128)(2,1)}, u32[]{:S(2)}) copy-start(bf16[64,256]{1,0:T(8,128)(2,1)} %own_factor.1) | copy-start | bytes 98308
  46.7 45.4 %copy-start.4 = (f32[3,8,128]{2,1,0:T(8,128)S(1)}, f32[3,8,128]{2,1,0:T(8,128)}, u32[]{:S(2)}) copy-start(f32[3,8,128]{2,1,0:T(8,128)} %first.3) | copy-start | bytes 36868
  46.7 45.4 %copy-start.5 = (f32[3,8,128]{2,1,0:T(8,128)S(1)}, f32[3,8,128]{2,1,0:T(8,128)}, u32[]{:S(2)}) copy-start(f32[3,8,128]{2,1,0:T(8,128)} %second.3) | copy-start | bytes 36868
  46.7 17.0 %all-to-all-start.2 = ((bf16[32,24,128]{2,1,0:T(8,128)(2,1)}), bf16[32,24,128]{2,1,0:T(8,128)(2,1)S(1)}, u32[]{:S(2)}, u32[]{:S(2)}) async-start(bf16[32,24,128]{2,1,0:T(8,128)(2,1)} %get-tuple-element.10), calls=%async_computation.2 | async-start | bytes 393216 | tf_op jit(solution)/shard_map/all_to_all | solution.py:218
  53.9 15.0 %collective-permute-start.5 = (bf16[8,240,128]{2,1,0:T(8,128)(2,1)S(1)}, bf16[8,240,128]{2,1,0:T(8,128)(2,1)S(1)}, u32[]{:S(2)}, u32[]{:S(2)}) collective-permute-start(bf16[8,240,128]{2,1,0:T(8,128)(2,1)S(1)} %constant_dynamic-update-slice_fusion.2.state), channel_id=1, source_target_pairs={{0,8},{8,16},{16,24},{24,0},{1,9},{9,17},{17,25},{25,1},{2,10},{10... | collective-permute-start | bytes 1474568 | tf_op jit(solution)/shard_map/ppermute | solution.py:29
  55.2 15.5 %collective-permute-start.6 = (bf16[8,240,128]{2,1,0:T(8,128)(2,1)S(1)}, bf16[8,240,128]{2,1,0:T(8,128)(2,1)S(1)}, u32[]{:S(2)}, u32[]{:S(2)}) collective-permute-start(bf16[8,240,128]{2,1,0:T(8,128)(2,1)S(1)} %constant_dynamic-update-slice_fusion.2.state), channel_id=1, source_target_pairs={{0,24},{8,0},{16,8},{24,16},{1,25},{9,1},{17,9},{25,17},{2,26},{10... | collective-permute-start | bytes 1474568 | tf_op jit(solution)/shard_map/ppermute | solution.py:29
  64.5 14.2 %all-to-all-start.3 = ((bf16[32,24,128]{2,1,0:T(8,128)(2,1)}), bf16[32,24,128]{2,1,0:T(8,128)(2,1)S(1)}, u32[]{:S(2)}, u32[]{:S(2)}) async-start(bf16[32,24,128]{2,1,0:T(8,128)(2,1)} %broadcast_in_dim.7), calls=%async_computation.3 | async-start | bytes 393216 | tf_op jit(solution)/shard_map/all_to_all | solution.py:24
  69.6 17.8 %collective-permute-start.7 = (bf16[4,240,128]{2,1,0:T(8,128)(2,1)}, bf16[4,240,128]{2,1,0:T(8,128)(2,1)}, u32[]{:S(2)}, u32[]{:S(2)}) collective-permute-start(bf16[4,240,128]{2,1,0:T(8,128)(2,1)} %slice.16), channel_id=1, source_target_pairs={{0,8},{8,16},{16,24},{24,0},{1,9},{9,17},{17,25},{25,1},{2,10},{10... | collective-permute-start | bytes 737288 | tf_op jit(solution)/shard_map/ppermute | solution.py:29
  71.4 16.0 %collective-permute-start.8 = (bf16[4,240,128]{2,1,0:T(8,128)(2,1)}, bf16[4,240,128]{2,1,0:T(8,128)(2,1)}, u32[]{:S(2)}, u32[]{:S(2)}) collective-permute-start(bf16[4,240,128]{2,1,0:T(8,128)(2,1)} %slice.17), channel_id=1, source_target_pairs={{0,24},{8,0},{16,8},{24,16},{1,25},{9,1},{17,9},{25,17},{2,26},{10... | collective-permute-start | bytes 737288 | tf_op jit(solution)/shard_map/ppermute | solution.py:29
  79.3 12.7 %all-to-all-start.4 = ((f32[8,8,128]{2,1,0:T(8,128)}), f32[8,8,128]{2,1,0:T(8,128)S(1)}, u32[]{:S(2)}, u32[]{:S(2)}) async-start(f32[8,8,128]{2,1,0:T(8,128)} %shard_map.103), calls=%async_computation.4 | async-start | bytes 65536 | tf_op jit(solution)/shard_map/all_to_all | solution.py:228
  92.1 1.2 %copy-start.1 = (bf16[2048,256]{1,0:T(8,128)(2,1)S(1)}, bf16[2048,256]{1,0:T(8,128)(2,1)}, u32[]{:S(2)}) copy-start(bf16[2048,256]{1,0:T(8,128)(2,1)} %get-tuple-element.12.factor) | copy-start | bytes 3145732

commit v7 on v6

--- a/solution.py
+++ b/solution.py
@@ -12,8 +12,7 @@
 FS = ("fs_0", "fs_1")
 TP = ("tp_0", "tp_1")
 CORE = "tp_1"
-AWAY = (0, 7, 6, 5, 2, 1, 4, 3)
-CUT = 1024
+AWAY = (0, 4, 2, 6, 1, 5, 3, 7)
 BF = jnp.bfloat16
 F32 = jnp.float32
 VMEM = pl.BlockSpec(memory_space=pltpu.VMEM)
@@ -29,11 +28,15 @@
     return lax.ppermute(array, axis, [(i, (i + shift) % size) for i in range(size)])
 
 
+def swapped(array, axis, bit):
+    size = lax.axis_size(axis)
+    return lax.ppermute(array, axis, [(i, i ^ bit) for i in range(size)])
+
+
 def gathered_z(array):
-    pair = jnp.concatenate([array, moved(array, Z, 1)])
-    below = moved(pair, Z, 2)
-    above = moved(pair, Z, -2)
-    return jnp.concatenate([pair, below, above, moved(above, Z, -2)])
+    for bit in (4, 2, 1):
+        array = jnp.concatenate([array, swapped(array, Z, bit)])
+    return array
 
 
 def gathered_y(array):
@@ -46,37 +49,34 @@
 
 
 def head_kernel(factor, weights, first, second, half, state):
-    rows = factor[pl.ds(pl.multiple_of(lax.axis_index(CORE) * 32, 32), 32)]
-    half[...] = jnp.broadcast_to(rows, half.shape)
+    low, high = factor[:, :128], factor[:, 128:]
+    columns = jnp.where(lax.axis_index(CORE) == 0, low, high)
+    half[...] = jnp.broadcast_to(columns, half.shape)
     state[0, :192] = weights[...].reshape(192, 128).astype(BF)
     moments = jnp.concatenate([first[...].reshape(24, 128), second[...].reshape(24, 128)])
     state[0, 192:] = moments.astype(BF)
 
 
-def partial_kernel(
-    gradient_a, gradient_b, mine, other, out, factor_out, factor, held_a, held_b, sems
-):
-    copies = [
-        pltpu.make_async_copy(gradient_a, held_a, sems.at[0]),
-        pltpu.make_async_copy(gradient_b, held_b, sems.at[1]),
-        pltpu.make_async_copy(factor, factor_out, sems.at[2]),
-    ]
-    copies[0].start()
-    copies[1].start()
-    first = lax.axis_index(CORE) * 32
-    for z in range(8):
-        for y in range(4):
-            row = z * 256 + y * 64
-            factor[pl.ds(row + pl.multiple_of(first, 32), 32)] = mine[y, z]
-            factor[pl.ds(row + pl.multiple_of(32 - first, 32), 32)] = other[y, z]
-    copies[2].start()
-    copies[0].wait()
-    projected = jnp.dot(held_a[...], factor[:CUT], preferred_element_type=F32)
-    copies[1].wait()
-    projected += jnp.dot(held_b[...], factor[CUT:], preferred_element_type=F32)
-    rows = [projected[m * 128 : (m + 1) * 128].T.reshape(32, 8, 128) for m in range(3)]
-    out[...] = jnp.concatenate(rows, axis=1).astype(BF)
-    copies[2].wait()
+def partial_of(gradient, half):
+    projected = jnp.dot(gradient[...], half[...].reshape(2048, 128), preferred_element_type=F32)
+    rows = [projected[m * 128 : (m + 1) * 128].T.reshape(16, 8, 128) for m in range(3)]
+    return jnp.concatenate(rows, axis=1).astype(BF)
+
+
+def first_kernel(gradient, mine, out, mine_out, sem):
+    copy = pltpu.make_async_copy(mine, mine_out, sem)
+    copy.start()
+    out[...] = partial_of(gradient, mine)
+    copy.wait()
+
+
+def second_kernel(gradient, other, before, out, other_out, sem):
+    copy = pltpu.make_async_copy(other, other_out, sem)
+    copy.start()
+    first = lax.axis_index(CORE) * 16
+    out[pl.ds(first, 16)] = before[...]
+    out[pl.ds(16 - first, 16)] = partial_of(gradient, other)
+    copy.wait()
 
 
 def square_kernel(projected, out):
@@ -93,7 +93,7 @@
 
 def final_kernel(
     squares, projected, own, state, right, left, across_a, across_b,
-    first, second, weights, factor, own_factor,
+    first, second, weights, mine, other, own_factor,
     update_out, weights_out, copies_out, first_out, second_out,
     update, new_weights, copies, new_first, new_second, normed, change, own_sems, sems,
 ):
@@ -104,7 +104,7 @@
 
     def blocks_of(j):
         across = across_a.at[j] if j < 4 else across_b.at[j - 4]
-        z = (place[0] + AWAY[j]) % 8
+        z = place[0] ^ AWAY[j]
         return [
             (z * 4 + (place[1] + 4 - i) % 4, block)
             for i, block in enumerate((state.at[j], right.at[j], across, left.at[j]))
@@ -130,6 +130,10 @@
                     m * 8 : (m + 1) * 8
                 ]
     values = normed[...].astype(BF)
+    side = lax.axis_index(CORE) * 128
+    sided = jnp.concatenate(
+        [normed[pl.ds(pl.multiple_of(at, 128), 128)] for at in (side, 128 - side)]
+    ).astype(BF)
     own_change = jnp.dot(own_factor[...], values, preferred_element_type=F32)
     for m in range(3):
         part = own_change[:, m * 128 : (m + 1) * 128]
@@ -147,10 +151,13 @@
     for copy in sent:
         copy.start()
     for q in range(4):
-        places = [(place[0] + AWAY[2 * q + k]) % 8 * 256 for k in range(2)]
-        chunks = [factor[pl.ds(pl.multiple_of(at, 256), 256)] for at in places]
+        places = [(place[0] ^ AWAY[2 * q + k]) * 256 for k in range(2)]
+        chunks = [
+            half[pl.ds(pl.multiple_of(at, 256), 256)] for half in (mine, other) for at in places
+        ]
         change[q % 2] = jnp.dot(
-            jnp.concatenate(chunks), values, preferred_element_type=F32
+            jnp.concatenate([jnp.concatenate(chunks[:2]), jnp.concatenate(chunks[2:])], axis=1),
+            sided, preferred_element_type=F32,
         )
         for k in range(2):
             for at, block in blocks[2 * q + k]:
@@ -176,45 +183,42 @@
     half, state = pl.pallas_call(
         head_kernel,
         out_shape=(
-            jax.ShapeDtypeStruct((8, 32, RANK), BF),
+            jax.ShapeDtypeStruct((32, 64, 128), BF),
             jax.ShapeDtypeStruct((1, 240, 128), BF),
         ),
         in_specs=[VMEM] * 4,
         out_specs=(VMEM, VMEM),
         compiler_params=pltpu.CompilerParams(vmem_limit_bytes=60 << 20),
     )(factor, weights, first_moment, second_moment)
-    half = lax.all_to_all(half, Z, split_axis=0, concat_axis=0, tiled=True)
-    half = sent_to_all(half, Y)
+    half = lax.all_to_all(half, FS, split_axis=0, concat_axis=0, tiled=True)
     other_half = moved(half, CORE, 1)
     state_z = gathered_z(state)
     states = gathered_y(state_z)
 
 
-    def gradient_of(part):
-        return (
-            jnp.einsum("mtc,td->mcd", cotangents, part, preferred_element_type=F32)
-            .astype(BF)
-            .reshape(384, -1)
-        )
-
-    gradient_a = gradient_of(inputs[:, :CUT])
-    gradient_b = gradient_of(inputs[:, CUT:])
-    partial_value, factor_all = pl.pallas_call(
-        partial_kernel,
-        out_shape=(
-            jax.ShapeDtypeStruct((32, 24, 128), BF),
-            jax.ShapeDtypeStruct((2048, RANK), BF),
-        ),
-        in_specs=[hbm, hbm, VMEM, VMEM],
+    gradient = (
+        jnp.einsum("mtc,td->mcd", cotangents, inputs, preferred_element_type=F32)
+        .astype(BF)
+        .reshape(384, 2048)
+    )
+    small = pltpu.CompilerParams(vmem_limit_bytes=8 << 20)
+    half_shape = jax.ShapeDtypeStruct((32, 64, 128), BF)
+    partial_first, mine = pl.pallas_call(
+        first_kernel,
+        out_shape=(jax.ShapeDtypeStruct((16, 24, 128), BF), half_shape),
+        in_specs=[VMEM] * 2,
         out_specs=(VMEM, hbm),
-        scratch_shapes=[
-            pltpu.VMEM((2048, RANK), BF),
-            pltpu.VMEM((384, CUT), BF),
-            pltpu.VMEM((384, 2048 - CUT), BF),
-            pltpu.SemaphoreType.DMA((3,)),
-        ],
-        compiler_params=pltpu.CompilerParams(vmem_limit_bytes=60 << 20),
-    )(gradient_a, gradient_b, half, other_half)
+        scratch_shapes=[pltpu.SemaphoreType.DMA],
+        compiler_params=small,
+    )(gradient, half)
+    partial_value, other = pl.pallas_call(
+        second_kernel,
+        out_shape=(jax.ShapeDtypeStruct((32, 24, 128), BF), half_shape),
+        in_specs=[VMEM] * 3,
+        out_specs=(VMEM, hbm),
+        scratch_shapes=[pltpu.SemaphoreType.DMA],
+        compiler_params=small,
+    )(gradient, other_half, partial_first)
     arrived = lax.all_to_all(partial_value, FS, split_axis=0, concat_axis=0, tiled=True)
     projected = arrived.astype(F32).sum(axis=0)
     projected_all = sent_to_all(projected.astype(BF), FS)
@@ -235,7 +239,7 @@
             jax.ShapeDtypeStruct((3, 8, 128), F32),
             jax.ShapeDtypeStruct((3, 8, 128), F32),
         ),
-        in_specs=[VMEM] * 13,
+        in_specs=[VMEM] * 14,
         out_specs=(hbm,) * 5,
         scratch_shapes=[
             pltpu.VMEM((3, 64, 128), F32),
@@ -251,7 +255,7 @@
         compiler_params=pltpu.CompilerParams(vmem_limit_bytes=24 << 20),
     )(
         squares, projected_all, projected, *states, first_moment, second_moment,
-        weights, factor_all, factor,
+        weights, mine.reshape(2048, 128), other.reshape(2048, 128), factor,
     )
 
 

time: 97.5 us -> 99.7 us (1.023)
  waiting for transfers between devices: 23.9 us -> 29.4 us
  matrix products: 9.83 us -> 6.85 us
  other arithmetic: 0.04 us -> 2.53 us
  Pallas kernels: 10.3 us -> 8.24 us
  starting transfers between devices: 46.9 us -> 45.8 us
    ppermute x0 -> x3, waiting for transfers between devices: none -> 12.1 us  [swapped(): return lax.ppermute(array, axis, [(i, i ^ bit) for i in range(size)])]
    all_to_all x1, waiting for transfers between devices: 6.3 us -> 0.01 us  [step(): half = lax.all_to_all(half, FS, split_axis=0, concat_axis=0, tiled=True)]
    ppermute x0 -> x3, starting transfers between devices: none -> 5.83 us  [swapped(): return lax.ppermute(array, axis, [(i, i ^ bit) for i in range(size)])]
    ppermute x9 -> x5, starting transfers between devices: 14.3 us -> 8.79 us  [moved(): lax.ppermute(array, axis, [(i, (i + shift) % size) for i in range(size)])]
    all_to_all x2 -> x1, starting transfers between devices: 8.43 us -> 4.12 us  [sent_to_all(): return lax.all_to_all(copies, axis, split_axis=0, concat_axis=0, tiled=True)]
    all_to_all x1, starting transfers between devices: 9 us -> 12 us  [step(): half = lax.all_to_all(half, FS, split_axis=0, concat_axis=0, tiled=True)]
    dot_general x2 -> x1, matrix products: 9.83 us -> 6.85 us  [step(): jnp.einsum('mtc,td->mcd', cotangents, inputs, preferred_element_type=F32)]
    pallas_call x2 -> x3, Pallas kernels: 6.02 us -> 4.01 us  [the longest x1 1.94 us: step(): pl.pallas_call(head_kernel, out_shape=(jax.ShapeDtypeStruct((32, 64, 128)...]
  transfers between devices with their start and end apart: 14 -> 12, of which waited for: 5 -> 5; matrix products, arithmetic and copies ran while one was open for 13% -> 13% of each run, Pallas kernels for 5% -> 3%
where the time goes in v7:
time: 99.7 us; the launch traced here: 99 us
  starting transfers between devices  45.8 us (46%)
  waiting for transfers between devices  29.4 us (29%)
  Pallas kernels  8.24 us (8%)
  matrix products  6.85 us (7%)
  local copies, waits for them, and re-layouts  5.25 us (5%)
  other arithmetic  2.53 us (3%)
    ppermute x3, waiting for transfers between devices, swapped(): return lax.ppermute(array, axis, [(i, i ^ bit) for i in range(size)])  12.1 us
    all_to_all x1, starting transfers between devices, step(): half = lax.all_to_all(half, FS, split_axis=0, concat_axis=0, tiled=True)  12 us
    ppermute x5, starting transfers between devices, moved(): lax.ppermute(array, axis, [(i, (i + shift) % size) for i in range(size)])  8.79 us
    all_to_all x1, starting transfers between devices, step(): lax.all_to_all(partial_value, FS, split_axis=0, concat_axis=0, tiled=True)  7.72 us
    all_to_all x1, starting transfers between devices, step(): lax.all_to_all(squares, TP, split_axis=0, concat_axis=0, tiled=True)  7.36 us
    dot_general x1, matrix products, step(): jnp.einsum('mtc,td->mcd', cotangents, inputs, preferred_element_type=F32)  6.85 us
    all_to_all x1, waiting for transfers between devices, step(): lax.all_to_all(partial_value, FS, split_axis=0, concat_axis=0, tiled=True)  6.79 us
    ppermute x3, starting transfers between devices, swapped(): return lax.ppermute(array, axis, [(i, i ^ bit) for i in range(size)])  5.83 us
  transfers between devices with their start and end apart: 12, of which 5 were waited for; matrix products, arithmetic and copies ran while one was open for 13% of the time, Pallas kernels for 3%

profile of v7, /device:TPU:1, one launch (start us, length us, event | category | flops | bytes accessed | tf_op | source)
XLA Modules:
  0.0 99.0 jit_solution(4631966497059983801)
XLA Ops:
  0.6 0.0 copy-start
  0.6 1.9 %shard_map.101 = (bf16[32,64,128]{2,1,0:T(8,128)(2,1)}, bf16[1,240,128]{2,1,0:T(8,128)(2,1)}) custom-call(bf16[64,256]{1,0:T(8,128)(2,1)} %own_factor.1, f32[3,64,128]{2,1,0:T(8,128)} %weights.3, f32[3,8,128]{2,1,0:T(8,128)} %first.3, f32[3,8,128]{2,1,0:T(8,128)} %second.3), custom_call_target="tpu_custom_call" | custom-call | tf_op jit(solution)/shard_map/pallas_call | solution.py:183
  2.6 12.0 %all-to-all-start = ((bf16[32,64,128]{2,1,0:T(8,128)(2,1)}), bf16[32,64,128]{2,1,0:T(8,128)(2,1)S(1)}, u32[]{:S(2)}, u32[]{:S(2)}) async-start(bf16[32,64,128]{2,1,0:T(8,128)(2,1)} %get-tuple-element.11), calls=%async_computation | async-start | bytes 1048576 | tf_op jit(solution)/shard_map/all_to_all | solution.py:193
  14.6 5.2 %collective-permute-start.1 = (bf16[1,240,128]{2,1,0:T(8,128)(2,1)}, bf16[1,240,128]{2,1,0:T(8,128)(2,1)S(1)}, u32[]{:S(2)}, u32[]{:S(2)}) collective-permute-start(bf16[1,240,128]{2,1,0:T(8,128)(2,1)} %get-tuple-element.14), channel_id=1, source_target_pairs={{0,128},{32,160},{64,192},{96,224},{128,0},{160,32},{192,64},{224,... | collective-permute-start | bytes 184328 | tf_op jit(solution)/shard_map/ppermute | solution.py:33
  19.9 12.1 %collective-permute-done.1 = bf16[1,240,128]{2,1,0:T(8,128)(2,1)S(1)} collective-permute-done((bf16[1,240,128]{2,1,0:T(8,128)(2,1)}, bf16[1,240,128]{2,1,0:T(8,128)(2,1)S(1)}, u32[]{:S(2)}, u32[]{:S(2)}) %collective-permute-start.1) | collective-permute-done | bytes 61472 | tf_op jit(solution)/shard_map/ppermute | solution.py:33
  31.9 0.8 pad_maximum_fusion.1
  32.8 0.6 collective-permute-start.2
  33.4 3.4 %collective-permute-start = (bf16[32,64,128]{2,1,0:T(8,128)(2,1)S(1)}, bf16[32,64,128]{2,1,0:T(8,128)(2,1)S(1)}, u32[]{:S(2)}, u32[]{:S(2)}) collective-permute-start(bf16[32,64,128]{2,1,0:T(8,128)(2,1)S(1)} %all-to-all-done.mine), channel_id=1, source_target_pairs={{0,1},{1,0},{2,3},{3,2},{4,5},{5,4},{6,7},{7,6},{8,9},{9,8},{10,11... | collective-permute-start | bytes 1572872 | tf_op jit(solution)/shard_map/ppermute | solution.py:28
  36.7 6.9 %fusion.2 = bf16[3,128,2048]{2,1,0:T(8,128)(2,1)S(1)} fusion(bf16[3,2048,128]{2,1,0:T(8,128)(2,1)S(1)} %copy-done, bf16[2048,2048]{1,0:T(8,128)(2,1)} %param.6), kind=kOutput, calls=%fused_computation.2 | convolution fusion | flops 3222011904 | bytes 11534336 | tf_op jit(solution)/shard_map/mtc,td->mcd/dot_general | solution.py:200
  43.6 0.7 pad_maximum_fusion
  44.4 0.7 shard_map.102
  45.1 1.4 %shard_map.103 = (bf16[32,24,128]{2,1,0:T(8,128)(2,1)}, bf16[32,64,128]{2,1,0:T(8,128)(2,1)S(1)}) custom-call(bf16[384,2048]{1,0:T(8,128)(2,1)S(1)} %bitcast.10, bf16[32,64,128]{2,1,0:T(8,128)(2,1)S(1)} %collective-permute-done.other, bf16[16,24,128]{2,1,0:T(8,128)(2,1)S(1)} %get-tuple-element.12.before), custom_call_target="tpu_custom_call" | custom-call | tf_op jit(solution)/shard_map/pallas_call | solution.py:214
  46.5 7.7 %all-to-all-start.1 = ((bf16[32,24,128]{2,1,0:T(8,128)(2,1)}), bf16[32,24,128]{2,1,0:T(8,128)(2,1)}, u32[]{:S(2)}, u32[]{:S(2)}) async-start(bf16[32,24,128]{2,1,0:T(8,128)(2,1)} %get-tuple-element.13), calls=%async_computation.1 | async-start | bytes 393216 | tf_op jit(solution)/shard_map/all_to_all | solution.py:222
  54.3 1.0 constant_dynamic-update-slice_fusion.state
  55.3 1.2 %collective-permute-start.4 = (bf16[8,240,128]{2,1,0:T(8,128)(2,1)S(1)}, bf16[8,240,128]{2,1,0:T(8,128)(2,1)S(1)}, u32[]{:S(2)}, u32[]{:S(2)}) collective-permute-start(bf16[8,240,128]{2,1,0:T(8,128)(2,1)S(1)} %constant_dynamic-update-slice_fusion.state), channel_id=1, source_target_pairs={{0,8},{8,16},{16,24},{24,0},{1,9},{9,17},{17,25},{25,1},{2,10},{10... | collective-permute-start | bytes 1474568 | tf_op jit(solution)/shard_map/ppermute | solution.py:28
  56.5 1.5 %collective-permute-start.5 = (bf16[8,240,128]{2,1,0:T(8,128)(2,1)S(1)}, bf16[8,240,128]{2,1,0:T(8,128)(2,1)S(1)}, u32[]{:S(2)}, u32[]{:S(2)}) collective-permute-start(bf16[8,240,128]{2,1,0:T(8,128)(2,1)S(1)} %constant_dynamic-update-slice_fusion.state), channel_id=1, source_target_pairs={{0,24},{8,0},{16,8},{24,16},{1,25},{9,1},{17,9},{25,17},{2,26},{10... | collective-permute-start | bytes 1474568 | tf_op jit(solution)/shard_map/ppermute | solution.py:28
  58.1 6.8 %all-to-all-done.1 = bf16[32,24,128]{2,1,0:T(8,128)(2,1)} async-done(((bf16[32,24,128]{2,1,0:T(8,128)(2,1)}), bf16[32,24,128]{2,1,0:T(8,128)(2,1)}, u32[]{:S(2)}, u32[]{:S(2)}) %all-to-all-start.1) | async-done | bytes 196640 | tf_op jit(solution)/shard_map/all_to_all | solution.py:222
  64.8 1.0 convert_reduce_fusion.own
  65.8 0.7 broadcast_in_dim.3
  66.5 4.1 %all-to-all-start.2 = ((bf16[32,24,128]{2,1,0:T(8,128)(2,1)}), bf16[32,24,128]{2,1,0:T(8,128)(2,1)S(1)}, u32[]{:S(2)}, u32[]{:S(2)}) async-start(bf16[32,24,128]{2,1,0:T(8,128)(2,1)} %broadcast_in_dim.3), calls=%async_computation.2 | async-start | bytes 393216 | tf_op jit(solution)/shard_map/all_to_all | solution.py:23
  70.6 0.2 collective-permute-done.4.right
  70.8 0.7 slice.8
  71.5 1.1 %collective-permute-start.6 = (bf16[4,240,128]{2,1,0:T(8,128)(2,1)}, bf16[4,240,128]{2,1,0:T(8,128)(2,1)}, u32[]{:S(2)}, u32[]{:S(2)}) collective-permute-start(bf16[4,240,128]{2,1,0:T(8,128)(2,1)} %slice.8), channel_id=1, source_target_pairs={{0,8},{8,16},{16,24},{24,0},{1,9},{9,17},{17,25},{25,1},{2,10},{10... | collective-permute-start | bytes 737288 | tf_op jit(solution)/shard_map/ppermute | solution.py:28
  72.6 0.7 slice.9
  73.3 1.6 %collective-permute-start.7 = (bf16[4,240,128]{2,1,0:T(8,128)(2,1)}, bf16[4,240,128]{2,1,0:T(8,128)(2,1)}, u32[]{:S(2)}, u32[]{:S(2)}) collective-permute-start(bf16[4,240,128]{2,1,0:T(8,128)(2,1)} %slice.9), channel_id=1, source_target_pairs={{0,24},{8,0},{16,8},{24,16},{1,25},{9,1},{17,9},{25,17},{2,26},{10... | collective-permute-start | bytes 737288 | tf_op jit(solution)/shard_map/ppermute | solution.py:28
  74.9 5.6 %all-to-all-done.2.projected = bf16[32,24,128]{2,1,0:T(8,128)(2,1)S(1)} async-done(((bf16[32,24,128]{2,1,0:T(8,128)(2,1)}), bf16[32,24,128]{2,1,0:T(8,128)(2,1)S(1)}, u32[]{:S(2)}, u32[]{:S(2)}) %all-to-all-start.2) | async-done | bytes 196640 | tf_op jit(solution)/shard_map/all_to_all | solution.py:23
  80.5 0.7 shard_map.104
  81.3 7.4 %all-to-all-start.3 = ((f32[8,8,128]{2,1,0:T(8,128)}), f32[8,8,128]{2,1,0:T(8,128)S(1)}, u32[]{:S(2)}, u32[]{:S(2)}) async-start(f32[8,8,128]{2,1,0:T(8,128)} %shard_map.104), calls=%async_computation.3 | async-start | bytes 65536 | tf_op jit(solution)/shard_map/all_to_all | solution.py:232
  88.6 4.7 %all-to-all-done.3.squares = f32[8,8,128]{2,1,0:T(8,128)S(1)} async-done(((f32[8,8,128]{2,1,0:T(8,128)}), f32[8,8,128]{2,1,0:T(8,128)S(1)}, u32[]{:S(2)}, u32[]{:S(2)}) %all-to-all-start.3) | async-done | bytes 32800 | tf_op jit(solution)/shard_map/all_to_all | solution.py:232
  93.4 1.0 %copy-done.2 = bf16[32,64,128]{2,1,0:T(8,128)(2,1)S(1)} copy-done((bf16[32,64,128]{2,1,0:T(8,128)(2,1)S(1)}, bf16[32,64,128]{2,1,0:T(8,128)(2,1)}, u32[]{:S(2)}) %copy-start.2) | copy-done | bytes 524312
  94.4 1.0 %copy-done.4 = bf16[32,64,128]{2,1,0:T(8,128)(2,1)S(1)} copy-done((bf16[32,64,128]{2,1,0:T(8,128)(2,1)S(1)}, bf16[32,64,128]{2,1,0:T(8,128)(2,1)}, u32[]{:S(2)}) %copy-start.4) | copy-done | bytes 524312
  95.4 3.5 %shard_map.105 = (f32[3,64,128]{2,1,0:T(8,128)}, f32[3,64,128]{2,1,0:T(8,128)}, bf16[3,2048,128]{2,1,0:T(8,128)(2,1)}, f32[3,8,128]{2,1,0:T(8,128)}, f32[3,8,128]{2,1,0:T(8,128)}) custom-call(f32[8,8,128]{2,1,0:T(8,128)S(1)} %all-to-all-done.3.squares, bf16[32,24,128]{2,1,0:T(8,128)(2,1)S(1)} %all-to-all-done.2.projected, ...), custom_call_target="tpu_custom_call" | custom-call | tf_op jit(solution)/shard_map/pallas_call | solution.py:233
  (29 shorter events, 0.1 us)
Async XLA Ops:
  0.6 36.1 %copy-start = (bf16[3,2048,128]{2,1,0:T(8,128)(2,1)S(1)}, bf16[3,2048,128]{2,1,0:T(8,128)(2,1)}, u32[]{:S(2)}) copy-start(bf16[3,2048,128]{2,1,0:T(8,128)(2,1)} %param.7) | copy-start | bytes 4718596
  2.6 30.8 %all-to-all-start = ((bf16[32,64,128]{2,1,0:T(8,128)(2,1)}), bf16[32,64,128]{2,1,0:T(8,128)(2,1)S(1)}, u32[]{:S(2)}, u32[]{:S(2)}) async-start(bf16[32,64,128]{2,1,0:T(8,128)(2,1)} %get-tuple-element.11), calls=%async_computation | async-start | bytes 1048576 | tf_op jit(solution)/shard_map/all_to_all | solution.py:193
  14.6 17.3 %collective-permute-start.1 = (bf16[1,240,128]{2,1,0:T(8,128)(2,1)}, bf16[1,240,128]{2,1,0:T(8,128)(2,1)S(1)}, u32[]{:S(2)}, u32[]{:S(2)}) collective-permute-start(bf16[1,240,128]{2,1,0:T(8,128)(2,1)} %get-tuple-element.14), channel_id=1, source_target_pairs={{0,128},{32,160},{64,192},{96,224},{128,0},{160,32},{192,64},{224,... | collective-permute-start | bytes 184328 | tf_op jit(solution)/shard_map/ppermute | solution.py:33
  32.8 10.8 %copy-start.9 = (bf16[1,240,128]{2,1,0:T(8,128)(2,1)S(1)}, bf16[1,240,128]{2,1,0:T(8,128)(2,1)}, u32[]{:S(2)}) copy-start(bf16[1,240,128]{2,1,0:T(8,128)(2,1)} %get-tuple-element.14) | copy-start | bytes 184324
  32.8 10.8 %collective-permute-start.2 = (bf16[2,240,128]{2,1,0:T(8,128)(2,1)S(1)}, bf16[2,240,128]{2,1,0:T(8,128)(2,1)S(1)}, u32[]{:S(2)}, u32[]{:S(2)}) collective-permute-start(bf16[2,240,128]{2,1,0:T(8,128)(2,1)S(1)} %pad_maximum_fusion.1), channel_id=1, source_target_pairs={{0,64},{32,96},{64,0},{96,32},{128,192},{160,224},{192,128},{224,1... | collective-permute-start | bytes 368648 | tf_op jit(solution)/shard_map/ppermute | solution.py:33
  33.4 11.7 %collective-permute-start = (bf16[32,64,128]{2,1,0:T(8,128)(2,1)S(1)}, bf16[32,64,128]{2,1,0:T(8,128)(2,1)S(1)}, u32[]{:S(2)}, u32[]{:S(2)}) collective-permute-start(bf16[32,64,128]{2,1,0:T(8,128)(2,1)S(1)} %all-to-all-done.mine), channel_id=1, source_target_pairs={{0,1},{1,0},{2,3},{3,2},{4,5},{5,4},{6,7},{7,6},{8,9},{9,8},{10,11... | collective-permute-start | bytes 1572872 | tf_op jit(solution)/shard_map/ppermute | solution.py:28
  44.3 9.9 %collective-permute-start.3 = (bf16[4,240,128]{2,1,0:T(8,128)(2,1)}, bf16[4,240,128]{2,1,0:T(8,128)(2,1)}, u32[]{:S(2)}, u32[]{:S(2)}) collective-permute-start(bf16[4,240,128]{2,1,0:T(8,128)(2,1)} %pad_maximum_fusion), channel_id=1, source_target_pairs={{0,32},{32,0},{64,96},{96,64},{128,160},{160,128},{192,224},{224,1... | collective-permute-start | bytes 737288 | tf_op jit(solution)/shard_map/ppermute | solution.py:33
  45.1 9.2 %copy-start.1 = (bf16[32,64,128]{2,1,0:T(8,128)(2,1)}, bf16[32,64,128]{2,1,0:T(8,128)(2,1)S(1)}, u32[]{:S(2)}) copy-start(bf16[32,64,128]{2,1,0:T(8,128)(2,1)S(1)} %get-tuple-element.15) | copy-start | bytes 1572868
  46.5 7.8 %copy-start.3 = (bf16[32,64,128]{2,1,0:T(8,128)(2,1)}, bf16[32,64,128]{2,1,0:T(8,128)(2,1)S(1)}, u32[]{:S(2)}) copy-start(bf16[32,64,128]{2,1,0:T(8,128)(2,1)S(1)} %get-tuple-element.16) | copy-start | bytes 1572868
  46.5 46.9 %copy-start.5 = (f32[3,64,128]{2,1,0:T(8,128)S(1)}, f32[3,64,128]{2,1,0:T(8,128)}, u32[]{:S(2)}) copy-start(f32[3,64,128]{2,1,0:T(8,128)} %weights.3) | copy-start | bytes 294916
  46.5 46.8 %copy-start.6 = (bf16[64,256]{1,0:T(8,128)(2,1)S(1)}, bf16[64,256]{1,0:T(8,128)(2,1)}, u32[]{:S(2)}) copy-start(bf16[64,256]{1,0:T(8,128)(2,1)} %own_factor.1) | copy-start | bytes 98308
  46.5 46.8 %copy-start.7 = (f32[3,8,128]{2,1,0:T(8,128)S(1)}, f32[3,8,128]{2,1,0:T(8,128)}, u32[]{:S(2)}) copy-start(f32[3,8,128]{2,1,0:T(8,128)} %first.3) | copy-start | bytes 36868
  46.5 46.8 %copy-start.8 = (f32[3,8,128]{2,1,0:T(8,128)S(1)}, f32[3,8,128]{2,1,0:T(8,128)}, u32[]{:S(2)}) copy-start(f32[3,8,128]{2,1,0:T(8,128)} %second.3) | copy-start | bytes 36868
  46.5 18.3 %all-to-all-start.1 = ((bf16[32,24,128]{2,1,0:T(8,128)(2,1)}), bf16[32,24,128]{2,1,0:T(8,128)(2,1)}, u32[]{:S(2)}, u32[]{:S(2)}) async-start(bf16[32,24,128]{2,1,0:T(8,128)(2,1)} %get-tuple-element.13), calls=%async_computation.1 | async-start | bytes 393216 | tf_op jit(solution)/shard_map/all_to_all | solution.py:222
  55.3 15.5 %collective-permute-start.4 = (bf16[8,240,128]{2,1,0:T(8,128)(2,1)S(1)}, bf16[8,240,128]{2,1,0:T(8,128)(2,1)S(1)}, u32[]{:S(2)}, u32[]{:S(2)}) collective-permute-start(bf16[8,240,128]{2,1,0:T(8,128)(2,1)S(1)} %constant_dynamic-update-slice_fusion.state), channel_id=1, source_target_pairs={{0,8},{8,16},{16,24},{24,0},{1,9},{9,17},{17,25},{25,1},{2,10},{10... | collective-permute-start | bytes 1474568 | tf_op jit(solution)/shard_map/ppermute | solution.py:28
  56.5 16.1 %collective-permute-start.5 = (bf16[8,240,128]{2,1,0:T(8,128)(2,1)S(1)}, bf16[8,240,128]{2,1,0:T(8,128)(2,1)S(1)}, u32[]{:S(2)}, u32[]{:S(2)}) collective-permute-start(bf16[8,240,128]{2,1,0:T(8,128)(2,1)S(1)} %constant_dynamic-update-slice_fusion.state), channel_id=1, source_target_pairs={{0,24},{8,0},{16,8},{24,16},{1,25},{9,1},{17,9},{25,17},{2,26},{10... | collective-permute-start | bytes 1474568 | tf_op jit(solution)/shard_map/ppermute | solution.py:28
  66.5 14.0 %all-to-all-start.2 = ((bf16[32,24,128]{2,1,0:T(8,128)(2,1)}), bf16[32,24,128]{2,1,0:T(8,128)(2,1)S(1)}, u32[]{:S(2)}, u32[]{:S(2)}) async-start(bf16[32,24,128]{2,1,0:T(8,128)(2,1)} %broadcast_in_dim.3), calls=%async_computation.2 | async-start | bytes 393216 | tf_op jit(solution)/shard_map/all_to_all | solution.py:23
  71.5 17.1 %collective-permute-start.6 = (bf16[4,240,128]{2,1,0:T(8,128)(2,1)}, bf16[4,240,128]{2,1,0:T(8,128)(2,1)}, u32[]{:S(2)}, u32[]{:S(2)}) collective-permute-start(bf16[4,240,128]{2,1,0:T(8,128)(2,1)} %slice.8), channel_id=1, source_target_pairs={{0,8},{8,16},{16,24},{24,0},{1,9},{9,17},{17,25},{25,1},{2,10},{10... | collective-permute-start | bytes 737288 | tf_op jit(solution)/shard_map/ppermute | solution.py:28
  73.3 15.3 %collective-permute-start.7 = (bf16[4,240,128]{2,1,0:T(8,128)(2,1)}, bf16[4,240,128]{2,1,0:T(8,128)(2,1)}, u32[]{:S(2)}, u32[]{:S(2)}) collective-permute-start(bf16[4,240,128]{2,1,0:T(8,128)(2,1)} %slice.9), channel_id=1, source_target_pairs={{0,24},{8,0},{16,8},{24,16},{1,25},{9,1},{17,9},{25,17},{2,26},{10... | collective-permute-start | bytes 737288 | tf_op jit(solution)/shard_map/ppermute | solution.py:28
  81.3 12.1 %all-to-all-start.3 = ((f32[8,8,128]{2,1,0:T(8,128)}), f32[8,8,128]{2,1,0:T(8,128)S(1)}, u32[]{:S(2)}, u32[]{:S(2)}) async-start(f32[8,8,128]{2,1,0:T(8,128)} %shard_map.104), calls=%async_computation.3 | async-start | bytes 65536 | tf_op jit(solution)/shard_map/all_to_all | solution.py:232
  93.4 1.0 %copy-start.2 = (bf16[32,64,128]{2,1,0:T(8,128)(2,1)S(1)}, bf16[32,64,128]{2,1,0:T(8,128)(2,1)}, u32[]{:S(2)}) copy-start(bf16[32,64,128]{2,1,0:T(8,128)(2,1)} %copy-done.1) | copy-start | bytes 1572868
  94.4 1.0 %copy-start.4 = (bf16[32,64,128]{2,1,0:T(8,128)(2,1)S(1)}, bf16[32,64,128]{2,1,0:T(8,128)(2,1)}, u32[]{:S(2)}) copy-start(bf16[32,64,128]{2,1,0:T(8,128)(2,1)} %copy-done.3) | copy-start | bytes 1572868

commit v8 on v7

--- a/solution.py
+++ b/solution.py
@@ -12,7 +12,8 @@
 FS = ("fs_0", "fs_1")
 TP = ("tp_0", "tp_1")
 CORE = "tp_1"
-AWAY = (0, 4, 2, 6, 1, 5, 3, 7)
+AWAY = (0, 7, 2, 5, 1, 6, 3, 4)
+CUT = 1024
 BF = jnp.bfloat16
 F32 = jnp.float32
 VMEM = pl.BlockSpec(memory_space=pltpu.VMEM)
@@ -34,7 +35,7 @@
 
 
 def gathered_z(array):
-    for bit in (4, 2, 1):
+    for bit in (7, 2, 1):
         array = jnp.concatenate([array, swapped(array, Z, bit)])
     return array
 
@@ -57,25 +58,27 @@
     state[0, 192:] = moments.astype(BF)
 
 
-def partial_of(gradient, half):
-    projected = jnp.dot(gradient[...], half[...].reshape(2048, 128), preferred_element_type=F32)
-    rows = [projected[m * 128 : (m + 1) * 128].T.reshape(16, 8, 128) for m in range(3)]
-    return jnp.concatenate(rows, axis=1).astype(BF)
-
-
-def first_kernel(gradient, mine, out, mine_out, sem):
+def partial_of(gradient_a, gradient_b, half):
+    rows = jnp.concatenate([half[:, z].reshape(256, 128) for z in range(8)])
+    projected = jnp.dot(gradient_a[...], rows[:CUT], preferred_element_type=F32)
+    projected += jnp.dot(gradient_b[...], rows[CUT:], preferred_element_type=F32)
+    parts = [projected[m * 128 : (m + 1) * 128].T.reshape(16, 8, 128) for m in range(3)]
+    return jnp.concatenate(parts, axis=1).astype(BF)
+
+
+def first_kernel(gradient_a, gradient_b, mine, out, mine_out, sem):
     copy = pltpu.make_async_copy(mine, mine_out, sem)
     copy.start()
-    out[...] = partial_of(gradient, mine)
+    out[...] = partial_of(gradient_a, gradient_b, mine)
     copy.wait()
 
 
-def second_kernel(gradient, other, before, out, other_out, sem):
+def second_kernel(gradient_a, gradient_b, other, before, out, other_out, sem):
     copy = pltpu.make_async_copy(other, other_out, sem)
     copy.start()
     first = lax.axis_index(CORE) * 16
     out[pl.ds(first, 16)] = before[...]
-    out[pl.ds(16 - first, 16)] = partial_of(gradient, other)
+    out[pl.ds(16 - first, 16)] = partial_of(gradient_a, gradient_b, other)
     copy.wait()
 
 
@@ -151,13 +154,12 @@
     for copy in sent:
         copy.start()
     for q in range(4):
-        places = [(place[0] ^ AWAY[2 * q + k]) * 256 for k in range(2)]
-        chunks = [
-            half[pl.ds(pl.multiple_of(at, 256), 256)] for half in (mine, other) for at in places
+        zs = [place[0] ^ AWAY[2 * q + k] for k in range(2)]
+        sides = [
+            jnp.concatenate([half[y, z] for z in zs for y in range(4)]) for half in (mine, other)
         ]
         change[q % 2] = jnp.dot(
-            jnp.concatenate([jnp.concatenate(chunks[:2]), jnp.concatenate(chunks[2:])], axis=1),
-            sided, preferred_element_type=F32,
+            jnp.concatenate(sides, axis=1), sided, preferred_element_type=F32
         )
         for k in range(2):
             for at, block in blocks[2 * q + k]:
@@ -167,7 +169,7 @@
                     before = block[m * 64 : (m + 1) * 64].astype(F32)
                     part = change[q % 2, inner, m * 128 : (m + 1) * 128]
                     copies[m, rows] = (before - 0.02 * part).astype(BF)
-            rows = pl.ds(pl.multiple_of(places[k], 256), 256)
+            rows = pl.ds(pl.multiple_of(zs[k] * 256, 256), 256)
             for m in range(3):
                 copy = pltpu.make_async_copy(
                     copies.at[m, rows], copies_out.at[m, rows], sems.at[2 * q + k, m]
@@ -183,42 +185,47 @@
     half, state = pl.pallas_call(
         head_kernel,
         out_shape=(
-            jax.ShapeDtypeStruct((32, 64, 128), BF),
+            jax.ShapeDtypeStruct((8, 64, 128), BF),
             jax.ShapeDtypeStruct((1, 240, 128), BF),
         ),
         in_specs=[VMEM] * 4,
         out_specs=(VMEM, VMEM),
         compiler_params=pltpu.CompilerParams(vmem_limit_bytes=60 << 20),
     )(factor, weights, first_moment, second_moment)
-    half = lax.all_to_all(half, FS, split_axis=0, concat_axis=0, tiled=True)
+    half = lax.all_to_all(half, Z, split_axis=0, concat_axis=0, tiled=True)
+    half = sent_to_all(half, Y)
     other_half = moved(half, CORE, 1)
     state_z = gathered_z(state)
     states = gathered_y(state_z)
 
 
-    gradient = (
-        jnp.einsum("mtc,td->mcd", cotangents, inputs, preferred_element_type=F32)
-        .astype(BF)
-        .reshape(384, 2048)
-    )
+    def gradient_of(part):
+        return (
+            jnp.einsum("mtc,td->mcd", cotangents, part, preferred_element_type=F32)
+            .astype(BF)
+            .reshape(384, -1)
+        )
+
+    gradient_a = gradient_of(inputs[:, :CUT])
+    gradient_b = gradient_of(inputs[:, CUT:])
     small = pltpu.CompilerParams(vmem_limit_bytes=8 << 20)
-    half_shape = jax.ShapeDtypeStruct((32, 64, 128), BF)
+    half_shape = jax.ShapeDtypeStruct((4, 8, 64, 128), BF)
     partial_first, mine = pl.pallas_call(
         first_kernel,
         out_shape=(jax.ShapeDtypeStruct((16, 24, 128), BF), half_shape),
-        in_specs=[VMEM] * 2,
-        out_specs=(VMEM, hbm),
-        scratch_shapes=[pltpu.SemaphoreType.DMA],
-        compiler_params=small,
-    )(gradient, half)
-    partial_value, other = pl.pallas_call(
-        second_kernel,
-        out_shape=(jax.ShapeDtypeStruct((32, 24, 128), BF), half_shape),
         in_specs=[VMEM] * 3,
         out_specs=(VMEM, hbm),
         scratch_shapes=[pltpu.SemaphoreType.DMA],
         compiler_params=small,
-    )(gradient, other_half, partial_first)
+    )(gradient_a, gradient_b, half)
+    partial_value, other = pl.pallas_call(
+        second_kernel,
+        out_shape=(jax.ShapeDtypeStruct((32, 24, 128), BF), half_shape),
+        in_specs=[VMEM] * 4,
+        out_specs=(VMEM, hbm),
+        scratch_shapes=[pltpu.SemaphoreType.DMA],
+        compiler_params=small,
+    )(gradient_a, gradient_b, other_half, partial_first)
     arrived = lax.all_to_all(partial_value, FS, split_axis=0, concat_axis=0, tiled=True)
     projected = arrived.astype(F32).sum(axis=0)
     projected_all = sent_to_all(projected.astype(BF), FS)
@@ -255,7 +262,7 @@
         compiler_params=pltpu.CompilerParams(vmem_limit_bytes=24 << 20),
     )(
         squares, projected_all, projected, *states, first_moment, second_moment,
-        weights, mine.reshape(2048, 128), other.reshape(2048, 128), factor,
+        weights, mine, other, factor,
     )
 
 

time: 99.7 us -> 94.2 us (0.945)
  waiting for transfers between devices: 29.4 us -> 25.1 us
  starting transfers between devices: 45.8 us -> 43.5 us
  local copies, waits for them, and re-layouts: 5.25 us -> 6.92 us
  matrix products: 6.85 us -> 8 us
    ppermute x3, waiting for transfers between devices: 12.1 us -> 0.01 us  [swapped(): return lax.ppermute(array, axis, [(i, i ^ bit) for i in range(size)])]
    all_to_all x1, waiting for transfers between devices: 0.01 us -> 5.08 us  [step(): half = lax.all_to_all(half, Z, split_axis=0, concat_axis=0, tiled=True)]
    all_to_all x1 -> x2, starting transfers between devices: 4.12 us -> 8.34 us  [sent_to_all(): return lax.all_to_all(copies, axis, split_axis=0, concat_axis=0, tiled=True)]
    all_to_all x1, starting transfers between devices: 12 us -> 9 us  [step(): half = lax.all_to_all(half, Z, split_axis=0, concat_axis=0, tiled=True)]
    all_to_all x1, starting transfers between devices: 7.72 us -> 4.71 us  [step(): lax.all_to_all(partial_value, FS, split_axis=0, concat_axis=0, tiled=True)]
    all_to_all x1 -> x2, waiting for transfers between devices: 5.61 us -> 8.34 us  [sent_to_all(): return lax.all_to_all(copies, axis, split_axis=0, concat_axis=0, tiled=True)]
    dot_general x1 -> x2, matrix products: 6.85 us -> 8 us  [gradient_of(): jnp.einsum('mtc,td->mcd', cotangents, part, preferred_element_type=F32)]
    unnamed x23 -> x29, local copies, waits for them, and re-layouts: 2.17 us -> 2.9 us
  transfers between devices with their start and end apart: 12 -> 13, of which waited for: 5 -> 6; matrix products, arithmetic and copies ran while one was open for 13% -> 15% of each run, Pallas kernels for 3% -> 2%
where the time goes in v8:
time: 94.2 us; the launch traced here: 93.5 us
  starting transfers between devices  43.5 us (46%)
  waiting for transfers between devices  25.1 us (27%)
  matrix products  8 us (8%)
  Pallas kernels  7.34 us (8%)
  local copies, waits for them, and re-layouts  6.92 us (7%)
  other arithmetic  1.73 us (2%)
    ppermute x5, starting transfers between devices, moved(): lax.ppermute(array, axis, [(i, (i + shift) % size) for i in range(size)])  9.15 us
    all_to_all x1, starting transfers between devices, step(): half = lax.all_to_all(half, Z, split_axis=0, concat_axis=0, tiled=True)  9 us
    all_to_all x2, starting transfers between devices, sent_to_all(): return lax.all_to_all(copies, axis, split_axis=0, concat_axis=0, tiled=True)  8.34 us
    all_to_all x2, waiting for transfers between devices, sent_to_all(): return lax.all_to_all(copies, axis, split_axis=0, concat_axis=0, tiled=True)  8.34 us
    dot_general x2, matrix products, gradient_of(): jnp.einsum('mtc,td->mcd', cotangents, part, preferred_element_type=F32)  8 us
    all_to_all x1, starting transfers between devices, step(): lax.all_to_all(squares, TP, split_axis=0, concat_axis=0, tiled=True)  7.43 us
    all_to_all x1, waiting for transfers between devices, step(): lax.all_to_all(partial_value, FS, split_axis=0, concat_axis=0, tiled=True)  6.78 us
    all_to_all x1, waiting for transfers between devices, step(): half = lax.all_to_all(half, Z, split_axis=0, concat_axis=0, tiled=True)  5.08 us
  transfers between devices with their start and end apart: 13, of which 6 were waited for; matrix products, arithmetic and copies ran while one was open for 15% of the time, Pallas kernels for 2%

profile of v8, /device:TPU:1, one launch (start us, length us, event | category | flops | bytes accessed | tf_op | source)
XLA Modules:
  0.0 93.5 jit_solution(10150853274478736934)
XLA Ops:
  0.6 1.7 %shard_map.101 = (bf16[8,64,128]{2,1,0:T(8,128)(2,1)}, bf16[1,240,128]{2,1,0:T(8,128)(2,1)}) custom-call(bf16[64,256]{1,0:T(8,128)(2,1)} %own_factor.1, f32[3,64,128]{2,1,0:T(8,128)} %weights.3, f32[3,8,128]{2,1,0:T(8,128)} %first.3, f32[3,8,128]{2,1,0:T(8,128)} %second.3), custom_call_target="tpu_custom_call" | custom-call | tf_op jit(solution)/shard_map/pallas_call | solution.py:185
  2.4 9.0 %all-to-all-start = ((bf16[8,64,128]{2,1,0:T(8,128)(2,1)}), bf16[8,64,128]{2,1,0:T(8,128)(2,1)S(1)}, u32[]{:S(2)}, u32[]{:S(2)}) async-start(bf16[8,64,128]{2,1,0:T(8,128)(2,1)} %get-tuple-element.11), calls=%async_computation | async-start | bytes 262144 | tf_op jit(solution)/shard_map/all_to_all | solution.py:195
  11.4 2.7 %collective-permute-start.1 = (bf16[1,240,128]{2,1,0:T(8,128)(2,1)}, bf16[1,240,128]{2,1,0:T(8,128)(2,1)S(1)}, u32[]{:S(2)}, u32[]{:S(2)}) collective-permute-start(bf16[1,240,128]{2,1,0:T(8,128)(2,1)} %get-tuple-element.14), channel_id=1, source_target_pairs={{0,224},{32,192},{64,160},{96,128},{128,96},{160,64},{192,32},{224... | collective-permute-start | bytes 184328 | tf_op jit(solution)/shard_map/ppermute | solution.py:34
  14.0 5.1 %all-to-all-done = bf16[8,64,128]{2,1,0:T(8,128)(2,1)S(1)} async-done(((bf16[8,64,128]{2,1,0:T(8,128)(2,1)}), bf16[8,64,128]{2,1,0:T(8,128)(2,1)S(1)}, u32[]{:S(2)}, u32[]{:S(2)}) %all-to-all-start) | async-done | bytes 131104 | tf_op jit(solution)/shard_map/all_to_all | solution.py:195
  19.1 0.9 broadcast_in_dim.6
  20.0 4.2 %all-to-all-start.1 = ((bf16[4,8,64,128]{3,2,1,0:T(8,128)(2,1)}), bf16[4,8,64,128]{3,2,1,0:T(8,128)(2,1)S(1)}, u32[]{:S(2)}, u32[]{:S(2)}) async-start(bf16[4,8,64,128]{3,2,1,0:T(8,128)(2,1)} %broadcast_in_dim.6), calls=%async_computation.1 | async-start | bytes 1048576 | tf_op jit(solution)/shard_map/all_to_all | solution.py:24
  24.2 4.0 %fusion.6 = bf16[3,128,1024]{2,1,0:T(8,128)(2,1)S(1)} fusion(bf16[3,2048,128]{2,1,0:T(8,128)(2,1)S(1)} %copy-done, bf16[2048,2048]{1,0:T(8,128)(2,1)} %param.6), kind=kOutput, calls=%fused_computation.6 | convolution fusion | flops 1611005952 | bytes 6553600 | tf_op jit(solution)/shard_map/mtc,td->mcd/dot_general | solution.py:204
  28.4 2.7 %all-to-all-done.1.mine = bf16[4,8,64,128]{3,2,1,0:T(8,128)(2,1)S(1)} async-done(((bf16[4,8,64,128]{3,2,1,0:T(8,128)(2,1)}), bf16[4,8,64,128]{3,2,1,0:T(8,128)(2,1)S(1)}, u32[]{:S(2)}, u32[]{:S(2)}) %all-to-all-start.1) | async-done | bytes 524320 | tf_op jit(solution)/shard_map/all_to_all | solution.py:24
  31.1 3.7 %collective-permute-start = (bf16[4,8,64,128]{3,2,1,0:T(8,128)(2,1)S(1)}, bf16[4,8,64,128]{3,2,1,0:T(8,128)(2,1)S(1)}, u32[]{:S(2)}, u32[]{:S(2)}) collective-permute-start(bf16[4,8,64,128]{3,2,1,0:T(8,128)(2,1)S(1)} %all-to-all-done.1.mine), channel_id=1, source_target_pairs={{0,1},{1,0},{2,3},{3,2},{4,5},{5,4},{6,7},{7,6},{8,9},{9,8},{10,11... | collective-permute-start | bytes 1572872 | tf_op jit(solution)/shard_map/ppermute | solution.py:29
  34.9 4.0 %fusion.9 = bf16[3,128,1024]{2,1,0:T(8,128)(2,1)S(1)} fusion(bf16[3,2048,128]{2,1,0:T(8,128)(2,1)S(1)} %copy-done, bf16[2048,2048]{1,0:T(8,128)(2,1)} %param.6), kind=kOutput, calls=%fused_computation.7 | convolution fusion | flops 1611005952 | bytes 6553600 | tf_op jit(solution)/shard_map/mtc,td->mcd/dot_general | solution.py:204
  38.9 0.7 pad_maximum_fusion
  39.6 2.1 %collective-permute-start.3 = (bf16[4,240,128]{2,1,0:T(8,128)(2,1)}, bf16[4,240,128]{2,1,0:T(8,128)(2,1)}, u32[]{:S(2)}, u32[]{:S(2)}) collective-permute-start(bf16[4,240,128]{2,1,0:T(8,128)(2,1)} %pad_maximum_fusion), channel_id=1, source_target_pairs={{0,32},{32,0},{64,96},{96,64},{128,160},{160,128},{192,224},{224,1... | collective-permute-start | bytes 737288 | tf_op jit(solution)/shard_map/ppermute | solution.py:34
  41.8 0.7 shard_map.102
  43.9 4.7 %all-to-all-start.2 = ((bf16[32,24,128]{2,1,0:T(8,128)(2,1)}), bf16[32,24,128]{2,1,0:T(8,128)(2,1)}, u32[]{:S(2)}, u32[]{:S(2)}) async-start(bf16[32,24,128]{2,1,0:T(8,128)(2,1)} %copy-done.6), calls=%async_computation.2 | async-start | bytes 393216 | tf_op jit(solution)/shard_map/all_to_all | solution.py:229
  48.7 1.0 %constant_dynamic-update-slice_fusion.state = bf16[8,240,128]{2,1,0:T(8,128)(2,1)S(1)} fusion(bf16[8,240,128]{2,1,0:T(8,128)(2,1)S(1)} %constant_dynamic-update-slice_fusion.1, bf16[4,240,128]{2,1,0:T(8,128)(2,1)} %collective-permute-done.3), kind=kLoop, calls=%fused_computation.11 | loop fusion | bytes 491520 | tf_op jit(solution)/shard_map/concatenate | solution.py:39
  49.7 1.1 %collective-permute-start.4 = (bf16[8,240,128]{2,1,0:T(8,128)(2,1)S(1)}, bf16[8,240,128]{2,1,0:T(8,128)(2,1)S(1)}, u32[]{:S(2)}, u32[]{:S(2)}) collective-permute-start(bf16[8,240,128]{2,1,0:T(8,128)(2,1)S(1)} %constant_dynamic-update-slice_fusion.state), channel_id=1, source_target_pairs={{0,8},{8,16},{16,24},{24,0},{1,9},{9,17},{17,25},{25,1},{2,10},{10... | collective-permute-start | bytes 1474568 | tf_op jit(solution)/shard_map/ppermute | solution.py:29
  50.8 1.6 %collective-permute-start.5 = (bf16[8,240,128]{2,1,0:T(8,128)(2,1)S(1)}, bf16[8,240,128]{2,1,0:T(8,128)(2,1)S(1)}, u32[]{:S(2)}, u32[]{:S(2)}) collective-permute-start(bf16[8,240,128]{2,1,0:T(8,128)(2,1)S(1)} %constant_dynamic-update-slice_fusion.state), channel_id=1, source_target_pairs={{0,24},{8,0},{16,8},{24,16},{1,25},{9,1},{17,9},{25,17},{2,26},{10... | collective-permute-start | bytes 1474568 | tf_op jit(solution)/shard_map/ppermute | solution.py:29
  52.5 6.8 %all-to-all-done.2 = bf16[32,24,128]{2,1,0:T(8,128)(2,1)} async-done(((bf16[32,24,128]{2,1,0:T(8,128)(2,1)}), bf16[32,24,128]{2,1,0:T(8,128)(2,1)}, u32[]{:S(2)}, u32[]{:S(2)}) %all-to-all-start.2) | async-done | bytes 196640 | tf_op jit(solution)/shard_map/all_to_all | solution.py:229
  59.2 1.0 %convert_reduce_fusion.own = f32[24,128]{1,0:T(8,128)S(1)} fusion(bf16[32,24,128]{2,1,0:T(8,128)(2,1)} %all-to-all-done.2), kind=kLoop, calls=%fused_computation.8 | loop fusion | flops 193536 | bytes 208896 | tf_op jit(solution)/shard_map/reduce_sum | solution.py:230
  60.2 0.7 broadcast_in_dim.7
  60.9 4.2 %all-to-all-start.3 = ((bf16[32,24,128]{2,1,0:T(8,128)(2,1)}), bf16[32,24,128]{2,1,0:T(8,128)(2,1)S(1)}, u32[]{:S(2)}, u32[]{:S(2)}) async-start(bf16[32,24,128]{2,1,0:T(8,128)(2,1)} %broadcast_in_dim.7), calls=%async_computation.3 | async-start | bytes 393216 | tf_op jit(solution)/shard_map/all_to_all | solution.py:24
  65.3 0.7 slice.16
  66.0 1.1 %collective-permute-start.6 = (bf16[4,240,128]{2,1,0:T(8,128)(2,1)}, bf16[4,240,128]{2,1,0:T(8,128)(2,1)}, u32[]{:S(2)}, u32[]{:S(2)}) collective-permute-start(bf16[4,240,128]{2,1,0:T(8,128)(2,1)} %slice.16), channel_id=1, source_target_pairs={{0,8},{8,16},{16,24},{24,0},{1,9},{9,17},{17,25},{25,1},{2,10},{10... | collective-permute-start | bytes 737288 | tf_op jit(solution)/shard_map/ppermute | solution.py:29
  67.0 0.7 slice.17
  67.8 1.6 %collective-permute-start.7 = (bf16[4,240,128]{2,1,0:T(8,128)(2,1)}, bf16[4,240,128]{2,1,0:T(8,128)(2,1)}, u32[]{:S(2)}, u32[]{:S(2)}) collective-permute-start(bf16[4,240,128]{2,1,0:T(8,128)(2,1)} %slice.17), channel_id=1, source_target_pairs={{0,24},{8,0},{16,8},{24,16},{1,25},{9,1},{17,9},{25,17},{2,26},{10... | collective-permute-start | bytes 737288 | tf_op jit(solution)/shard_map/ppermute | solution.py:29
  69.4 5.6 %all-to-all-done.3.projected = bf16[32,24,128]{2,1,0:T(8,128)(2,1)S(1)} async-done(((bf16[32,24,128]{2,1,0:T(8,128)(2,1)}), bf16[32,24,128]{2,1,0:T(8,128)(2,1)S(1)}, u32[]{:S(2)}, u32[]{:S(2)}) %all-to-all-start.3) | async-done | bytes 196640 | tf_op jit(solution)/shard_map/all_to_all | solution.py:24
  75.0 0.7 shard_map.104
  75.7 7.4 %all-to-all-start.4 = ((f32[8,8,128]{2,1,0:T(8,128)}), f32[8,8,128]{2,1,0:T(8,128)S(1)}, u32[]{:S(2)}, u32[]{:S(2)}) async-start(f32[8,8,128]{2,1,0:T(8,128)} %shard_map.104), calls=%async_computation.4 | async-start | bytes 65536 | tf_op jit(solution)/shard_map/all_to_all | solution.py:239
  83.1 4.7 %all-to-all-done.4.squares = f32[8,8,128]{2,1,0:T(8,128)S(1)} async-done(((f32[8,8,128]{2,1,0:T(8,128)}), f32[8,8,128]{2,1,0:T(8,128)S(1)}, u32[]{:S(2)}, u32[]{:S(2)}) %all-to-all-start.4) | async-done | bytes 32800 | tf_op jit(solution)/shard_map/all_to_all | solution.py:239
  87.9 1.0 %copy-done.2 = bf16[4,8,64,128]{3,2,1,0:T(8,128)(2,1)S(1)} copy-done((bf16[4,8,64,128]{3,2,1,0:T(8,128)(2,1)S(1)}, bf16[4,8,64,128]{3,2,1,0:T(8,128)(2,1)}, u32[]{:S(2)}) %copy-start.2) | copy-done | bytes 524312
  88.9 1.0 %copy-done.4 = bf16[4,8,64,128]{3,2,1,0:T(8,128)(2,1)S(1)} copy-done((bf16[4,8,64,128]{3,2,1,0:T(8,128)(2,1)S(1)}, bf16[4,8,64,128]{3,2,1,0:T(8,128)(2,1)}, u32[]{:S(2)}) %copy-start.4) | copy-done | bytes 524312
  89.9 3.5 %shard_map.105 = (f32[3,64,128]{2,1,0:T(8,128)}, f32[3,64,128]{2,1,0:T(8,128)}, bf16[3,2048,128]{2,1,0:T(8,128)(2,1)}, f32[3,8,128]{2,1,0:T(8,128)}, f32[3,8,128]{2,1,0:T(8,128)}) custom-call(f32[8,8,128]{2,1,0:T(8,128)S(1)} %all-to-all-done.4.squares, bf16[32,24,128]{2,1,0:T(8,128)(2,1)S(1)} %all-to-all-done.3.projected, ...), custom_call_target="tpu_custom_call" | custom-call | tf_op jit(solution)/shard_map/pallas_call | solution.py:240
  (39 shorter events, 1.9 us)
Async XLA Ops:
  0.6 23.6 %copy-start = (bf16[3,2048,128]{2,1,0:T(8,128)(2,1)S(1)}, bf16[3,2048,128]{2,1,0:T(8,128)(2,1)}, u32[]{:S(2)}) copy-start(bf16[3,2048,128]{2,1,0:T(8,128)(2,1)} %param.7) | copy-start | bytes 4718596
  2.4 16.8 %all-to-all-start = ((bf16[8,64,128]{2,1,0:T(8,128)(2,1)}), bf16[8,64,128]{2,1,0:T(8,128)(2,1)S(1)}, u32[]{:S(2)}, u32[]{:S(2)}) async-start(bf16[8,64,128]{2,1,0:T(8,128)(2,1)} %get-tuple-element.11), calls=%async_computation | async-start | bytes 262144 | tf_op jit(solution)/shard_map/all_to_all | solution.py:195
  11.4 16.9 %collective-permute-start.1 = (bf16[1,240,128]{2,1,0:T(8,128)(2,1)}, bf16[1,240,128]{2,1,0:T(8,128)(2,1)S(1)}, u32[]{:S(2)}, u32[]{:S(2)}) collective-permute-start(bf16[1,240,128]{2,1,0:T(8,128)(2,1)} %get-tuple-element.14), channel_id=1, source_target_pairs={{0,224},{32,192},{64,160},{96,128},{128,96},{160,64},{192,32},{224... | collective-permute-start | bytes 184328 | tf_op jit(solution)/shard_map/ppermute | solution.py:34
  20.0 11.1 %all-to-all-start.1 = ((bf16[4,8,64,128]{3,2,1,0:T(8,128)(2,1)}), bf16[4,8,64,128]{3,2,1,0:T(8,128)(2,1)S(1)}, u32[]{:S(2)}, u32[]{:S(2)}) async-start(bf16[4,8,64,128]{3,2,1,0:T(8,128)(2,1)} %broadcast_in_dim.6), calls=%async_computation.1 | async-start | bytes 1048576 | tf_op jit(solution)/shard_map/all_to_all | solution.py:24
  24.2 4.0 %copy-start.10 = (bf16[1,240,128]{2,1,0:T(8,128)(2,1)S(1)}, bf16[1,240,128]{2,1,0:T(8,128)(2,1)}, u32[]{:S(2)}) copy-start(bf16[1,240,128]{2,1,0:T(8,128)(2,1)} %get-tuple-element.14) | copy-start | bytes 184324
  28.3 10.6 %collective-permute-start.2 = (bf16[2,240,128]{2,1,0:T(8,128)(2,1)S(1)}, bf16[2,240,128]{2,1,0:T(8,128)(2,1)S(1)}, u32[]{:S(2)}, u32[]{:S(2)}) collective-permute-start(bf16[2,240,128]{2,1,0:T(8,128)(2,1)S(1)} %pad_maximum_fusion.1), channel_id=1, source_target_pairs={{0,64},{32,96},{64,0},{96,32},{128,192},{160,224},{192,128},{224,1... | collective-permute-start | bytes 368648 | tf_op jit(solution)/shard_map/ppermute | solution.py:34
  31.1 11.3 %collective-permute-start = (bf16[4,8,64,128]{3,2,1,0:T(8,128)(2,1)S(1)}, bf16[4,8,64,128]{3,2,1,0:T(8,128)(2,1)S(1)}, u32[]{:S(2)}, u32[]{:S(2)}) collective-permute-start(bf16[4,8,64,128]{3,2,1,0:T(8,128)(2,1)S(1)} %all-to-all-done.1.mine), channel_id=1, source_target_pairs={{0,1},{1,0},{2,3},{3,2},{4,5},{5,4},{6,7},{7,6},{8,9},{9,8},{10,11... | collective-permute-start | bytes 1572872 | tf_op jit(solution)/shard_map/ppermute | solution.py:29
  38.9 0.8 copy-start.11
  39.6 9.1 %collective-permute-start.3 = (bf16[4,240,128]{2,1,0:T(8,128)(2,1)}, bf16[4,240,128]{2,1,0:T(8,128)(2,1)}, u32[]{:S(2)}, u32[]{:S(2)}) collective-permute-start(bf16[4,240,128]{2,1,0:T(8,128)(2,1)} %pad_maximum_fusion), channel_id=1, source_target_pairs={{0,32},{32,0},{64,96},{96,64},{128,160},{160,128},{192,224},{224,1... | collective-permute-start | bytes 737288 | tf_op jit(solution)/shard_map/ppermute | solution.py:34
  42.5 0.8 copy-start.1
  42.5 6.2 %copy-start.12 = (bf16[2,240,128]{2,1,0:T(8,128)(2,1)S(1)}, bf16[2,240,128]{2,1,0:T(8,128)(2,1)}, u32[]{:S(2)}) copy-start(bf16[2,240,128]{2,1,0:T(8,128)(2,1)} %copy-done.11) | copy-start | bytes 368644
  43.2 0.7 copy-start.6
  43.9 5.8 %copy-start.3 = (bf16[4,8,64,128]{3,2,1,0:T(8,128)(2,1)}, bf16[4,8,64,128]{3,2,1,0:T(8,128)(2,1)S(1)}, u32[]{:S(2)}) copy-start(bf16[4,8,64,128]{3,2,1,0:T(8,128)(2,1)S(1)} %get-tuple-element.16.other) | copy-start | bytes 1572868
  43.9 43.9 %copy-start.5 = (f32[3,64,128]{2,1,0:T(8,128)S(1)}, f32[3,64,128]{2,1,0:T(8,128)}, u32[]{:S(2)}) copy-start(f32[3,64,128]{2,1,0:T(8,128)} %weights.3) | copy-start | bytes 294916
  43.9 43.9 %copy-start.7 = (bf16[64,256]{1,0:T(8,128)(2,1)S(1)}, bf16[64,256]{1,0:T(8,128)(2,1)}, u32[]{:S(2)}) copy-start(bf16[64,256]{1,0:T(8,128)(2,1)} %own_factor.1) | copy-start | bytes 98308
  43.9 43.9 %copy-start.8 = (f32[3,8,128]{2,1,0:T(8,128)S(1)}, f32[3,8,128]{2,1,0:T(8,128)}, u32[]{:S(2)}) copy-start(f32[3,8,128]{2,1,0:T(8,128)} %first.3) | copy-start | bytes 36868
  43.9 43.9 %copy-start.9 = (f32[3,8,128]{2,1,0:T(8,128)S(1)}, f32[3,8,128]{2,1,0:T(8,128)}, u32[]{:S(2)}) copy-start(f32[3,8,128]{2,1,0:T(8,128)} %second.3) | copy-start | bytes 36868
  43.9 15.3 %all-to-all-start.2 = ((bf16[32,24,128]{2,1,0:T(8,128)(2,1)}), bf16[32,24,128]{2,1,0:T(8,128)(2,1)}, u32[]{:S(2)}, u32[]{:S(2)}) async-start(bf16[32,24,128]{2,1,0:T(8,128)(2,1)} %copy-done.6), calls=%async_computation.2 | async-start | bytes 393216 | tf_op jit(solution)/shard_map/all_to_all | solution.py:229
  49.7 15.6 %collective-permute-start.4 = (bf16[8,240,128]{2,1,0:T(8,128)(2,1)S(1)}, bf16[8,240,128]{2,1,0:T(8,128)(2,1)S(1)}, u32[]{:S(2)}, u32[]{:S(2)}) collective-permute-start(bf16[8,240,128]{2,1,0:T(8,128)(2,1)S(1)} %constant_dynamic-update-slice_fusion.state), channel_id=1, source_target_pairs={{0,8},{8,16},{16,24},{24,0},{1,9},{9,17},{17,25},{25,1},{2,10},{10... | collective-permute-start | bytes 1474568 | tf_op jit(solution)/shard_map/ppermute | solution.py:29
  50.8 16.2 %collective-permute-start.5 = (bf16[8,240,128]{2,1,0:T(8,128)(2,1)S(1)}, bf16[8,240,128]{2,1,0:T(8,128)(2,1)S(1)}, u32[]{:S(2)}, u32[]{:S(2)}) collective-permute-start(bf16[8,240,128]{2,1,0:T(8,128)(2,1)S(1)} %constant_dynamic-update-slice_fusion.state), channel_id=1, source_target_pairs={{0,24},{8,0},{16,8},{24,16},{1,25},{9,1},{17,9},{25,17},{2,26},{10... | collective-permute-start | bytes 1474568 | tf_op jit(solution)/shard_map/ppermute | solution.py:29
  60.9 14.0 %all-to-all-start.3 = ((bf16[32,24,128]{2,1,0:T(8,128)(2,1)}), bf16[32,24,128]{2,1,0:T(8,128)(2,1)S(1)}, u32[]{:S(2)}, u32[]{:S(2)}) async-start(bf16[32,24,128]{2,1,0:T(8,128)(2,1)} %broadcast_in_dim.7), calls=%async_computation.3 | async-start | bytes 393216 | tf_op jit(solution)/shard_map/all_to_all | solution.py:24
  66.0 17.1 %collective-permute-start.6 = (bf16[4,240,128]{2,1,0:T(8,128)(2,1)}, bf16[4,240,128]{2,1,0:T(8,128)(2,1)}, u32[]{:S(2)}, u32[]{:S(2)}) collective-permute-start(bf16[4,240,128]{2,1,0:T(8,128)(2,1)} %slice.16), channel_id=1, source_target_pairs={{0,8},{8,16},{16,24},{24,0},{1,9},{9,17},{17,25},{25,1},{2,10},{10... | collective-permute-start | bytes 737288 | tf_op jit(solution)/shard_map/ppermute | solution.py:29
  67.8 15.4 %collective-permute-start.7 = (bf16[4,240,128]{2,1,0:T(8,128)(2,1)}, bf16[4,240,128]{2,1,0:T(8,128)(2,1)}, u32[]{:S(2)}, u32[]{:S(2)}) collective-permute-start(bf16[4,240,128]{2,1,0:T(8,128)(2,1)} %slice.17), channel_id=1, source_target_pairs={{0,24},{8,0},{16,8},{24,16},{1,25},{9,1},{17,9},{25,17},{2,26},{10... | collective-permute-start | bytes 737288 | tf_op jit(solution)/shard_map/ppermute | solution.py:29
  75.7 12.2 %all-to-all-start.4 = ((f32[8,8,128]{2,1,0:T(8,128)}), f32[8,8,128]{2,1,0:T(8,128)S(1)}, u32[]{:S(2)}, u32[]{:S(2)}) async-start(f32[8,8,128]{2,1,0:T(8,128)} %shard_map.104), calls=%async_computation.4 | async-start | bytes 65536 | tf_op jit(solution)/shard_map/all_to_all | solution.py:239
  87.9 1.0 %copy-start.2 = (bf16[4,8,64,128]{3,2,1,0:T(8,128)(2,1)S(1)}, bf16[4,8,64,128]{3,2,1,0:T(8,128)(2,1)}, u32[]{:S(2)}) copy-start(bf16[4,8,64,128]{3,2,1,0:T(8,128)(2,1)} %copy-done.1) | copy-start | bytes 1572868
  88.9 1.0 %copy-start.4 = (bf16[4,8,64,128]{3,2,1,0:T(8,128)(2,1)S(1)}, bf16[4,8,64,128]{3,2,1,0:T(8,128)(2,1)}, u32[]{:S(2)}) copy-start(bf16[4,8,64,128]{3,2,1,0:T(8,128)(2,1)} %copy-done.3) | copy-start | bytes 1572868

commit v9 on v8

--- a/solution.py
+++ b/solution.py
@@ -34,9 +34,24 @@
     return lax.ppermute(array, axis, [(i, i ^ bit) for i in range(size)])
 
 
+def join_kernel(a, b, out):
+    out[: a.shape[0]] = a[...]
+    out[a.shape[0] :] = b[...]
+
+
+def joined(a, b):
+    return pl.pallas_call(
+        join_kernel,
+        out_shape=jax.ShapeDtypeStruct((2 * a.shape[0], *a.shape[1:]), a.dtype),
+        in_specs=[VMEM] * 2,
+        out_specs=VMEM,
+        compiler_params=pltpu.CompilerParams(vmem_limit_bytes=4 << 20),
+    )(a, b)
+
+
 def gathered_z(array):
     for bit in (7, 2, 1):
-        array = jnp.concatenate([array, swapped(array, Z, bit)])
+        array = joined(array, swapped(array, Z, bit))
     return array
 
 
@@ -66,25 +81,19 @@
     return jnp.concatenate(parts, axis=1).astype(BF)
 
 
-def first_kernel(gradient_a, gradient_b, mine, out, mine_out, sem):
-    copy = pltpu.make_async_copy(mine, mine_out, sem)
-    copy.start()
+def first_kernel(gradient_a, gradient_b, mine, out):
     out[...] = partial_of(gradient_a, gradient_b, mine)
-    copy.wait()
-
-
-def second_kernel(gradient_a, gradient_b, other, before, out, other_out, sem):
-    copy = pltpu.make_async_copy(other, other_out, sem)
-    copy.start()
+
+
+def second_kernel(gradient_a, gradient_b, other, before, out):
     first = lax.axis_index(CORE) * 16
     out[pl.ds(first, 16)] = before[...]
     out[pl.ds(16 - first, 16)] = partial_of(gradient_a, gradient_b, other)
-    copy.wait()
 
 
 def square_kernel(projected, out):
     values = projected[...].astype(F32).reshape(96, 8, 128)
-    out[...] = jnp.broadcast_to(jnp.sum(values * values, axis=0), out.shape)
+    out[...] = jnp.sum(values * values, axis=0)
 
 
 def moments(clip, projected, first, second):
@@ -95,13 +104,14 @@
 
 
 def final_kernel(
-    squares, projected, own, state, right, left, across_a, across_b,
+    squares_0, squares_1, squares_2, squares_3, projected, own, state, right, left, across_a, across_b,
     first, second, weights, mine, other, own_factor,
     update_out, weights_out, copies_out, first_out, second_out,
     update, new_weights, copies, new_first, new_second, normed, change, own_sems, sems,
 ):
     place = (lax.axis_index(Z), lax.axis_index(Y))
-    total = jnp.sum(jnp.sum(squares[...], axis=0), keepdims=True)
+    squares = (squares_0[...] + squares_1[...]) + (squares_2[...] + squares_3[...])
+    total = jnp.sum(squares, keepdims=True)
     root_mean = jnp.sqrt(total / (3 * RANK * MW) + 1e-06)
     clip = jnp.minimum(1.0, 0.25 / root_mean)
 
@@ -184,10 +194,7 @@
     hbm = pl.BlockSpec(memory_space=pl.ANY)
     half, state = pl.pallas_call(
         head_kernel,
-        out_shape=(
-            jax.ShapeDtypeStruct((8, 64, 128), BF),
-            jax.ShapeDtypeStruct((1, 240, 128), BF),
-        ),
+        out_shape=(jax.ShapeDtypeStruct((8, 64, 128), BF), jax.ShapeDtypeStruct((1, 240, 128), BF)),
         in_specs=[VMEM] * 4,
         out_specs=(VMEM, VMEM),
         compiler_params=pltpu.CompilerParams(vmem_limit_bytes=60 << 20),
@@ -209,21 +216,18 @@
     gradient_a = gradient_of(inputs[:, :CUT])
     gradient_b = gradient_of(inputs[:, CUT:])
     small = pltpu.CompilerParams(vmem_limit_bytes=8 << 20)
-    half_shape = jax.ShapeDtypeStruct((4, 8, 64, 128), BF)
-    partial_first, mine = pl.pallas_call(
+    partial_first = pl.pallas_call(
         first_kernel,
-        out_shape=(jax.ShapeDtypeStruct((16, 24, 128), BF), half_shape),
+        out_shape=jax.ShapeDtypeStruct((16, 24, 128), BF),
         in_specs=[VMEM] * 3,
-        out_specs=(VMEM, hbm),
-        scratch_shapes=[pltpu.SemaphoreType.DMA],
+        out_specs=VMEM,
         compiler_params=small,
     )(gradient_a, gradient_b, half)
-    partial_value, other = pl.pallas_call(
+    partial_value = pl.pallas_call(
         second_kernel,
-        out_shape=(jax.ShapeDtypeStruct((32, 24, 128), BF), half_shape),
+        out_shape=jax.ShapeDtypeStruct((32, 24, 128), BF),
         in_specs=[VMEM] * 4,
-        out_specs=(VMEM, hbm),
-        scratch_shapes=[pltpu.SemaphoreType.DMA],
+        out_specs=VMEM,
         compiler_params=small,
     )(gradient_a, gradient_b, other_half, partial_first)
     arrived = lax.all_to_all(partial_value, FS, split_axis=0, concat_axis=0, tiled=True)
@@ -231,12 +235,13 @@
     projected_all = sent_to_all(projected.astype(BF), FS)
     squares = pl.pallas_call(
         square_kernel,
-        out_shape=jax.ShapeDtypeStruct((8, 8, 128), F32),
+        out_shape=jax.ShapeDtypeStruct((8, 128), F32),
         in_specs=[VMEM],
         out_specs=VMEM,
         compiler_params=pltpu.CompilerParams(vmem_limit_bytes=4 << 20),
     )(projected_all)
-    squares = lax.all_to_all(squares, TP, split_axis=0, concat_axis=0, tiled=True)
+    squares += swapped(squares, CORE, 1)
+    squares = [squares] + [swapped(squares, "tp_0", bit) for bit in (1, 2, 3)]
     return pl.pallas_call(
         final_kernel,
         out_shape=(
@@ -246,7 +251,7 @@
             jax.ShapeDtypeStruct((3, 8, 128), F32),
             jax.ShapeDtypeStruct((3, 8, 128), F32),
         ),
-        in_specs=[VMEM] * 14,
+        in_specs=[VMEM] * 17,
         out_specs=(hbm,) * 5,
         scratch_shapes=[
             pltpu.VMEM((3, 64, 128), F32),
@@ -261,8 +266,8 @@
         ],
         compiler_params=pltpu.CompilerParams(vmem_limit_bytes=24 << 20),
     )(
-        squares, projected_all, projected, *states, first_moment, second_moment,
-        weights, mine, other, factor,
+        *squares, projected_all, projected, *states, first_moment, second_moment,
+        weights, half, other_half, factor,
     )
 
 

time: 94.2 us -> 92.2 us (0.979)
  the two profiles are of different devices: /device:TPU:1 before, /device:TPU:32 now
where the time goes in v9:
time: 92.2 us; the launch traced here: 90.7 us
  starting transfers between devices  27.9 us (30%)
  waiting for transfers between devices  24.7 us (27%)
  blocking collectives  16.1 us (17%)
  Pallas kernels  7.63 us (8%)
  local copies, waits for them, and re-layouts  6.6 us (7%)
  matrix products  5.97 us (6%)
  other arithmetic  0.98 us (1%)
    all_to_all x1, blocking collectives, step(): half = lax.all_to_all(half, Z, split_axis=0, concat_axis=0, tiled=True)  16.1 us
    ppermute x7, waiting for transfers between devices, swapped(): return lax.ppermute(array, axis, [(i, i ^ bit) for i in range(size)])  13.6 us
    all_to_all x2, starting transfers between devices, sent_to_all(): return lax.all_to_all(copies, axis, split_axis=0, concat_axis=0, tiled=True)  8.89 us
    all_to_all x1, starting transfers between devices, step(): lax.all_to_all(partial_value, FS, split_axis=0, concat_axis=0, tiled=True)  7.64 us
    all_to_all x1, waiting for transfers between devices, step(): lax.all_to_all(partial_value, FS, split_axis=0, concat_axis=0, tiled=True)  6.77 us
    dot_general x2, matrix products, gradient_of(): jnp.einsum('mtc,td->mcd', cotangents, part, preferred_element_type=F32)  5.97 us
    ppermute x7, starting transfers between devices, swapped(): return lax.ppermute(array, axis, [(i, i ^ bit) for i in range(size)])  5.82 us
    ppermute x5, starting transfers between devices, moved(): lax.ppermute(array, axis, [(i, (i + shift) % size) for i in range(size)])  5.52 us
  transfers between devices with their start and end apart: 15, of which 7 were waited for; matrix products, arithmetic and copies ran while one was open for 12% of the time, Pallas kernels for 2%

profile of v9, /device:TPU:32, one launch (start us, length us, event | category | flops | bytes accessed | tf_op | source)
XLA Modules:
  0.0 90.7 jit_solution(13058351058554749394)
XLA Ops:
  0.6 1.7 %shard_map.101 = (bf16[8,64,128]{2,1,0:T(8,128)(2,1)}, bf16[1,240,128]{2,1,0:T(8,128)(2,1)}) custom-call(bf16[64,256]{1,0:T(8,128)(2,1)} %own_factor.1, f32[3,64,128]{2,1,0:T(8,128)} %weights.3, f32[3,8,128]{2,1,0:T(8,128)} %first.3, f32[3,8,128]{2,1,0:T(8,128)} %second.3), custom_call_target="tpu_custom_call" | custom-call | tf_op jit(solution)/shard_map/pallas_call | solution.py:195
  2.4 16.1 %all_to_all.20 = bf16[8,64,128]{2,1,0:T(8,128)(2,1)S(1)} all-to-all(bf16[8,64,128]{2,1,0:T(8,128)(2,1)} %get-tuple-element.7), channel_id=1, replica_groups=mesh['fs_0'=8,'fs_1'=4,'tp_0'=4,'tp_1'=2] {'fs_0'}, dimensions={0} | all-to-all | bytes 262144 | tf_op jit(solution)/shard_map/all_to_all | solution.py:202
  18.5 0.9 %broadcast_in_dim.6 = bf16[4,8,64,128]{3,2,1,0:T(8,128)(2,1)} broadcast(bf16[8,64,128]{2,1,0:T(8,128)(2,1)S(1)} %all_to_all.20), dimensions={1,2,3} | broadcast | bytes 655360 | tf_op jit(solution)/shard_map/broadcast_in_dim | solution.py:23
  19.4 4.5 %all-to-all-start.1 = ((bf16[4,8,64,128]{3,2,1,0:T(8,128)(2,1)}), bf16[4,8,64,128]{3,2,1,0:T(8,128)(2,1)S(1)}, u32[]{:S(2)}, u32[]{:S(2)}) async-start(bf16[4,8,64,128]{3,2,1,0:T(8,128)(2,1)} %broadcast_in_dim.6), calls=%async_computation.1 | async-start | bytes 1048576 | tf_op jit(solution)/shard_map/all_to_all | solution.py:24
  23.9 1.5 %collective-permute-start.5 = (bf16[1,240,128]{2,1,0:T(8,128)(2,1)S(1)}, bf16[1,240,128]{2,1,0:T(8,128)(2,1)S(1)}, u32[]{:S(2)}, u32[]{:S(2)}) collective-permute-start(bf16[1,240,128]{2,1,0:T(8,128)(2,1)S(1)} %copy-done.5), channel_id=1, source_target_pairs={{0,224},{32,192},{64,160},{96,128},{128,96},{160,64},{192,32},{224... | collective-permute-start | bytes 184328 | tf_op jit(solution)/shard_map/ppermute | solution.py:34
  25.3 7.1 %collective-permute-done.5.b = bf16[1,240,128]{2,1,0:T(8,128)(2,1)S(1)} collective-permute-done((bf16[1,240,128]{2,1,0:T(8,128)(2,1)S(1)}, bf16[1,240,128]{2,1,0:T(8,128)(2,1)S(1)}, u32[]{:S(2)}, u32[]{:S(2)}) %collective-permute-start.5) | collective-permute-done | bytes 61472 | tf_op jit(solution)/shard_map/ppermute | solution.py:34
  32.5 0.1 collective-permute-start.6
  32.7 4.1 %fusion.9 = bf16[3,128,1024]{2,1,0:T(8,128)(2,1)S(1)} fusion(bf16[3,2048,128]{2,1,0:T(8,128)(2,1)S(1)} %copy-done, bf16[2048,2048]{1,0:T(8,128)(2,1)} %param.6), kind=kOutput, calls=%fused_computation.7 | convolution fusion | flops 1611005952 | bytes 6553600 | tf_op jit(solution)/shard_map/mtc,td->mcd/dot_general | solution.py:211
  36.9 1.5 %collective-permute-done.6.b = bf16[2,240,128]{2,1,0:T(8,128)(2,1)S(1)} collective-permute-done((bf16[2,240,128]{2,1,0:T(8,128)(2,1)S(1)}, bf16[2,240,128]{2,1,0:T(8,128)(2,1)S(1)}, u32[]{:S(2)}, u32[]{:S(2)}) %collective-permute-start.6) | collective-permute-done | bytes 122912 | tf_op jit(solution)/shard_map/ppermute | solution.py:34
  38.5 1.8 %fusion.6 = bf16[3,128,1024]{2,1,0:T(8,128)(2,1)S(1)} fusion(bf16[3,2048,128]{2,1,0:T(8,128)(2,1)S(1)} %copy-done, bf16[2048,2048]{1,0:T(8,128)(2,1)S(1)} %copy-done.8), kind=kOutput, calls=%fused_computation.6 | convolution fusion | flops 1611005952 | bytes 6553600 | tf_op jit(solution)/shard_map/mtc,td->mcd/dot_general | solution.py:211
  40.3 0.6 shard_map.102.before
  41.0 1.3 %shard_map.103 = bf16[32,24,128]{2,1,0:T(8,128)(2,1)} custom-call(bf16[384,1024]{1,0:T(8,128)(2,1)S(1)} %bitcast.17, bf16[384,1024]{1,0:T(8,128)(2,1)S(1)} %bitcast.15, bf16[4,8,64,128]{3,2,1,0:T(8,128)(2,1)S(1)} %collective-permute-done.other, bf16[16,24,128]{2,1,0:T(8,128)(2,1)S(1)} %shard_map.102.before), custom_call_target="tpu_custom_call" | custom-call | tf_op jit(solution)/shard_map/pallas_call | solution.py:226
  42.3 7.6 %all-to-all-start.2 = ((bf16[32,24,128]{2,1,0:T(8,128)(2,1)}), bf16[32,24,128]{2,1,0:T(8,128)(2,1)}, u32[]{:S(2)}, u32[]{:S(2)}) async-start(bf16[32,24,128]{2,1,0:T(8,128)(2,1)} %shard_map.103), calls=%async_computation.2 | async-start | bytes 393216 | tf_op jit(solution)/shard_map/all_to_all | solution.py:233
  50.0 0.7 copy-done.2
  50.7 0.9 %copy-done.3 = bf16[4,240,128]{2,1,0:T(8,128)(2,1)S(1)} copy-done((bf16[4,240,128]{2,1,0:T(8,128)(2,1)S(1)}, bf16[4,240,128]{2,1,0:T(8,128)(2,1)}, u32[]{:S(2)}) %copy-start.3) | copy-done | bytes 245784
  51.7 2.8 %collective-permute-start.9 = (bf16[8,240,128]{2,1,0:T(8,128)(2,1)S(1)}, bf16[8,240,128]{2,1,0:T(8,128)(2,1)}, u32[]{:S(2)}, u32[]{:S(2)}) collective-permute-start(bf16[8,240,128]{2,1,0:T(8,128)(2,1)S(1)} %shard_map.107.state), channel_id=1, source_target_pairs={{0,24},{8,0},{16,8},{24,16},{1,25},{9,1},{17,9},{25,17},{2,26},{10... | collective-permute-start | bytes 1474568 | tf_op jit(solution)/shard_map/ppermute | solution.py:29
  54.4 6.8 %all-to-all-done.2 = bf16[32,24,128]{2,1,0:T(8,128)(2,1)} async-done(((bf16[32,24,128]{2,1,0:T(8,128)(2,1)}), bf16[32,24,128]{2,1,0:T(8,128)(2,1)}, u32[]{:S(2)}, u32[]{:S(2)}) %all-to-all-start.2) | async-done | bytes 196640 | tf_op jit(solution)/shard_map/all_to_all | solution.py:233
  61.2 1.0 %convert_reduce_fusion.own = f32[24,128]{1,0:T(8,128)S(1)} fusion(bf16[32,24,128]{2,1,0:T(8,128)(2,1)} %all-to-all-done.2), kind=kLoop, calls=%fused_computation.8 | loop fusion | flops 193536 | bytes 208896 | tf_op jit(solution)/shard_map/reduce_sum | solution.py:234
  62.2 0.7 broadcast_in_dim.7
  62.9 4.4 %all-to-all-start.3 = ((bf16[32,24,128]{2,1,0:T(8,128)(2,1)}), bf16[32,24,128]{2,1,0:T(8,128)(2,1)S(1)}, u32[]{:S(2)}, u32[]{:S(2)}) async-start(bf16[32,24,128]{2,1,0:T(8,128)(2,1)} %broadcast_in_dim.7), calls=%async_computation.3 | async-start | bytes 393216 | tf_op jit(solution)/shard_map/all_to_all | solution.py:24
  67.3 1.6 %slice.17 = bf16[4,240,128]{2,1,0:T(8,128)(2,1)} slice(bf16[8,240,128]{2,1,0:T(8,128)(2,1)} %collective-permute-done.9.left), slice={[4:8], [0:240], [0:128]} | slice | bytes 491520 | tf_op jit(solution)/shard_map/slice | solution.py:63
  69.0 2.7 %collective-permute-start.11 = (bf16[4,240,128]{2,1,0:T(8,128)(2,1)}, bf16[4,240,128]{2,1,0:T(8,128)(2,1)}, u32[]{:S(2)}, u32[]{:S(2)}) collective-permute-start(bf16[4,240,128]{2,1,0:T(8,128)(2,1)} %slice.17), channel_id=1, source_target_pairs={{0,24},{8,0},{16,8},{24,16},{1,25},{9,1},{17,9},{25,17},{2,26},{10... | collective-permute-start | bytes 737288 | tf_op jit(solution)/shard_map/ppermute | solution.py:29
  71.6 1.7 %slice.16 = bf16[4,240,128]{2,1,0:T(8,128)(2,1)} slice(bf16[8,240,128]{2,1,0:T(8,128)(2,1)} %collective-permute-done.8.right), slice={[0:4], [0:240], [0:128]} | slice | bytes 491520 | tf_op jit(solution)/shard_map/slice | solution.py:63
  73.3 4.2 %all-to-all-done.3.projected = bf16[32,24,128]{2,1,0:T(8,128)(2,1)S(1)} async-done(((bf16[32,24,128]{2,1,0:T(8,128)(2,1)}), bf16[32,24,128]{2,1,0:T(8,128)(2,1)S(1)}, u32[]{:S(2)}, u32[]{:S(2)}) %all-to-all-start.3) | async-done | bytes 196640 | tf_op jit(solution)/shard_map/all_to_all | solution.py:24
  77.6 0.1 shard_map.104
  77.8 1.2 %collective-permute-done.1 = f32[8,128]{1,0:T(8,128)S(1)} collective-permute-done((f32[8,128]{1,0:T(8,128)S(1)}, f32[8,128]{1,0:T(8,128)S(1)}, u32[]{:S(2)}, u32[]{:S(2)}) %collective-permute-start.1) | collective-permute-done | bytes 4128 | tf_op jit(solution)/shard_map/ppermute | solution.py:34
  78.9 2.8 %collective-permute-start.4 = (f32[8,128]{1,0:T(8,128)S(1)}, f32[8,128]{1,0:T(8,128)S(1)}, u32[]{:S(2)}, u32[]{:S(2)}) collective-permute-start(f32[8,128]{1,0:T(8,128)S(1)} %add.3.squares_0), channel_id=1, source_target_pairs={{0,6},{2,4},{4,2},{6,0},{1,7},{3,5},{5,3},{7,1},{8,14},{10,12},{12... | collective-permute-start | bytes 12296 | tf_op jit(solution)/shard_map/ppermute | solution.py:34
  81.7 0.7 collective-permute-start.3
  82.5 0.5 collective-permute-start.2
  83.0 0.7 collective-permute-done.4.squares_3
  83.7 3.1 %collective-permute-done.3.squares_2 = f32[8,128]{1,0:T(8,128)S(1)} collective-permute-done((f32[8,128]{1,0:T(8,128)S(1)}, f32[8,128]{1,0:T(8,128)S(1)}, u32[]{:S(2)}, u32[]{:S(2)}) %collective-permute-start.3) | collective-permute-done | bytes 4128 | tf_op jit(solution)/shard_map/ppermute | solution.py:34
  86.9 3.8 %shard_map.108 = (f32[3,64,128]{2,1,0:T(8,128)}, f32[3,64,128]{2,1,0:T(8,128)}, bf16[3,2048,128]{2,1,0:T(8,128)(2,1)}, f32[3,8,128]{2,1,0:T(8,128)}, f32[3,8,128]{2,1,0:T(8,128)}) custom-call(f32[8,128]{1,0:T(8,128)S(1)} %add.3.squares_0, f32[8,128]{1,0:T(8,128)S(1)} %collective-permute-done.2.squares_1, f32[8,128]{1,0:T(8,128)S(1)} %collective-permute-done.3.squares_2, ...), custom_call_target="tpu_custom_call" | custom-call | tf_op jit(solution)/shard_map/pallas_call | solution.py:245
  (34 shorter events, 0.4 us)
Async XLA Ops:
  0.6 32.1 %copy-start = (bf16[3,2048,128]{2,1,0:T(8,128)(2,1)S(1)}, bf16[3,2048,128]{2,1,0:T(8,128)(2,1)}, u32[]{:S(2)}) copy-start(bf16[3,2048,128]{2,1,0:T(8,128)(2,1)} %param.7) | copy-start | bytes 4718596
  2.4 21.5 %copy-start.5 = (bf16[1,240,128]{2,1,0:T(8,128)(2,1)S(1)}, bf16[1,240,128]{2,1,0:T(8,128)(2,1)}, u32[]{:S(2)}) copy-start(bf16[1,240,128]{2,1,0:T(8,128)(2,1)} %get-tuple-element.8.a) | copy-start | bytes 184324
  19.4 13.2 %all-to-all-start.1 = ((bf16[4,8,64,128]{3,2,1,0:T(8,128)(2,1)}), bf16[4,8,64,128]{3,2,1,0:T(8,128)(2,1)S(1)}, u32[]{:S(2)}, u32[]{:S(2)}) async-start(bf16[4,8,64,128]{3,2,1,0:T(8,128)(2,1)} %broadcast_in_dim.6), calls=%async_computation.1 | async-start | bytes 1048576 | tf_op jit(solution)/shard_map/all_to_all | solution.py:24
  23.9 8.6 %collective-permute-start.5 = (bf16[1,240,128]{2,1,0:T(8,128)(2,1)S(1)}, bf16[1,240,128]{2,1,0:T(8,128)(2,1)S(1)}, u32[]{:S(2)}, u32[]{:S(2)}) collective-permute-start(bf16[1,240,128]{2,1,0:T(8,128)(2,1)S(1)} %copy-done.5), channel_id=1, source_target_pairs={{0,224},{32,192},{64,160},{96,128},{128,96},{160,64},{192,32},{224... | collective-permute-start | bytes 184328 | tf_op jit(solution)/shard_map/ppermute | solution.py:34
  32.5 5.9 %collective-permute-start.6 = (bf16[2,240,128]{2,1,0:T(8,128)(2,1)S(1)}, bf16[2,240,128]{2,1,0:T(8,128)(2,1)S(1)}, u32[]{:S(2)}, u32[]{:S(2)}) collective-permute-start(bf16[2,240,128]{2,1,0:T(8,128)(2,1)S(1)} %shard_map.105.a), channel_id=1, source_target_pairs={{0,64},{32,96},{64,0},{96,32},{128,192},{160,224},{192,128},{224,1... | collective-permute-start | bytes 368648 | tf_op jit(solution)/shard_map/ppermute | solution.py:34
  32.6 5.9 %copy-start.8 = (bf16[2048,2048]{1,0:T(8,128)(2,1)S(1)}, bf16[2048,2048]{1,0:T(8,128)(2,1)}, u32[]{:S(2)}) copy-start(bf16[2048,2048]{1,0:T(8,128)(2,1)} %param.6) | copy-start | bytes 25165828
  32.6 8.4 %collective-permute-start = (bf16[4,8,64,128]{3,2,1,0:T(8,128)(2,1)S(1)}, bf16[4,8,64,128]{3,2,1,0:T(8,128)(2,1)S(1)}, u32[]{:S(2)}, u32[]{:S(2)}) collective-permute-start(bf16[4,8,64,128]{3,2,1,0:T(8,128)(2,1)S(1)} %all-to-all-done.1.mine), channel_id=1, source_target_pairs={{0,1},{1,0},{2,3},{3,2},{4,5},{5,4},{6,7},{7,6},{8,9},{9,8},{10,11... | collective-permute-start | bytes 1572872 | tf_op jit(solution)/shard_map/ppermute | solution.py:29
  38.4 11.6 %collective-permute-start.7 = (bf16[4,240,128]{2,1,0:T(8,128)(2,1)S(1)}, bf16[4,240,128]{2,1,0:T(8,128)(2,1)S(1)}, u32[]{:S(2)}, u32[]{:S(2)}) collective-permute-start(bf16[4,240,128]{2,1,0:T(8,128)(2,1)S(1)} %shard_map.106.a), channel_id=1, source_target_pairs={{0,32},{32,0},{64,96},{96,64},{128,160},{160,128},{192,224},{224,1... | collective-permute-start | bytes 737288 | tf_op jit(solution)/shard_map/ppermute | solution.py:34
  42.3 18.9 %all-to-all-start.2 = ((bf16[32,24,128]{2,1,0:T(8,128)(2,1)}), bf16[32,24,128]{2,1,0:T(8,128)(2,1)}, u32[]{:S(2)}, u32[]{:S(2)}) async-start(bf16[32,24,128]{2,1,0:T(8,128)(2,1)} %shard_map.103), calls=%async_computation.2 | async-start | bytes 393216 | tf_op jit(solution)/shard_map/all_to_all | solution.py:233
  50.0 36.9 %copy-start.1 = (f32[3,64,128]{2,1,0:T(8,128)S(1)}, f32[3,64,128]{2,1,0:T(8,128)}, u32[]{:S(2)}) copy-start(f32[3,64,128]{2,1,0:T(8,128)} %weights.3) | copy-start | bytes 294916
  50.0 0.7 copy-start.2
  50.7 0.9 %copy-start.3 = (bf16[4,240,128]{2,1,0:T(8,128)(2,1)S(1)}, bf16[4,240,128]{2,1,0:T(8,128)(2,1)}, u32[]{:S(2)}) copy-start(bf16[4,240,128]{2,1,0:T(8,128)(2,1)} %copy-done.2) | copy-start | bytes 737284
  51.6 35.2 %copy-start.4 = (bf16[64,256]{1,0:T(8,128)(2,1)S(1)}, bf16[64,256]{1,0:T(8,128)(2,1)}, u32[]{:S(2)}) copy-start(bf16[64,256]{1,0:T(8,128)(2,1)} %own_factor.1) | copy-start | bytes 98308
  51.6 35.2 %copy-start.6 = (f32[3,8,128]{2,1,0:T(8,128)S(1)}, f32[3,8,128]{2,1,0:T(8,128)}, u32[]{:S(2)}) copy-start(f32[3,8,128]{2,1,0:T(8,128)} %first.3) | copy-start | bytes 36868
  51.6 35.3 %copy-start.7 = (f32[3,8,128]{2,1,0:T(8,128)S(1)}, f32[3,8,128]{2,1,0:T(8,128)}, u32[]{:S(2)}) copy-start(f32[3,8,128]{2,1,0:T(8,128)} %second.3) | copy-start | bytes 36868
  51.7 15.6 %collective-permute-start.9 = (bf16[8,240,128]{2,1,0:T(8,128)(2,1)S(1)}, bf16[8,240,128]{2,1,0:T(8,128)(2,1)}, u32[]{:S(2)}, u32[]{:S(2)}) collective-permute-start(bf16[8,240,128]{2,1,0:T(8,128)(2,1)S(1)} %shard_map.107.state), channel_id=1, source_target_pairs={{0,24},{8,0},{16,8},{24,16},{1,25},{9,1},{17,9},{25,17},{2,26},{10... | collective-permute-start | bytes 1474568 | tf_op jit(solution)/shard_map/ppermute | solution.py:29
  54.4 17.2 %collective-permute-start.8 = (bf16[8,240,128]{2,1,0:T(8,128)(2,1)S(1)}, bf16[8,240,128]{2,1,0:T(8,128)(2,1)}, u32[]{:S(2)}, u32[]{:S(2)}) collective-permute-start(bf16[8,240,128]{2,1,0:T(8,128)(2,1)S(1)} %shard_map.107.state), channel_id=1, source_target_pairs={{0,8},{8,16},{16,24},{24,0},{1,9},{9,17},{17,25},{25,1},{2,10},{10... | collective-permute-start | bytes 1474568 | tf_op jit(solution)/shard_map/ppermute | solution.py:29
  62.9 14.7 %all-to-all-start.3 = ((bf16[32,24,128]{2,1,0:T(8,128)(2,1)}), bf16[32,24,128]{2,1,0:T(8,128)(2,1)S(1)}, u32[]{:S(2)}, u32[]{:S(2)}) async-start(bf16[32,24,128]{2,1,0:T(8,128)(2,1)} %broadcast_in_dim.7), calls=%async_computation.3 | async-start | bytes 393216 | tf_op jit(solution)/shard_map/all_to_all | solution.py:24
  69.0 14.0 %collective-permute-start.11 = (bf16[4,240,128]{2,1,0:T(8,128)(2,1)}, bf16[4,240,128]{2,1,0:T(8,128)(2,1)}, u32[]{:S(2)}, u32[]{:S(2)}) collective-permute-start(bf16[4,240,128]{2,1,0:T(8,128)(2,1)} %slice.17), channel_id=1, source_target_pairs={{0,24},{8,0},{16,8},{24,16},{1,25},{9,1},{17,9},{25,17},{2,26},{10... | collective-permute-start | bytes 737288 | tf_op jit(solution)/shard_map/ppermute | solution.py:29
  73.3 9.7 %collective-permute-start.10 = (bf16[4,240,128]{2,1,0:T(8,128)(2,1)}, bf16[4,240,128]{2,1,0:T(8,128)(2,1)}, u32[]{:S(2)}, u32[]{:S(2)}) collective-permute-start(bf16[4,240,128]{2,1,0:T(8,128)(2,1)} %slice.16), channel_id=1, source_target_pairs={{0,8},{8,16},{16,24},{24,0},{1,9},{9,17},{17,25},{25,1},{2,10},{10... | collective-permute-start | bytes 737288 | tf_op jit(solution)/shard_map/ppermute | solution.py:29
  77.7 1.2 %collective-permute-start.1 = (f32[8,128]{1,0:T(8,128)S(1)}, f32[8,128]{1,0:T(8,128)S(1)}, u32[]{:S(2)}, u32[]{:S(2)}) collective-permute-start(f32[8,128]{1,0:T(8,128)S(1)} %shard_map.104), channel_id=1, source_target_pairs={{0,1},{1,0},{2,3},{3,2},{4,5},{5,4},{6,7},{7,6},{8,9},{9,8},{10,11... | collective-permute-start | bytes 12296 | tf_op jit(solution)/shard_map/ppermute | solution.py:34
  78.9 4.8 %collective-permute-start.4 = (f32[8,128]{1,0:T(8,128)S(1)}, f32[8,128]{1,0:T(8,128)S(1)}, u32[]{:S(2)}, u32[]{:S(2)}) collective-permute-start(f32[8,128]{1,0:T(8,128)S(1)} %add.3.squares_0), channel_id=1, source_target_pairs={{0,6},{2,4},{4,2},{6,0},{1,7},{3,5},{5,3},{7,1},{8,14},{10,12},{12... | collective-permute-start | bytes 12296 | tf_op jit(solution)/shard_map/ppermute | solution.py:34
  81.7 5.1 %collective-permute-start.3 = (f32[8,128]{1,0:T(8,128)S(1)}, f32[8,128]{1,0:T(8,128)S(1)}, u32[]{:S(2)}, u32[]{:S(2)}) collective-permute-start(f32[8,128]{1,0:T(8,128)S(1)} %add.3.squares_0), channel_id=1, source_target_pairs={{0,4},{2,6},{4,0},{6,2},{1,5},{3,7},{5,1},{7,3},{8,12},{10,14},{12... | collective-permute-start | bytes 12296 | tf_op jit(solution)/shard_map/ppermute | solution.py:34
  82.5 4.4 %collective-permute-start.2 = (f32[8,128]{1,0:T(8,128)S(1)}, f32[8,128]{1,0:T(8,128)S(1)}, u32[]{:S(2)}, u32[]{:S(2)}) collective-permute-start(f32[8,128]{1,0:T(8,128)S(1)} %add.3.squares_0), channel_id=1, source_target_pairs={{0,2},{2,0},{4,6},{6,4},{1,3},{3,1},{5,7},{7,5},{8,10},{10,8},{12,... | collective-permute-start | bytes 12296 | tf_op jit(solution)/shard_map/ppermute | solution.py:34

commit v10 on v9

--- a/solution.py
+++ b/solution.py
@@ -50,18 +50,16 @@
 
 
 def gathered_z(array):
-    for bit in (7, 2, 1):
+    for bit in (7, 2):
         array = joined(array, swapped(array, Z, bit))
-    return array
-
-
-def gathered_y(array):
-    right = moved(array, Y, 1)
-    left = moved(array, Y, -1)
-    return (
-        array, right, left,
-        moved(right[:4], Y, 1), moved(left[4:], Y, -1),
-    )
+    return array, swapped(array, Z, 1)
+
+
+def gathered_y(a, b):
+    right, left = moved(a, Y, 1), moved(b, Y, -1)
+    other_right, other_left = moved(b, Y, 1), moved(a, Y, -1)
+    across = moved(right, Y, 1), moved(left, Y, -1)
+    return (a, right, across[0], other_left, b, other_right, across[1], left)
 
 
 def head_kernel(factor, weights, first, second, half, state):
@@ -104,11 +102,25 @@
 
 
 def final_kernel(
-    squares_0, squares_1, squares_2, squares_3, projected, own, state, right, left, across_a, across_b,
-    first, second, weights, mine, other, own_factor,
+    squares_0, squares_1, squares_2, squares_3, projected, own,
+    state_0, state_1, state_2, state_3, state_4, state_5, state_6, state_7,
+    first, second, weights, mine, other,
     update_out, weights_out, copies_out, first_out, second_out,
-    update, new_weights, copies, new_first, new_second, normed, change, own_sems, sems,
+    update, new_weights, copies, new_first, new_second, normed, change, held,
+    own_sems, sems, held_sems,
 ):
+    states = (state_0, state_1, state_2, state_3, state_4, state_5, state_6, state_7)
+    brought = [
+        [
+            pltpu.make_async_copy(
+                state.at[:, rows], held.at[k, :, rows], held_sems.at[k, part]
+            )
+            for k, state in enumerate(states)
+        ]
+        for part, rows in enumerate((pl.ds(192, 48), pl.ds(0, 192)))
+    ]
+    for copy in brought[0] + brought[1]:
+        copy.start()
     place = (lax.axis_index(Z), lax.axis_index(Y))
     squares = (squares_0[...] + squares_1[...]) + (squares_2[...] + squares_3[...])
     total = jnp.sum(squares, keepdims=True)
@@ -116,11 +128,9 @@
     clip = jnp.minimum(1.0, 0.25 / root_mean)
 
     def blocks_of(j):
-        across = across_a.at[j] if j < 4 else across_b.at[j - 4]
         z = place[0] ^ AWAY[j]
         return [
-            (z * 4 + (place[1] + 4 - i) % 4, block)
-            for i, block in enumerate((state.at[j], right.at[j], across, left.at[j]))
+            (z * 4 + (place[1] + 4 - i) % 4, held.at[j // 4 * 4 + i, j % 4]) for i in range(4)
         ]
 
     blocks = [blocks_of(j) for j in range(8)]
@@ -130,6 +140,8 @@
         )
         new_first[m] = own_first
         new_second[m] = own_second
+    for copy in brought[0]:
+        copy.wait()
     for j in range(8):
         for at, block in blocks[j]:
             _, _, values = moments(
@@ -142,12 +154,14 @@
                 normed[pl.ds(pl.multiple_of(at * 8, 8), 8), m * 128 : (m + 1) * 128] = values[
                     m * 8 : (m + 1) * 8
                 ]
-    values = normed[...].astype(BF)
     side = lax.axis_index(CORE) * 128
     sided = jnp.concatenate(
         [normed[pl.ds(pl.multiple_of(at, 128), 128)] for at in (side, 128 - side)]
     ).astype(BF)
-    own_change = jnp.dot(own_factor[...], values, preferred_element_type=F32)
+    own_rows = [half[place[1], place[0]] for half in (mine, other)]
+    own_change = jnp.dot(
+        jnp.concatenate(own_rows, axis=1), sided, preferred_element_type=F32
+    )
     for m in range(3):
         part = own_change[:, m * 128 : (m + 1) * 128]
         update[m] = part
@@ -163,6 +177,8 @@
     ]
     for copy in sent:
         copy.start()
+    for copy in brought[1]:
+        copy.wait()
     for q in range(4):
         zs = [place[0] ^ AWAY[2 * q + k] for k in range(2)]
         sides = [
@@ -202,8 +218,7 @@
     half = lax.all_to_all(half, Z, split_axis=0, concat_axis=0, tiled=True)
     half = sent_to_all(half, Y)
     other_half = moved(half, CORE, 1)
-    state_z = gathered_z(state)
-    states = gathered_y(state_z)
+    states = gathered_y(*gathered_z(state))
 
 
     def gradient_of(part):
@@ -251,7 +266,7 @@
             jax.ShapeDtypeStruct((3, 8, 128), F32),
             jax.ShapeDtypeStruct((3, 8, 128), F32),
         ),
-        in_specs=[VMEM] * 17,
+        in_specs=[VMEM] * 6 + [hbm] * 8 + [VMEM] * 5,
         out_specs=(hbm,) * 5,
         scratch_shapes=[
             pltpu.VMEM((3, 64, 128), F32),
@@ -261,13 +276,15 @@
             pltpu.VMEM((3, 8, 128), F32),
             pltpu.VMEM((RANK, 384), F32),
             pltpu.VMEM((2, 512, 384), F32),
+            pltpu.VMEM((8, 4, 240, 128), BF),
             pltpu.SemaphoreType.DMA((4,)),
             pltpu.SemaphoreType.DMA((8, 3)),
+            pltpu.SemaphoreType.DMA((8, 2)),
         ],
         compiler_params=pltpu.CompilerParams(vmem_limit_bytes=24 << 20),
     )(
         *squares, projected_all, projected, *states, first_moment, second_moment,
-        weights, half, other_half, factor,
+        weights, half, other_half,
     )
 
 

time: 92.2 us -> 102 us (1.11)
  starting transfers between devices: 27.9 us -> 39.8 us
  local copies, waits for them, and re-layouts: 6.6 us -> 2.13 us
  waiting for transfers between devices: 24.7 us -> 26.9 us
    all_to_all x1, waiting for transfers between devices: 6.77 us -> 0.01 us  [step(): lax.all_to_all(partial_value, FS, split_axis=0, concat_axis=0, tiled=True)]
    all_to_all x2, waiting for transfers between devices: 4.25 us -> 11 us  [sent_to_all(): return lax.all_to_all(copies, axis, split_axis=0, concat_axis=0, tiled=True)]
    ppermute x7, starting transfers between devices: 5.82 us -> 11.6 us  [swapped(): return lax.ppermute(array, axis, [(i, i ^ bit) for i in range(size)])]
    ppermute x5 -> x7, starting transfers between devices: 5.52 us -> 10.3 us  [moved(): lax.ppermute(array, axis, [(i, (i + shift) % size) for i in range(size)])]
    slice x2 -> x0, local copies, waits for them, and re-layouts: 3.3 us -> none  [gathered_y(): return (array, right, left, moved(right[:4], Y, 1), moved(left[4:], Y, -1))]
    all_to_all x2, starting transfers between devices: 8.89 us -> 12.1 us  [sent_to_all(): return lax.all_to_all(copies, axis, split_axis=0, concat_axis=0, tiled=True)]
    all_to_all x1, starting transfers between devices: 7.64 us -> 5.82 us  [step(): lax.all_to_all(partial_value, FS, split_axis=0, concat_axis=0, tiled=True)]
    ppermute x7, waiting for transfers between devices: 13.6 us -> 15.3 us  [swapped(): return lax.ppermute(array, axis, [(i, i ^ bit) for i in range(size)])]
  transfers between devices with their start and end apart: 15 -> 17, of which waited for: 7 -> 7; matrix products, arithmetic and copies ran while one was open for 12% -> 8% of each run, Pallas kernels for 2% -> 2%
where the time goes in v10:
time: 102 us; the launch traced here: 100 us
  starting transfers between devices  39.8 us (39%)
  waiting for transfers between devices  26.9 us (26%)
  blocking collectives  16.1 us (16%)
  Pallas kernels  7.4 us (7%)
  matrix products  5.96 us (6%)
  local copies, waits for them, and re-layouts  2.13 us (2%)
    all_to_all x1, blocking collectives, step(): half = lax.all_to_all(half, Z, split_axis=0, concat_axis=0, tiled=True)  16.1 us
    ppermute x7, waiting for transfers between devices, swapped(): return lax.ppermute(array, axis, [(i, i ^ bit) for i in range(size)])  15.3 us
    all_to_all x2, starting transfers between devices, sent_to_all(): return lax.all_to_all(copies, axis, split_axis=0, concat_axis=0, tiled=True)  12.1 us
    ppermute x7, starting transfers between devices, swapped(): return lax.ppermute(array, axis, [(i, i ^ bit) for i in range(size)])  11.6 us
    all_to_all x2, waiting for transfers between devices, sent_to_all(): return lax.all_to_all(copies, axis, split_axis=0, concat_axis=0, tiled=True)  11 us
    ppermute x7, starting transfers between devices, moved(): lax.ppermute(array, axis, [(i, (i + shift) % size) for i in range(size)])  10.3 us
    dot_general x2, matrix products, gradient_of(): jnp.einsum('mtc,td->mcd', cotangents, part, preferred_element_type=F32)  5.96 us
    all_to_all x1, starting transfers between devices, step(): lax.all_to_all(partial_value, FS, split_axis=0, concat_axis=0, tiled=True)  5.82 us
  transfers between devices with their start and end apart: 17, of which 7 were waited for; matrix products, arithmetic and copies ran while one was open for 8% of the time, Pallas kernels for 2%

profile of v10, /device:TPU:32, one launch (start us, length us, event | category | flops | bytes accessed | tf_op | source)
XLA Modules:
  0.0 100.2 jit_solution(16099304896559951518)
XLA Ops:
  0.6 1.7 %shard_map.101 = (bf16[8,64,128]{2,1,0:T(8,128)(2,1)}, bf16[1,240,128]{2,1,0:T(8,128)(2,1)}) custom-call(bf16[64,256]{1,0:T(8,128)(2,1)} %factor.1, f32[3,64,128]{2,1,0:T(8,128)} %weights.3, f32[3,8,128]{2,1,0:T(8,128)} %first.3, f32[3,8,128]{2,1,0:T(8,128)} %second.3), custom_call_target="tpu_custom_call" | custom-call | tf_op jit(solution)/shard_map/pallas_call | solution.py:211
  2.4 16.1 %all_to_all.20 = bf16[8,64,128]{2,1,0:T(8,128)(2,1)S(1)} all-to-all(bf16[8,64,128]{2,1,0:T(8,128)(2,1)} %get-tuple-element.7), channel_id=1, replica_groups=mesh['fs_0'=8,'fs_1'=4,'tp_0'=4,'tp_1'=2] {'fs_0'}, dimensions={0} | all-to-all | bytes 262144 | tf_op jit(solution)/shard_map/all_to_all | solution.py:218
  18.5 0.9 broadcast_in_dim.6
  19.4 4.5 %all-to-all-start.1 = ((bf16[4,8,64,128]{3,2,1,0:T(8,128)(2,1)}), bf16[4,8,64,128]{3,2,1,0:T(8,128)(2,1)S(1)}, u32[]{:S(2)}, u32[]{:S(2)}) async-start(bf16[4,8,64,128]{3,2,1,0:T(8,128)(2,1)} %broadcast_in_dim.6), calls=%async_computation.1 | async-start | bytes 1048576 | tf_op jit(solution)/shard_map/all_to_all | solution.py:24
  23.9 1.5 %collective-permute-start.5 = (bf16[1,240,128]{2,1,0:T(8,128)(2,1)S(1)}, bf16[1,240,128]{2,1,0:T(8,128)(2,1)S(1)}, u32[]{:S(2)}, u32[]{:S(2)}) collective-permute-start(bf16[1,240,128]{2,1,0:T(8,128)(2,1)S(1)} %copy-done.2), channel_id=1, source_target_pairs={{0,224},{32,192},{64,160},{96,128},{128,96},{160,64},{192,32},{224... | collective-permute-start | bytes 184328 | tf_op jit(solution)/shard_map/ppermute | solution.py:34
  25.3 6.8 %all-to-all-done.1.mine = bf16[4,8,64,128]{3,2,1,0:T(8,128)(2,1)S(1)} async-done(((bf16[4,8,64,128]{3,2,1,0:T(8,128)(2,1)}), bf16[4,8,64,128]{3,2,1,0:T(8,128)(2,1)S(1)}, u32[]{:S(2)}, u32[]{:S(2)}) %all-to-all-start.1) | async-done | bytes 524320 | tf_op jit(solution)/shard_map/all_to_all | solution.py:24
  32.1 4.1 %fusion.9 = bf16[3,128,1024]{2,1,0:T(8,128)(2,1)S(1)} fusion(bf16[3,2048,128]{2,1,0:T(8,128)(2,1)S(1)} %copy-done, bf16[2048,2048]{1,0:T(8,128)(2,1)} %param.6), kind=kOutput, calls=%fused_computation.7 | convolution fusion | flops 1611005952 | bytes 6553600 | tf_op jit(solution)/shard_map/mtc,td->mcd/dot_general | solution.py:226
  36.3 0.5 copy-done.5
  36.7 1.8 %fusion.6 = bf16[3,128,1024]{2,1,0:T(8,128)(2,1)S(1)} fusion(bf16[3,2048,128]{2,1,0:T(8,128)(2,1)S(1)} %copy-done, bf16[2048,2048]{1,0:T(8,128)(2,1)S(1)} %copy-done.5), kind=kOutput, calls=%fused_computation.6 | convolution fusion | flops 1611005952 | bytes 6553600 | tf_op jit(solution)/shard_map/mtc,td->mcd/dot_general | solution.py:226
  38.6 0.6 shard_map.102.before
  39.2 1.3 %shard_map.103 = bf16[32,24,128]{2,1,0:T(8,128)(2,1)} custom-call(bf16[384,1024]{1,0:T(8,128)(2,1)S(1)} %bitcast.17, bf16[384,1024]{1,0:T(8,128)(2,1)S(1)} %bitcast.15, bf16[4,8,64,128]{3,2,1,0:T(8,128)(2,1)S(1)} %collective-permute-done.other, bf16[16,24,128]{2,1,0:T(8,128)(2,1)S(1)} %shard_map.102.before), custom_call_target="tpu_custom_call" | custom-call | tf_op jit(solution)/shard_map/pallas_call | solution.py:241
  40.6 5.8 %all-to-all-start.2 = ((bf16[32,24,128]{2,1,0:T(8,128)(2,1)}), bf16[32,24,128]{2,1,0:T(8,128)(2,1)}, u32[]{:S(2)}, u32[]{:S(2)}) async-start(bf16[32,24,128]{2,1,0:T(8,128)(2,1)} %shard_map.103), calls=%async_computation.2 | async-start | bytes 393216 | tf_op jit(solution)/shard_map/all_to_all | solution.py:248
  46.4 2.5 %collective-permute-start.6 = (bf16[2,240,128]{2,1,0:T(8,128)(2,1)S(1)}, bf16[2,240,128]{2,1,0:T(8,128)(2,1)S(1)}, u32[]{:S(2)}, u32[]{:S(2)}) collective-permute-start(bf16[2,240,128]{2,1,0:T(8,128)(2,1)S(1)} %shard_map.105.a), channel_id=1, source_target_pairs={{0,64},{32,96},{64,0},{96,32},{128,192},{160,224},{192,128},{224,1... | collective-permute-start | bytes 368648 | tf_op jit(solution)/shard_map/ppermute | solution.py:34
  48.9 7.2 %collective-permute-done.6.b = bf16[2,240,128]{2,1,0:T(8,128)(2,1)S(1)} collective-permute-done((bf16[2,240,128]{2,1,0:T(8,128)(2,1)S(1)}, bf16[2,240,128]{2,1,0:T(8,128)(2,1)S(1)}, u32[]{:S(2)}, u32[]{:S(2)}) %collective-permute-start.6) | collective-permute-done | bytes 122912 | tf_op jit(solution)/shard_map/ppermute | solution.py:34
  56.2 3.3 %collective-permute-start.10 = (bf16[4,240,128]{2,1,0:T(8,128)(2,1)S(1)}, bf16[4,240,128]{2,1,0:T(8,128)(2,1)S(1)}, u32[]{:S(2)}, u32[]{:S(2)}) collective-permute-start(bf16[4,240,128]{2,1,0:T(8,128)(2,1)S(1)} %shard_map.106.state_0), channel_id=1, source_target_pairs={{0,32},{32,0},{64,96},{96,64},{128,160},{160,128},{192,224},{224,1... | collective-permute-start | bytes 737288 | tf_op jit(solution)/shard_map/ppermute | solution.py:34
  59.4 1.5 %collective-permute-start.7 = (bf16[4,240,128]{2,1,0:T(8,128)(2,1)S(1)}, bf16[4,240,128]{2,1,0:T(8,128)(2,1)}, u32[]{:S(2)}, u32[]{:S(2)}) collective-permute-start(bf16[4,240,128]{2,1,0:T(8,128)(2,1)S(1)} %shard_map.106.state_0), channel_id=1, source_target_pairs={{0,8},{8,16},{16,24},{24,0},{1,9},{9,17},{17,25},{25,1},{2,10},{10... | collective-permute-start | bytes 737288 | tf_op jit(solution)/shard_map/ppermute | solution.py:29
  60.9 3.8 %collective-permute-done.10.state_4 = bf16[4,240,128]{2,1,0:T(8,128)(2,1)S(1)} collective-permute-done((bf16[4,240,128]{2,1,0:T(8,128)(2,1)S(1)}, bf16[4,240,128]{2,1,0:T(8,128)(2,1)S(1)}, u32[]{:S(2)}, u32[]{:S(2)}) %collective-permute-start.10) | collective-permute-done | bytes 245792 | tf_op jit(solution)/shard_map/ppermute | solution.py:34
  64.7 2.7 %collective-permute-start.12 = (bf16[4,240,128]{2,1,0:T(8,128)(2,1)S(1)}, bf16[4,240,128]{2,1,0:T(8,128)(2,1)}, u32[]{:S(2)}, u32[]{:S(2)}) collective-permute-start(bf16[4,240,128]{2,1,0:T(8,128)(2,1)S(1)} %collective-permute-done.10.state_4), channel_id=1, source_target_pairs={{0,24},{8,0},{16,8},{24,16},{1,25},{9,1},{17,9},{25,17},{2,26},{10... | collective-permute-start | bytes 737288 | tf_op jit(solution)/shard_map/ppermute | solution.py:29
  67.4 1.0 convert_reduce_fusion.own
  68.4 0.7 broadcast_in_dim.7
  69.1 7.6 %all-to-all-start.3 = ((bf16[32,24,128]{2,1,0:T(8,128)(2,1)}), bf16[32,24,128]{2,1,0:T(8,128)(2,1)S(1)}, u32[]{:S(2)}, u32[]{:S(2)}) async-start(bf16[32,24,128]{2,1,0:T(8,128)(2,1)} %broadcast_in_dim.7), calls=%async_computation.3 | async-start | bytes 393216 | tf_op jit(solution)/shard_map/all_to_all | solution.py:24
  76.8 2.8 %collective-permute-start.9 = (bf16[4,240,128]{2,1,0:T(8,128)(2,1)S(1)}, bf16[4,240,128]{2,1,0:T(8,128)(2,1)}, u32[]{:S(2)}, u32[]{:S(2)}) collective-permute-start(bf16[4,240,128]{2,1,0:T(8,128)(2,1)S(1)} %shard_map.106.state_0), channel_id=1, source_target_pairs={{0,24},{8,0},{16,8},{24,16},{1,25},{9,1},{17,9},{25,17},{2,26},{10... | collective-permute-start | bytes 737288 | tf_op jit(solution)/shard_map/ppermute | solution.py:29
  79.5 0.8 collective-permute-start.8
  80.3 2.5 %collective-permute-start.13 = (bf16[4,240,128]{2,1,0:T(8,128)(2,1)}, bf16[4,240,128]{2,1,0:T(8,128)(2,1)}, u32[]{:S(2)}, u32[]{:S(2)}) collective-permute-start(bf16[4,240,128]{2,1,0:T(8,128)(2,1)} %collective-permute-done.12.state_7), channel_id=1, source_target_pairs={{0,24},{8,0},{16,8},{24,16},{1,25},{9,1},{17,9},{25,17},{2,26},{10... | collective-permute-start | bytes 737288 | tf_op jit(solution)/shard_map/ppermute | solution.py:29
  82.8 4.2 %all-to-all-done.3.projected = bf16[32,24,128]{2,1,0:T(8,128)(2,1)S(1)} async-done(((bf16[32,24,128]{2,1,0:T(8,128)(2,1)}), bf16[32,24,128]{2,1,0:T(8,128)(2,1)S(1)}, u32[]{:S(2)}, u32[]{:S(2)}) %all-to-all-start.3) | async-done | bytes 196640 | tf_op jit(solution)/shard_map/all_to_all | solution.py:24
  87.4 1.2 %collective-permute-done.1 = f32[8,128]{1,0:T(8,128)S(1)} collective-permute-done((f32[8,128]{1,0:T(8,128)S(1)}, f32[8,128]{1,0:T(8,128)S(1)}, u32[]{:S(2)}, u32[]{:S(2)}) %collective-permute-start.1) | collective-permute-done | bytes 4128 | tf_op jit(solution)/shard_map/ppermute | solution.py:34
  88.6 2.8 %collective-permute-start.4 = (f32[8,128]{1,0:T(8,128)S(1)}, f32[8,128]{1,0:T(8,128)S(1)}, u32[]{:S(2)}, u32[]{:S(2)}) collective-permute-start(f32[8,128]{1,0:T(8,128)S(1)} %add.3.squares_0), channel_id=1, source_target_pairs={{0,6},{2,4},{4,2},{6,0},{1,7},{3,5},{5,3},{7,1},{8,14},{10,12},{12... | collective-permute-start | bytes 12296 | tf_op jit(solution)/shard_map/ppermute | solution.py:34
  91.3 0.8 collective-permute-start.3
  92.1 0.5 collective-permute-start.2
  92.7 0.7 collective-permute-done.8.state_2
  93.4 3.1 %collective-permute-done.3.squares_2 = f32[8,128]{1,0:T(8,128)S(1)} collective-permute-done((f32[8,128]{1,0:T(8,128)S(1)}, f32[8,128]{1,0:T(8,128)S(1)}, u32[]{:S(2)}, u32[]{:S(2)}) %collective-permute-start.3) | collective-permute-done | bytes 4128 | tf_op jit(solution)/shard_map/ppermute | solution.py:34
  96.5 3.6 %shard_map.107 = (f32[3,64,128]{2,1,0:T(8,128)}, f32[3,64,128]{2,1,0:T(8,128)}, bf16[3,2048,128]{2,1,0:T(8,128)(2,1)}, f32[3,8,128]{2,1,0:T(8,128)}, f32[3,8,128]{2,1,0:T(8,128)}) custom-call(f32[8,128]{1,0:T(8,128)S(1)} %add.3.squares_0, f32[8,128]{1,0:T(8,128)S(1)} %collective-permute-done.2.squares_1, f32[8,128]{1,0:T(8,128)S(1)} %collective-permute-done.3.squares_2, ...), custom_call_target="tpu_custom_call" | custom-call | tf_op jit(solution)/shard_map/pallas_call | solution.py:260
  (29 shorter events, 0.5 us)
Async XLA Ops:
  0.6 31.5 %copy-start = (bf16[3,2048,128]{2,1,0:T(8,128)(2,1)S(1)}, bf16[3,2048,128]{2,1,0:T(8,128)(2,1)}, u32[]{:S(2)}) copy-start(bf16[3,2048,128]{2,1,0:T(8,128)(2,1)} %param.7) | copy-start | bytes 4718596
  2.4 21.5 %copy-start.2 = (bf16[1,240,128]{2,1,0:T(8,128)(2,1)S(1)}, bf16[1,240,128]{2,1,0:T(8,128)(2,1)}, u32[]{:S(2)}) copy-start(bf16[1,240,128]{2,1,0:T(8,128)(2,1)} %get-tuple-element.8.a) | copy-start | bytes 184324
  19.4 12.7 %all-to-all-start.1 = ((bf16[4,8,64,128]{3,2,1,0:T(8,128)(2,1)}), bf16[4,8,64,128]{3,2,1,0:T(8,128)(2,1)S(1)}, u32[]{:S(2)}, u32[]{:S(2)}) async-start(bf16[4,8,64,128]{3,2,1,0:T(8,128)(2,1)} %broadcast_in_dim.6), calls=%async_computation.1 | async-start | bytes 1048576 | tf_op jit(solution)/shard_map/all_to_all | solution.py:24
  23.9 22.5 %collective-permute-start.5 = (bf16[1,240,128]{2,1,0:T(8,128)(2,1)S(1)}, bf16[1,240,128]{2,1,0:T(8,128)(2,1)S(1)}, u32[]{:S(2)}, u32[]{:S(2)}) collective-permute-start(bf16[1,240,128]{2,1,0:T(8,128)(2,1)S(1)} %copy-done.2), channel_id=1, source_target_pairs={{0,224},{32,192},{64,160},{96,128},{128,96},{160,64},{192,32},{224... | collective-permute-start | bytes 184328 | tf_op jit(solution)/shard_map/ppermute | solution.py:34
  32.1 4.6 %copy-start.5 = (bf16[2048,2048]{1,0:T(8,128)(2,1)S(1)}, bf16[2048,2048]{1,0:T(8,128)(2,1)}, u32[]{:S(2)}) copy-start(bf16[2048,2048]{1,0:T(8,128)(2,1)} %param.6) | copy-start | bytes 25165828
  32.1 7.1 %collective-permute-start = (bf16[4,8,64,128]{3,2,1,0:T(8,128)(2,1)S(1)}, bf16[4,8,64,128]{3,2,1,0:T(8,128)(2,1)S(1)}, u32[]{:S(2)}, u32[]{:S(2)}) collective-permute-start(bf16[4,8,64,128]{3,2,1,0:T(8,128)(2,1)S(1)} %all-to-all-done.1.mine), channel_id=1, source_target_pairs={{0,1},{1,0},{2,3},{3,2},{4,5},{5,4},{6,7},{7,6},{8,9},{9,8},{10,11... | collective-permute-start | bytes 1572872 | tf_op jit(solution)/shard_map/ppermute | solution.py:29
  40.6 55.9 %copy-start.1 = (f32[3,64,128]{2,1,0:T(8,128)S(1)}, f32[3,64,128]{2,1,0:T(8,128)}, u32[]{:S(2)}) copy-start(f32[3,64,128]{2,1,0:T(8,128)} %weights.3) | copy-start | bytes 294916
  40.6 55.9 %copy-start.3 = (f32[3,8,128]{2,1,0:T(8,128)S(1)}, f32[3,8,128]{2,1,0:T(8,128)}, u32[]{:S(2)}) copy-start(f32[3,8,128]{2,1,0:T(8,128)} %first.3) | copy-start | bytes 36868
  40.6 55.9 %copy-start.4 = (f32[3,8,128]{2,1,0:T(8,128)S(1)}, f32[3,8,128]{2,1,0:T(8,128)}, u32[]{:S(2)}) copy-start(f32[3,8,128]{2,1,0:T(8,128)} %second.3) | copy-start | bytes 36868
  40.6 26.9 %all-to-all-start.2 = ((bf16[32,24,128]{2,1,0:T(8,128)(2,1)}), bf16[32,24,128]{2,1,0:T(8,128)(2,1)}, u32[]{:S(2)}, u32[]{:S(2)}) async-start(bf16[32,24,128]{2,1,0:T(8,128)(2,1)} %shard_map.103), calls=%async_computation.2 | async-start | bytes 393216 | tf_op jit(solution)/shard_map/all_to_all | solution.py:248
  46.4 9.7 %collective-permute-start.6 = (bf16[2,240,128]{2,1,0:T(8,128)(2,1)S(1)}, bf16[2,240,128]{2,1,0:T(8,128)(2,1)S(1)}, u32[]{:S(2)}, u32[]{:S(2)}) collective-permute-start(bf16[2,240,128]{2,1,0:T(8,128)(2,1)S(1)} %shard_map.105.a), channel_id=1, source_target_pairs={{0,64},{32,96},{64,0},{96,32},{128,192},{160,224},{192,128},{224,1... | collective-permute-start | bytes 368648 | tf_op jit(solution)/shard_map/ppermute | solution.py:34
  56.2 8.5 %collective-permute-start.10 = (bf16[4,240,128]{2,1,0:T(8,128)(2,1)S(1)}, bf16[4,240,128]{2,1,0:T(8,128)(2,1)S(1)}, u32[]{:S(2)}, u32[]{:S(2)}) collective-permute-start(bf16[4,240,128]{2,1,0:T(8,128)(2,1)S(1)} %shard_map.106.state_0), channel_id=1, source_target_pairs={{0,32},{32,0},{64,96},{96,64},{128,160},{160,128},{192,224},{224,1... | collective-permute-start | bytes 737288 | tf_op jit(solution)/shard_map/ppermute | solution.py:34
  59.4 20.1 %collective-permute-start.7 = (bf16[4,240,128]{2,1,0:T(8,128)(2,1)S(1)}, bf16[4,240,128]{2,1,0:T(8,128)(2,1)}, u32[]{:S(2)}, u32[]{:S(2)}) collective-permute-start(bf16[4,240,128]{2,1,0:T(8,128)(2,1)S(1)} %shard_map.106.state_0), channel_id=1, source_target_pairs={{0,8},{8,16},{16,24},{24,0},{1,9},{9,17},{17,25},{25,1},{2,10},{10... | collective-permute-start | bytes 737288 | tf_op jit(solution)/shard_map/ppermute | solution.py:29
  64.7 15.7 %collective-permute-start.12 = (bf16[4,240,128]{2,1,0:T(8,128)(2,1)S(1)}, bf16[4,240,128]{2,1,0:T(8,128)(2,1)}, u32[]{:S(2)}, u32[]{:S(2)}) collective-permute-start(bf16[4,240,128]{2,1,0:T(8,128)(2,1)S(1)} %collective-permute-done.10.state_4), channel_id=1, source_target_pairs={{0,24},{8,0},{16,8},{24,16},{1,25},{9,1},{17,9},{25,17},{2,26},{10... | collective-permute-start | bytes 737288 | tf_op jit(solution)/shard_map/ppermute | solution.py:29
  69.1 17.9 %all-to-all-start.3 = ((bf16[32,24,128]{2,1,0:T(8,128)(2,1)}), bf16[32,24,128]{2,1,0:T(8,128)(2,1)S(1)}, u32[]{:S(2)}, u32[]{:S(2)}) async-start(bf16[32,24,128]{2,1,0:T(8,128)(2,1)} %broadcast_in_dim.7), calls=%async_computation.3 | async-start | bytes 393216 | tf_op jit(solution)/shard_map/all_to_all | solution.py:24
  76.8 14.6 %collective-permute-start.9 = (bf16[4,240,128]{2,1,0:T(8,128)(2,1)S(1)}, bf16[4,240,128]{2,1,0:T(8,128)(2,1)}, u32[]{:S(2)}, u32[]{:S(2)}) collective-permute-start(bf16[4,240,128]{2,1,0:T(8,128)(2,1)S(1)} %shard_map.106.state_0), channel_id=1, source_target_pairs={{0,24},{8,0},{16,8},{24,16},{1,25},{9,1},{17,9},{25,17},{2,26},{10... | collective-permute-start | bytes 737288 | tf_op jit(solution)/shard_map/ppermute | solution.py:29
  79.5 12.6 %collective-permute-start.11 = (bf16[4,240,128]{2,1,0:T(8,128)(2,1)S(1)}, bf16[4,240,128]{2,1,0:T(8,128)(2,1)}, u32[]{:S(2)}, u32[]{:S(2)}) collective-permute-start(bf16[4,240,128]{2,1,0:T(8,128)(2,1)S(1)} %collective-permute-done.10.state_4), channel_id=1, source_target_pairs={{0,8},{8,16},{16,24},{24,0},{1,9},{9,17},{17,25},{25,1},{2,10},{10... | collective-permute-start | bytes 737288 | tf_op jit(solution)/shard_map/ppermute | solution.py:29
  79.5 13.8 %collective-permute-start.8 = (bf16[4,240,128]{2,1,0:T(8,128)(2,1)}, bf16[4,240,128]{2,1,0:T(8,128)(2,1)}, u32[]{:S(2)}, u32[]{:S(2)}) collective-permute-start(bf16[4,240,128]{2,1,0:T(8,128)(2,1)} %collective-permute-done.7.state_1), channel_id=1, source_target_pairs={{0,8},{8,16},{16,24},{24,0},{1,9},{9,17},{17,25},{25,1},{2,10},{10... | collective-permute-start | bytes 737288 | tf_op jit(solution)/shard_map/ppermute | solution.py:29
  80.3 13.0 %collective-permute-start.13 = (bf16[4,240,128]{2,1,0:T(8,128)(2,1)}, bf16[4,240,128]{2,1,0:T(8,128)(2,1)}, u32[]{:S(2)}, u32[]{:S(2)}) collective-permute-start(bf16[4,240,128]{2,1,0:T(8,128)(2,1)} %collective-permute-done.12.state_7), channel_id=1, source_target_pairs={{0,24},{8,0},{16,8},{24,16},{1,25},{9,1},{17,9},{25,17},{2,26},{10... | collective-permute-start | bytes 737288 | tf_op jit(solution)/shard_map/ppermute | solution.py:29
  87.1 1.4 %collective-permute-start.1 = (f32[8,128]{1,0:T(8,128)S(1)}, f32[8,128]{1,0:T(8,128)S(1)}, u32[]{:S(2)}, u32[]{:S(2)}) collective-permute-start(f32[8,128]{1,0:T(8,128)S(1)} %shard_map.104), channel_id=1, source_target_pairs={{0,1},{1,0},{2,3},{3,2},{4,5},{5,4},{6,7},{7,6},{8,9},{9,8},{10,11... | collective-permute-start | bytes 12296 | tf_op jit(solution)/shard_map/ppermute | solution.py:34
  88.6 4.8 %collective-permute-start.4 = (f32[8,128]{1,0:T(8,128)S(1)}, f32[8,128]{1,0:T(8,128)S(1)}, u32[]{:S(2)}, u32[]{:S(2)}) collective-permute-start(f32[8,128]{1,0:T(8,128)S(1)} %add.3.squares_0), channel_id=1, source_target_pairs={{0,6},{2,4},{4,2},{6,0},{1,7},{3,5},{5,3},{7,1},{8,14},{10,12},{12... | collective-permute-start | bytes 12296 | tf_op jit(solution)/shard_map/ppermute | solution.py:34
  91.3 5.1 %collective-permute-start.3 = (f32[8,128]{1,0:T(8,128)S(1)}, f32[8,128]{1,0:T(8,128)S(1)}, u32[]{:S(2)}, u32[]{:S(2)}) collective-permute-start(f32[8,128]{1,0:T(8,128)S(1)} %add.3.squares_0), channel_id=1, source_target_pairs={{0,4},{2,6},{4,0},{6,2},{1,5},{3,7},{5,1},{7,3},{8,12},{10,14},{12... | collective-permute-start | bytes 12296 | tf_op jit(solution)/shard_map/ppermute | solution.py:34
  92.1 4.3 %collective-permute-start.2 = (f32[8,128]{1,0:T(8,128)S(1)}, f32[8,128]{1,0:T(8,128)S(1)}, u32[]{:S(2)}, u32[]{:S(2)}) collective-permute-start(f32[8,128]{1,0:T(8,128)S(1)} %add.3.squares_0), channel_id=1, source_target_pairs={{0,2},{2,0},{4,6},{6,4},{1,3},{3,1},{5,7},{7,5},{8,10},{10,8},{12,... | collective-permute-start | bytes 12296 | tf_op jit(solution)/shard_map/ppermute | solution.py:34

commit v11 on v10

--- a/solution.py
+++ b/solution.py
@@ -45,7 +45,7 @@
         out_shape=jax.ShapeDtypeStruct((2 * a.shape[0], *a.shape[1:]), a.dtype),
         in_specs=[VMEM] * 2,
         out_specs=VMEM,
-        compiler_params=pltpu.CompilerParams(vmem_limit_bytes=4 << 20),
+        compiler_params=pltpu.CompilerParams(vmem_limit_bytes=60 << 20),
     )(a, b)
 
 
@@ -102,7 +102,7 @@
 
 
 def final_kernel(
-    squares_0, squares_1, squares_2, squares_3, projected, own,
+    squares_0, squares_1, projected, own,
     state_0, state_1, state_2, state_3, state_4, state_5, state_6, state_7,
     first, second, weights, mine, other,
     update_out, weights_out, copies_out, first_out, second_out,
@@ -122,8 +122,7 @@
     for copy in brought[0] + brought[1]:
         copy.start()
     place = (lax.axis_index(Z), lax.axis_index(Y))
-    squares = (squares_0[...] + squares_1[...]) + (squares_2[...] + squares_3[...])
-    total = jnp.sum(squares, keepdims=True)
+    total = jnp.sum(squares_0[...] + squares_1[...], keepdims=True)
     root_mean = jnp.sqrt(total / (3 * RANK * MW) + 1e-06)
     clip = jnp.minimum(1.0, 0.25 / root_mean)
 
@@ -210,7 +209,10 @@
     hbm = pl.BlockSpec(memory_space=pl.ANY)
     half, state = pl.pallas_call(
         head_kernel,
-        out_shape=(jax.ShapeDtypeStruct((8, 64, 128), BF), jax.ShapeDtypeStruct((1, 240, 128), BF)),
+        out_shape=(
+            jax.ShapeDtypeStruct((8, 64, 128), BF),
+            jax.ShapeDtypeStruct((1, 240, 128), BF),
+        ),
         in_specs=[VMEM] * 4,
         out_specs=(VMEM, VMEM),
         compiler_params=pltpu.CompilerParams(vmem_limit_bytes=60 << 20),
@@ -256,7 +258,8 @@
         compiler_params=pltpu.CompilerParams(vmem_limit_bytes=4 << 20),
     )(projected_all)
     squares += swapped(squares, CORE, 1)
-    squares = [squares] + [swapped(squares, "tp_0", bit) for bit in (1, 2, 3)]
+    squares += swapped(squares, "tp_0", 1)
+    squares = (squares, swapped(squares, "tp_0", 3))
     return pl.pallas_call(
         final_kernel,
         out_shape=(
@@ -266,7 +269,7 @@
             jax.ShapeDtypeStruct((3, 8, 128), F32),
             jax.ShapeDtypeStruct((3, 8, 128), F32),
         ),
-        in_specs=[VMEM] * 6 + [hbm] * 8 + [VMEM] * 5,
+        in_specs=[VMEM] * 4 + [hbm] * 8 + [VMEM] * 5,
         out_specs=(hbm,) * 5,
         scratch_shapes=[
             pltpu.VMEM((3, 64, 128), F32),

time: 102 us -> 105 us (1.029)
  Pallas kernels: 7.4 us -> 10.5 us
  local copies, waits for them, and re-layouts: 2.13 us -> 4.33 us
  starting transfers between devices: 39.8 us -> 38.5 us
    pallas_call x2, Pallas kernels: 0.03 us -> 3.19 us  [joined(): pl.pallas_call(join_kernel, out_shape=jax.ShapeDtypeStruct((2 * a.shape[0...]
    unnamed x12 -> x18, local copies, waits for them, and re-layouts: 0.51 us -> 2.71 us
    ppermute x7 -> x6, waiting for transfers between devices: 15.3 us -> 15.6 us  [swapped(): return lax.ppermute(array, axis, [(i, i ^ bit) for i in range(size)])]
    ppermute x7 -> x6, starting transfers between devices: 11.6 us -> 11.2 us  [swapped(): return lax.ppermute(array, axis, [(i, i ^ bit) for i in range(size)])]
  transfers between devices with their start and end apart: 17 -> 16, of which waited for: 7 -> 7; matrix products, arithmetic and copies ran while one was open for 8% -> 7% of each run, Pallas kernels for 2% -> 5%
where the time goes in v11:
time: 105 us; the launch traced here: 103 us
  starting transfers between devices  38.5 us (37%)
  waiting for transfers between devices  26.6 us (25%)
  blocking collectives  16.1 us (15%)
  Pallas kernels  10.5 us (10%)
  matrix products  5.96 us (6%)
  local copies, waits for them, and re-layouts  4.33 us (4%)
    all_to_all x1, blocking collectives, step(): half = lax.all_to_all(half, Z, split_axis=0, concat_axis=0, tiled=True)  16.1 us
    ppermute x6, waiting for transfers between devices, swapped(): return lax.ppermute(array, axis, [(i, i ^ bit) for i in range(size)])  15.6 us
    all_to_all x2, starting transfers between devices, sent_to_all(): return lax.all_to_all(copies, axis, split_axis=0, concat_axis=0, tiled=True)  11.9 us
    ppermute x6, starting transfers between devices, swapped(): return lax.ppermute(array, axis, [(i, i ^ bit) for i in range(size)])  11.2 us
    all_to_all x2, waiting for transfers between devices, sent_to_all(): return lax.all_to_all(copies, axis, split_axis=0, concat_axis=0, tiled=True)  10.9 us
    ppermute x7, starting transfers between devices, moved(): lax.ppermute(array, axis, [(i, (i + shift) % size) for i in range(size)])  10.2 us
    dot_general x2, matrix products, gradient_of(): jnp.einsum('mtc,td->mcd', cotangents, part, preferred_element_type=F32)  5.96 us
    all_to_all x1, starting transfers between devices, step(): lax.all_to_all(partial_value, FS, split_axis=0, concat_axis=0, tiled=True)  5.18 us
  transfers between devices with their start and end apart: 16, of which 7 were waited for; matrix products, arithmetic and copies ran while one was open for 7% of the time, Pallas kernels for 5%

profile of v11, /device:TPU:32, one launch (start us, length us, event | category | flops | bytes accessed | tf_op | source)
XLA Modules:
  0.0 103.0 jit_solution(10793862453530942548)
XLA Ops:
  0.6 1.7 %shard_map.101 = (bf16[8,64,128]{2,1,0:T(8,128)(2,1)}, bf16[1,240,128]{2,1,0:T(8,128)(2,1)}) custom-call(bf16[64,256]{1,0:T(8,128)(2,1)} %factor.1, f32[3,64,128]{2,1,0:T(8,128)} %weights.3, f32[3,8,128]{2,1,0:T(8,128)} %first.3, f32[3,8,128]{2,1,0:T(8,128)} %second.3), custom_call_target="tpu_custom_call" | custom-call | tf_op jit(solution)/shard_map/pallas_call | solution.py:210
  2.4 16.1 %all_to_all.20 = bf16[8,64,128]{2,1,0:T(8,128)(2,1)S(1)} all-to-all(bf16[8,64,128]{2,1,0:T(8,128)(2,1)} %get-tuple-element.7), channel_id=1, replica_groups=mesh['fs_0'=8,'fs_1'=4,'tp_0'=4,'tp_1'=2] {'fs_0'}, dimensions={0} | all-to-all | bytes 262144 | tf_op jit(solution)/shard_map/all_to_all | solution.py:220
  18.5 0.9 broadcast_in_dim.6
  19.4 4.5 %all-to-all-start.1 = ((bf16[4,8,64,128]{3,2,1,0:T(8,128)(2,1)}), bf16[4,8,64,128]{3,2,1,0:T(8,128)(2,1)S(1)}, u32[]{:S(2)}, u32[]{:S(2)}) async-start(bf16[4,8,64,128]{3,2,1,0:T(8,128)(2,1)} %broadcast_in_dim.6), calls=%async_computation.1 | async-start | bytes 1048576 | tf_op jit(solution)/shard_map/all_to_all | solution.py:24
  23.9 1.5 %collective-permute-start.4 = (bf16[1,240,128]{2,1,0:T(8,128)(2,1)S(1)}, bf16[1,240,128]{2,1,0:T(8,128)(2,1)S(1)}, u32[]{:S(2)}, u32[]{:S(2)}) collective-permute-start(bf16[1,240,128]{2,1,0:T(8,128)(2,1)S(1)} %copy-done.6), channel_id=1, source_target_pairs={{0,224},{32,192},{64,160},{96,128},{128,96},{160,64},{192,32},{224... | collective-permute-start | bytes 184328 | tf_op jit(solution)/shard_map/ppermute | solution.py:34
  25.3 6.8 %all-to-all-done.1.mine = bf16[4,8,64,128]{3,2,1,0:T(8,128)(2,1)S(1)} async-done(((bf16[4,8,64,128]{3,2,1,0:T(8,128)(2,1)}), bf16[4,8,64,128]{3,2,1,0:T(8,128)(2,1)S(1)}, u32[]{:S(2)}, u32[]{:S(2)}) %all-to-all-start.1) | async-done | bytes 524320 | tf_op jit(solution)/shard_map/all_to_all | solution.py:24
  32.1 4.1 %fusion.9 = bf16[3,128,1024]{2,1,0:T(8,128)(2,1)S(1)} fusion(bf16[3,2048,128]{2,1,0:T(8,128)(2,1)S(1)} %copy-done, bf16[2048,2048]{1,0:T(8,128)(2,1)} %param.6), kind=kOutput, calls=%fused_computation.7 | convolution fusion | flops 1611005952 | bytes 6553600 | tf_op jit(solution)/shard_map/mtc,td->mcd/dot_general | solution.py:228
  36.7 1.8 %fusion.6 = bf16[3,128,1024]{2,1,0:T(8,128)(2,1)S(1)} fusion(bf16[3,2048,128]{2,1,0:T(8,128)(2,1)S(1)} %copy-done, bf16[2048,2048]{1,0:T(8,128)(2,1)S(1)} %copy-done.8), kind=kOutput, calls=%fused_computation.6 | convolution fusion | flops 1611005952 | bytes 6553600 | tf_op jit(solution)/shard_map/mtc,td->mcd/dot_general | solution.py:228
  38.6 0.6 shard_map.102.before
  39.2 1.3 %shard_map.103 = bf16[32,24,128]{2,1,0:T(8,128)(2,1)} custom-call(bf16[384,1024]{1,0:T(8,128)(2,1)S(1)} %bitcast.17, bf16[384,1024]{1,0:T(8,128)(2,1)S(1)} %bitcast.15, bf16[4,8,64,128]{3,2,1,0:T(8,128)(2,1)S(1)} %collective-permute-done.other, bf16[16,24,128]{2,1,0:T(8,128)(2,1)S(1)} %shard_map.102.before), custom_call_target="tpu_custom_call" | custom-call | tf_op jit(solution)/shard_map/pallas_call | solution.py:243
  40.6 5.2 %all-to-all-start.2 = ((bf16[32,24,128]{2,1,0:T(8,128)(2,1)}), bf16[32,24,128]{2,1,0:T(8,128)(2,1)S(1)}, u32[]{:S(2)}, u32[]{:S(2)}) async-start(bf16[32,24,128]{2,1,0:T(8,128)(2,1)} %shard_map.103), calls=%async_computation.2 | async-start | bytes 393216 | tf_op jit(solution)/shard_map/all_to_all | solution.py:250
  46.4 1.5 %shard_map.105.a = bf16[2,240,128]{2,1,0:T(8,128)(2,1)} custom-call(bf16[1,240,128]{2,1,0:T(8,128)(2,1)} %get-tuple-element.8.a, bf16[1,240,128]{2,1,0:T(8,128)(2,1)} %copy-done.7), custom_call_target="tpu_custom_call" | custom-call | tf_op jit(solution)/shard_map/pallas_call | solution.py:43
  47.9 2.4 %collective-permute-start.5 = (bf16[2,240,128]{2,1,0:T(8,128)(2,1)}, bf16[2,240,128]{2,1,0:T(8,128)(2,1)S(1)}, u32[]{:S(2)}, u32[]{:S(2)}) collective-permute-start(bf16[2,240,128]{2,1,0:T(8,128)(2,1)} %shard_map.105.a), channel_id=1, source_target_pairs={{0,64},{32,96},{64,0},{96,32},{128,192},{160,224},{192,128},{224,1... | collective-permute-start | bytes 368648 | tf_op jit(solution)/shard_map/ppermute | solution.py:34
  50.3 5.8 %collective-permute-done.5.b = bf16[2,240,128]{2,1,0:T(8,128)(2,1)S(1)} collective-permute-done((bf16[2,240,128]{2,1,0:T(8,128)(2,1)}, bf16[2,240,128]{2,1,0:T(8,128)(2,1)S(1)}, u32[]{:S(2)}, u32[]{:S(2)}) %collective-permute-start.5) | collective-permute-done | bytes 122912 | tf_op jit(solution)/shard_map/ppermute | solution.py:34
  56.8 1.7 %shard_map.106.state_0 = bf16[4,240,128]{2,1,0:T(8,128)(2,1)} custom-call(bf16[2,240,128]{2,1,0:T(8,128)(2,1)} %shard_map.105.a, bf16[2,240,128]{2,1,0:T(8,128)(2,1)} %copy-done.5), custom_call_target="tpu_custom_call" | custom-call | tf_op jit(solution)/shard_map/pallas_call | solution.py:43
  58.4 2.8 %collective-permute-start.9 = (bf16[4,240,128]{2,1,0:T(8,128)(2,1)}, bf16[4,240,128]{2,1,0:T(8,128)(2,1)S(1)}, u32[]{:S(2)}, u32[]{:S(2)}) collective-permute-start(bf16[4,240,128]{2,1,0:T(8,128)(2,1)} %shard_map.106.state_0), channel_id=1, source_target_pairs={{0,32},{32,0},{64,96},{96,64},{128,160},{160,128},{192,224},{224,1... | collective-permute-start | bytes 737288 | tf_op jit(solution)/shard_map/ppermute | solution.py:34
  61.2 1.5 %collective-permute-start.6 = (bf16[4,240,128]{2,1,0:T(8,128)(2,1)}, bf16[4,240,128]{2,1,0:T(8,128)(2,1)S(1)}, u32[]{:S(2)}, u32[]{:S(2)}) collective-permute-start(bf16[4,240,128]{2,1,0:T(8,128)(2,1)} %shard_map.106.state_0), channel_id=1, source_target_pairs={{0,8},{8,16},{16,24},{24,0},{1,9},{9,17},{17,25},{25,1},{2,10},{10... | collective-permute-start | bytes 737288 | tf_op jit(solution)/shard_map/ppermute | solution.py:29
  62.7 4.5 %collective-permute-done.9.state_4 = bf16[4,240,128]{2,1,0:T(8,128)(2,1)S(1)} collective-permute-done((bf16[4,240,128]{2,1,0:T(8,128)(2,1)}, bf16[4,240,128]{2,1,0:T(8,128)(2,1)S(1)}, u32[]{:S(2)}, u32[]{:S(2)}) %collective-permute-start.9) | collective-permute-done | bytes 245792 | tf_op jit(solution)/shard_map/ppermute | solution.py:34
  67.3 2.7 %collective-permute-start.11 = (bf16[4,240,128]{2,1,0:T(8,128)(2,1)S(1)}, bf16[4,240,128]{2,1,0:T(8,128)(2,1)}, u32[]{:S(2)}, u32[]{:S(2)}) collective-permute-start(bf16[4,240,128]{2,1,0:T(8,128)(2,1)S(1)} %collective-permute-done.9.state_4), channel_id=1, source_target_pairs={{0,24},{8,0},{16,8},{24,16},{1,25},{9,1},{17,9},{25,17},{2,26},{10... | collective-permute-start | bytes 737288 | tf_op jit(solution)/shard_map/ppermute | solution.py:29
  70.0 0.7 broadcast_in_dim.7
  70.7 7.4 %all-to-all-start.3 = ((bf16[32,24,128]{2,1,0:T(8,128)(2,1)}), bf16[32,24,128]{2,1,0:T(8,128)(2,1)S(1)}, u32[]{:S(2)}, u32[]{:S(2)}) async-start(bf16[32,24,128]{2,1,0:T(8,128)(2,1)} %broadcast_in_dim.7), calls=%async_computation.3 | async-start | bytes 393216 | tf_op jit(solution)/shard_map/all_to_all | solution.py:24
  78.2 2.8 %collective-permute-start.8 = (bf16[4,240,128]{2,1,0:T(8,128)(2,1)}, bf16[4,240,128]{2,1,0:T(8,128)(2,1)}, u32[]{:S(2)}, u32[]{:S(2)}) collective-permute-start(bf16[4,240,128]{2,1,0:T(8,128)(2,1)} %shard_map.106.state_0), channel_id=1, source_target_pairs={{0,24},{8,0},{16,8},{24,16},{1,25},{9,1},{17,9},{25,17},{2,26},{10... | collective-permute-start | bytes 737288 | tf_op jit(solution)/shard_map/ppermute | solution.py:29
  80.9 0.8 collective-permute-start.7
  81.7 2.5 %collective-permute-start.12 = (bf16[4,240,128]{2,1,0:T(8,128)(2,1)}, bf16[4,240,128]{2,1,0:T(8,128)(2,1)}, u32[]{:S(2)}, u32[]{:S(2)}) collective-permute-start(bf16[4,240,128]{2,1,0:T(8,128)(2,1)} %collective-permute-done.11.state_7), channel_id=1, source_target_pairs={{0,24},{8,0},{16,8},{24,16},{1,25},{9,1},{17,9},{25,17},{2,26},{10... | collective-permute-start | bytes 737288 | tf_op jit(solution)/shard_map/ppermute | solution.py:29
  84.2 4.1 %all-to-all-done.3.projected = bf16[32,24,128]{2,1,0:T(8,128)(2,1)S(1)} async-done(((bf16[32,24,128]{2,1,0:T(8,128)(2,1)}), bf16[32,24,128]{2,1,0:T(8,128)(2,1)S(1)}, u32[]{:S(2)}, u32[]{:S(2)}) %all-to-all-start.3) | async-done | bytes 196640 | tf_op jit(solution)/shard_map/all_to_all | solution.py:24
  88.8 1.2 %collective-permute-done.1 = f32[8,128]{1,0:T(8,128)S(1)} collective-permute-done((f32[8,128]{1,0:T(8,128)S(1)}, f32[8,128]{1,0:T(8,128)S(1)}, u32[]{:S(2)}, u32[]{:S(2)}) %collective-permute-start.1) | collective-permute-done | bytes 4128 | tf_op jit(solution)/shard_map/ppermute | solution.py:34
  89.9 1.5 %collective-permute-start.2 = (f32[8,128]{1,0:T(8,128)S(1)}, f32[8,128]{1,0:T(8,128)S(1)}, u32[]{:S(2)}, u32[]{:S(2)}) collective-permute-start(f32[8,128]{1,0:T(8,128)S(1)} %add.6), channel_id=1, source_target_pairs={{0,2},{2,0},{4,6},{6,4},{1,3},{3,1},{5,7},{7,5},{8,10},{10,8},{12,... | collective-permute-start | bytes 12296 | tf_op jit(solution)/shard_map/ppermute | solution.py:34
  91.4 2.1 %collective-permute-done.2 = f32[8,128]{1,0:T(8,128)S(1)} collective-permute-done((f32[8,128]{1,0:T(8,128)S(1)}, f32[8,128]{1,0:T(8,128)S(1)}, u32[]{:S(2)}, u32[]{:S(2)}) %collective-permute-start.2) | collective-permute-done | bytes 4128 | tf_op jit(solution)/shard_map/ppermute | solution.py:34
  93.5 2.8 %collective-permute-start.3 = (f32[8,128]{1,0:T(8,128)S(1)}, f32[8,128]{1,0:T(8,128)S(1)}, u32[]{:S(2)}, u32[]{:S(2)}) collective-permute-start(f32[8,128]{1,0:T(8,128)S(1)} %add.7.squares_0), channel_id=1, source_target_pairs={{0,6},{2,4},{4,2},{6,0},{1,7},{3,5},{5,3},{7,1},{8,14},{10,12},{12... | collective-permute-start | bytes 12296 | tf_op jit(solution)/shard_map/ppermute | solution.py:34
  96.3 2.0 %collective-permute-done.3.squares_1 = f32[8,128]{1,0:T(8,128)S(1)} collective-permute-done((f32[8,128]{1,0:T(8,128)S(1)}, f32[8,128]{1,0:T(8,128)S(1)}, u32[]{:S(2)}, u32[]{:S(2)}) %collective-permute-start.3) | collective-permute-done | bytes 4128 | tf_op jit(solution)/shard_map/ppermute | solution.py:34
  98.4 0.9 copy-done.1
  99.3 3.5 %shard_map.107 = (f32[3,64,128]{2,1,0:T(8,128)}, f32[3,64,128]{2,1,0:T(8,128)}, bf16[3,2048,128]{2,1,0:T(8,128)(2,1)}, f32[3,8,128]{2,1,0:T(8,128)}, f32[3,8,128]{2,1,0:T(8,128)}) custom-call(f32[8,128]{1,0:T(8,128)S(1)} %add.7.squares_0, f32[8,128]{1,0:T(8,128)S(1)} %collective-permute-done.3.squares_1, bf16[32,24,128]{2,1,0:T(8,128)(2,1)S(1)} %all-to-all-done.3.projected, ...), custom_call_target="tpu_custom_call" | custom-call | tf_op jit(solution)/shard_map/pallas_call | solution.py:263
  (34 shorter events, 2.2 us)
Async XLA Ops:
  0.6 31.5 %copy-start = (bf16[3,2048,128]{2,1,0:T(8,128)(2,1)S(1)}, bf16[3,2048,128]{2,1,0:T(8,128)(2,1)}, u32[]{:S(2)}) copy-start(bf16[3,2048,128]{2,1,0:T(8,128)(2,1)} %param.7) | copy-start | bytes 4718596
  2.4 21.5 %copy-start.6 = (bf16[1,240,128]{2,1,0:T(8,128)(2,1)S(1)}, bf16[1,240,128]{2,1,0:T(8,128)(2,1)}, u32[]{:S(2)}) copy-start(bf16[1,240,128]{2,1,0:T(8,128)(2,1)} %get-tuple-element.8.a) | copy-start | bytes 184324
  19.4 12.7 %all-to-all-start.1 = ((bf16[4,8,64,128]{3,2,1,0:T(8,128)(2,1)}), bf16[4,8,64,128]{3,2,1,0:T(8,128)(2,1)S(1)}, u32[]{:S(2)}, u32[]{:S(2)}) async-start(bf16[4,8,64,128]{3,2,1,0:T(8,128)(2,1)} %broadcast_in_dim.6), calls=%async_computation.1 | async-start | bytes 1048576 | tf_op jit(solution)/shard_map/all_to_all | solution.py:24
  23.9 21.9 %collective-permute-start.4 = (bf16[1,240,128]{2,1,0:T(8,128)(2,1)S(1)}, bf16[1,240,128]{2,1,0:T(8,128)(2,1)S(1)}, u32[]{:S(2)}, u32[]{:S(2)}) collective-permute-start(bf16[1,240,128]{2,1,0:T(8,128)(2,1)S(1)} %copy-done.6), channel_id=1, source_target_pairs={{0,224},{32,192},{64,160},{96,128},{128,96},{160,64},{192,32},{224... | collective-permute-start | bytes 184328 | tf_op jit(solution)/shard_map/ppermute | solution.py:34
  32.1 4.6 %copy-start.8 = (bf16[2048,2048]{1,0:T(8,128)(2,1)S(1)}, bf16[2048,2048]{1,0:T(8,128)(2,1)}, u32[]{:S(2)}) copy-start(bf16[2048,2048]{1,0:T(8,128)(2,1)} %param.6) | copy-start | bytes 25165828
  32.1 7.1 %collective-permute-start = (bf16[4,8,64,128]{3,2,1,0:T(8,128)(2,1)S(1)}, bf16[4,8,64,128]{3,2,1,0:T(8,128)(2,1)S(1)}, u32[]{:S(2)}, u32[]{:S(2)}) collective-permute-start(bf16[4,8,64,128]{3,2,1,0:T(8,128)(2,1)S(1)} %all-to-all-done.1.mine), channel_id=1, source_target_pairs={{0,1},{1,0},{2,3},{3,2},{4,5},{5,4},{6,7},{7,6},{8,9},{9,8},{10,11... | collective-permute-start | bytes 1572872 | tf_op jit(solution)/shard_map/ppermute | solution.py:29
  40.5 57.8 %copy-start.2 = (f32[3,64,128]{2,1,0:T(8,128)S(1)}, f32[3,64,128]{2,1,0:T(8,128)}, u32[]{:S(2)}) copy-start(f32[3,64,128]{2,1,0:T(8,128)} %weights.3) | copy-start | bytes 294916
  40.6 57.8 %copy-start.3 = (f32[3,8,128]{2,1,0:T(8,128)S(1)}, f32[3,8,128]{2,1,0:T(8,128)}, u32[]{:S(2)}) copy-start(f32[3,8,128]{2,1,0:T(8,128)} %first.3) | copy-start | bytes 36868
  40.6 57.8 %copy-start.4 = (f32[3,8,128]{2,1,0:T(8,128)S(1)}, f32[3,8,128]{2,1,0:T(8,128)}, u32[]{:S(2)}) copy-start(f32[3,8,128]{2,1,0:T(8,128)} %second.3) | copy-start | bytes 36868
  40.6 29.4 %all-to-all-start.2 = ((bf16[32,24,128]{2,1,0:T(8,128)(2,1)}), bf16[32,24,128]{2,1,0:T(8,128)(2,1)S(1)}, u32[]{:S(2)}, u32[]{:S(2)}) async-start(bf16[32,24,128]{2,1,0:T(8,128)(2,1)} %shard_map.103), calls=%async_computation.2 | async-start | bytes 393216 | tf_op jit(solution)/shard_map/all_to_all | solution.py:250
  45.8 0.6 copy-start.7
  47.9 8.2 %collective-permute-start.5 = (bf16[2,240,128]{2,1,0:T(8,128)(2,1)}, bf16[2,240,128]{2,1,0:T(8,128)(2,1)S(1)}, u32[]{:S(2)}, u32[]{:S(2)}) collective-permute-start(bf16[2,240,128]{2,1,0:T(8,128)(2,1)} %shard_map.105.a), channel_id=1, source_target_pairs={{0,64},{32,96},{64,0},{96,32},{128,192},{160,224},{192,128},{224,1... | collective-permute-start | bytes 368648 | tf_op jit(solution)/shard_map/ppermute | solution.py:34
  56.1 0.6 copy-start.5
  58.4 8.8 %collective-permute-start.9 = (bf16[4,240,128]{2,1,0:T(8,128)(2,1)}, bf16[4,240,128]{2,1,0:T(8,128)(2,1)S(1)}, u32[]{:S(2)}, u32[]{:S(2)}) collective-permute-start(bf16[4,240,128]{2,1,0:T(8,128)(2,1)} %shard_map.106.state_0), channel_id=1, source_target_pairs={{0,32},{32,0},{64,96},{96,64},{128,160},{160,128},{192,224},{224,1... | collective-permute-start | bytes 737288 | tf_op jit(solution)/shard_map/ppermute | solution.py:34
  61.2 19.7 %collective-permute-start.6 = (bf16[4,240,128]{2,1,0:T(8,128)(2,1)}, bf16[4,240,128]{2,1,0:T(8,128)(2,1)S(1)}, u32[]{:S(2)}, u32[]{:S(2)}) collective-permute-start(bf16[4,240,128]{2,1,0:T(8,128)(2,1)} %shard_map.106.state_0), channel_id=1, source_target_pairs={{0,8},{8,16},{16,24},{24,0},{1,9},{9,17},{17,25},{25,1},{2,10},{10... | collective-permute-start | bytes 737288 | tf_op jit(solution)/shard_map/ppermute | solution.py:29
  67.3 14.5 %collective-permute-start.11 = (bf16[4,240,128]{2,1,0:T(8,128)(2,1)S(1)}, bf16[4,240,128]{2,1,0:T(8,128)(2,1)}, u32[]{:S(2)}, u32[]{:S(2)}) collective-permute-start(bf16[4,240,128]{2,1,0:T(8,128)(2,1)S(1)} %collective-permute-done.9.state_4), channel_id=1, source_target_pairs={{0,24},{8,0},{16,8},{24,16},{1,25},{9,1},{17,9},{25,17},{2,26},{10... | collective-permute-start | bytes 737288 | tf_op jit(solution)/shard_map/ppermute | solution.py:29
  70.7 17.7 %all-to-all-start.3 = ((bf16[32,24,128]{2,1,0:T(8,128)(2,1)}), bf16[32,24,128]{2,1,0:T(8,128)(2,1)S(1)}, u32[]{:S(2)}, u32[]{:S(2)}) async-start(bf16[32,24,128]{2,1,0:T(8,128)(2,1)} %broadcast_in_dim.7), calls=%async_computation.3 | async-start | bytes 393216 | tf_op jit(solution)/shard_map/all_to_all | solution.py:24
  78.2 18.1 %collective-permute-start.8 = (bf16[4,240,128]{2,1,0:T(8,128)(2,1)}, bf16[4,240,128]{2,1,0:T(8,128)(2,1)}, u32[]{:S(2)}, u32[]{:S(2)}) collective-permute-start(bf16[4,240,128]{2,1,0:T(8,128)(2,1)} %shard_map.106.state_0), channel_id=1, source_target_pairs={{0,24},{8,0},{16,8},{24,16},{1,25},{9,1},{17,9},{25,17},{2,26},{10... | collective-permute-start | bytes 737288 | tf_op jit(solution)/shard_map/ppermute | solution.py:29
  80.9 15.4 %collective-permute-start.10 = (bf16[4,240,128]{2,1,0:T(8,128)(2,1)S(1)}, bf16[4,240,128]{2,1,0:T(8,128)(2,1)}, u32[]{:S(2)}, u32[]{:S(2)}) collective-permute-start(bf16[4,240,128]{2,1,0:T(8,128)(2,1)S(1)} %collective-permute-done.9.state_4), channel_id=1, source_target_pairs={{0,8},{8,16},{16,24},{24,0},{1,9},{9,17},{17,25},{25,1},{2,10},{10... | collective-permute-start | bytes 737288 | tf_op jit(solution)/shard_map/ppermute | solution.py:29
  80.9 15.4 %collective-permute-start.7 = (bf16[4,240,128]{2,1,0:T(8,128)(2,1)S(1)}, bf16[4,240,128]{2,1,0:T(8,128)(2,1)}, u32[]{:S(2)}, u32[]{:S(2)}) collective-permute-start(bf16[4,240,128]{2,1,0:T(8,128)(2,1)S(1)} %collective-permute-done.6.state_1), channel_id=1, source_target_pairs={{0,8},{8,16},{16,24},{24,0},{1,9},{9,17},{17,25},{25,1},{2,10},{10... | collective-permute-start | bytes 737288 | tf_op jit(solution)/shard_map/ppermute | solution.py:29
  81.7 14.6 %collective-permute-start.12 = (bf16[4,240,128]{2,1,0:T(8,128)(2,1)}, bf16[4,240,128]{2,1,0:T(8,128)(2,1)}, u32[]{:S(2)}, u32[]{:S(2)}) collective-permute-start(bf16[4,240,128]{2,1,0:T(8,128)(2,1)} %collective-permute-done.11.state_7), channel_id=1, source_target_pairs={{0,24},{8,0},{16,8},{24,16},{1,25},{9,1},{17,9},{25,17},{2,26},{10... | collective-permute-start | bytes 737288 | tf_op jit(solution)/shard_map/ppermute | solution.py:29
  88.5 1.4 %collective-permute-start.1 = (f32[8,128]{1,0:T(8,128)S(1)}, f32[8,128]{1,0:T(8,128)S(1)}, u32[]{:S(2)}, u32[]{:S(2)}) collective-permute-start(f32[8,128]{1,0:T(8,128)S(1)} %shard_map.104), channel_id=1, source_target_pairs={{0,1},{1,0},{2,3},{3,2},{4,5},{5,4},{6,7},{7,6},{8,9},{9,8},{10,11... | collective-permute-start | bytes 12296 | tf_op jit(solution)/shard_map/ppermute | solution.py:34
  89.9 3.6 %collective-permute-start.2 = (f32[8,128]{1,0:T(8,128)S(1)}, f32[8,128]{1,0:T(8,128)S(1)}, u32[]{:S(2)}, u32[]{:S(2)}) collective-permute-start(f32[8,128]{1,0:T(8,128)S(1)} %add.6), channel_id=1, source_target_pairs={{0,2},{2,0},{4,6},{6,4},{1,3},{3,1},{5,7},{7,5},{8,10},{10,8},{12,... | collective-permute-start | bytes 12296 | tf_op jit(solution)/shard_map/ppermute | solution.py:34
  93.5 4.8 %collective-permute-start.3 = (f32[8,128]{1,0:T(8,128)S(1)}, f32[8,128]{1,0:T(8,128)S(1)}, u32[]{:S(2)}, u32[]{:S(2)}) collective-permute-start(f32[8,128]{1,0:T(8,128)S(1)} %add.7.squares_0), channel_id=1, source_target_pairs={{0,6},{2,4},{4,2},{6,0},{1,7},{3,5},{5,3},{7,1},{8,14},{10,12},{12... | collective-permute-start | bytes 12296 | tf_op jit(solution)/shard_map/ppermute | solution.py:34
  98.4 0.9 copy-start.1
